TPU v7x, 128 devices: a whole 4x4x4 slice. The times are simulated.
128 devices in a mesh: ep: 16 (over z, x), tp: 8 (over y, core).
Axes of the slice: x: 4, y: 4, z: 4, core: 2. Of those that a mesh axis runs over, the one named last changes fastest.
Arguments:
- mix_query: bfloat16 [32768, 2048], P('ep', 'tp'), may hold values from -6 to 6
- mix_key: bfloat16 [32768, 2048], P('ep', 'tp'), may hold values from -6 to 6
- mix_value: bfloat16 [32768, 2048], P('ep', 'tp'), may hold values from -6 to 6
- mix_gate: bfloat16 [32768, 2048], P('ep', 'tp'), may hold values from -6 to 6
- log_decay: float32 [32768, 8], P('ep', 'tp'), may hold values from -1 to 0, as said below
- ret_gain: float32 [2048], P('tp'), may hold values from 0.1 to 1.9
- w_out: bfloat16 [2048, 2048], replicated, may hold values from -0.125 to 0.125
- moe_in: bfloat16 [4096, 2048], P(('ep', 'tp')), may hold values from -6 to 6
- route_ids: int32 [4096, 2], P(('ep', 'tp')), may hold values from 0 to 15, as said below
- route_weights: float32 [4096, 2], P(('ep', 'tp')), may hold values from 0.1 to 1
- moe_gain: float32 [2048], replicated, may hold values from 0.1 to 1.9
- w_gate: bfloat16 [16, 2048, 7168], P('ep', None, 'tp'), may hold values from -0.125 to 0.125
- w_up: bfloat16 [16, 2048, 7168], P('ep', None, 'tp'), may hold values from -0.125 to 0.125
- w_down: bfloat16 [16, 7168, 2048], P('ep', 'tp'), may hold values from -0.0625 to 0.0625
Outputs:
- mix_out: bfloat16 [32768, 2048], P(('ep', 'tp'))
- moe_out: bfloat16 [4096, 2048], P(('ep', 'tp'))
Inputs may be any that keep to these rules, and one draw needn't show every extreme that they name: `log_decay`: log of a decay. `route_ids`: each row names 2 different experts. Among the rows of one device no expert is named by more than 8 rows, and one expert is named by exactly 8 rows of every device.
All inputs are finite; a program needn't handle non-finite values.
Results may differ from a plain program's by a relative error of at most 0.015.
Values may be sent and summed in bfloat16 or wider, within the bound.
No kernel may reach another device: no remote copies, remote signals or barrier semaphores. Data moves between devices by JAX's collectives and lax.ppermute only.
A program may use at most 128 MiB of HBM per device.

v0:
```python
import jax
import jax.numpy as jnp
from jax import lax
from jax.sharding import PartitionSpec as P

HEAD_DIM = 256
BLOCK = 512


norm_eps = 1e-06


def from_everyone(x, axis):
    copies = jnp.broadcast_to(x, (lax.axis_size(axis), *x.shape))
    return lax.all_to_all(copies, axis, split_axis=0, concat_axis=0, tiled=True)


def joined_by_halves(pieces, combine):
    while len(jax.tree.leaves(pieces)[0]) > 1:
        pieces = jax.vmap(combine)(
            *(jax.tree.map(lambda part: part[side::2], pieces) for side in (0, 1))
        )
    return jax.tree.map(lambda part: part[0], pieces)


def prefix(x, axis, combine, identity):
    length, position = (lax.axis_size(axis), lax.axis_index(axis))
    passed = jnp.arange(length) < position

    def kept(part, zero, own):
        part = jnp.where(
            passed.reshape(-1, *(1 for _ in own.shape)),
            part.astype(own.dtype),
            jnp.asarray(zero, own.dtype),
        )
        return part

    pieces = jax.tree.map(
        lambda part: from_everyone(part, axis),
        jax.tree.map(lambda part, kind: part.astype(kind), x, (jnp.bfloat16, jnp.bfloat16)),
    )
    return joined_by_halves(jax.tree.map(kept, pieces, identity, x), combine)


def rotate(tensor, position_index):
    head_dim = tensor.shape[-1]
    half_dim = head_dim // 2
    inverse = 10000.0 ** (-(jnp.arange(half_dim, dtype=jnp.float32) * 2.0) / head_dim)
    angle = position_index.astype(jnp.float32)[:, None] * inverse[None, :]
    cosine = jnp.cos(angle)[:, None, :]
    sine = jnp.sin(angle)[:, None, :]
    front = tensor[..., :half_dim]
    back = tensor[..., half_dim:]
    return jnp.concatenate([front * cosine - back * sine, back * cosine + front * sine], axis=-1)


def chain(earlier, later):
    return (earlier[0] * later[0], later[0][:, None, None] * earlier[1] + later[1])


def carry_block(carried, block_items):
    update, block_last = block_items
    return (jnp.exp(block_last)[:, None, None] * carried + update, carried)


def mixer_half(mix_query, mix_key, mix_value, mix_gate, log_decay, ret_gain, w_out):
    seq_rows = mix_query.shape[0]
    local_heads = mix_query.shape[1] // HEAD_DIM
    block_count = seq_rows // BLOCK
    position_index = lax.axis_index("ep") * seq_rows + jnp.arange(seq_rows, dtype=jnp.int32)
    query_rot = rotate(
        mix_query.astype(jnp.float32).reshape(seq_rows, local_heads, HEAD_DIM), position_index
    ).astype(jnp.bfloat16)
    key_rot = (
        rotate(mix_key.astype(jnp.float32).reshape(seq_rows, local_heads, HEAD_DIM), position_index)
        * HEAD_DIM ** (-0.5)
    ).astype(jnp.bfloat16)
    query_blocks = query_rot.reshape(block_count, BLOCK, local_heads, HEAD_DIM)
    key_blocks = key_rot.reshape(block_count, BLOCK, local_heads, HEAD_DIM)
    value_blocks = mix_value.reshape(block_count, BLOCK, local_heads, HEAD_DIM)
    cumulative = jnp.cumsum(log_decay.reshape(block_count, BLOCK, local_heads), axis=1)
    causal = jnp.arange(BLOCK)[:, None] >= jnp.arange(BLOCK)[None, :]
    scores = jnp.einsum(
        "nihd,njhd->nhij", query_blocks, key_blocks, preferred_element_type=jnp.float32
    )
    by_head = jnp.transpose(cumulative, (0, 2, 1))
    log_gap = by_head[:, :, :, None] - by_head[:, :, None, :]
    decay_mask = jnp.where(causal, jnp.exp(jnp.where(causal, log_gap, 0.0)), 0.0)
    weights = (scores * decay_mask).astype(jnp.bfloat16)
    within_block = jnp.einsum(
        "nhij,njhe->nihe", weights, value_blocks, preferred_element_type=jnp.float32
    )
    block_last = cumulative[:, -1, :]
    key_decayed = (
        key_blocks.astype(jnp.float32) * jnp.exp(block_last[:, None, :] - cumulative)[..., None]
    ).astype(jnp.bfloat16)
    updates = jnp.einsum(
        "njhd,njhe->nhde", key_decayed, value_blocks, preferred_element_type=jnp.float32
    )
    empty_state = jnp.zeros((local_heads, HEAD_DIM, HEAD_DIM), jnp.float32)
    local_end, starts = lax.scan(carry_block, empty_state, (updates, block_last))
    through = jnp.cumsum(block_last, axis=0)
    before = through - block_last
    incoming = prefix(
        (jnp.exp(through[-1]), local_end), "ep", chain, (jnp.ones_like(through[-1]), empty_state)
    )
    block_states = starts + jnp.exp(before)[:, :, None, None] * incoming[1][None]
    query_decayed = query_blocks.astype(jnp.float32) * jnp.exp(cumulative)[..., None]
    carried_part = jnp.einsum(
        "nihd,nhde->nihe", query_decayed, block_states, precision=lax.Precision.HIGHEST
    )
    retained = (within_block + carried_part).reshape(seq_rows, local_heads, HEAD_DIM)
    inverse_rms = lax.rsqrt(jnp.mean(retained * retained, axis=-1, keepdims=True) + norm_eps)
    gate_act = jax.nn.silu(mix_gate.astype(jnp.float32).reshape(seq_rows, local_heads, HEAD_DIM))
    heads_out = (
        gate_act * retained * inverse_rms * ret_gain.reshape(local_heads, HEAD_DIM)
    ).astype(jnp.bfloat16)
    by_rows = lax.all_to_all(
        heads_out.reshape(seq_rows, local_heads * HEAD_DIM),
        "tp",
        split_axis=0,
        concat_axis=1,
        tiled=True,
    )
    return jnp.dot(by_rows, w_out, preferred_element_type=jnp.float32).astype(jnp.bfloat16)


def expert_half(moe_in, route_ids, route_weights, moe_gain, w_gate, w_up, w_down):
    tokens, model_width = moe_in.shape
    route_count = route_ids.shape[1]
    experts = lax.axis_size("ep")
    lane_count = lax.axis_size("tp")
    capacity = 4 * tokens // experts
    floats = moe_in.astype(jnp.float32)
    normed = (
        floats * lax.rsqrt(jnp.mean(floats * floats, axis=-1, keepdims=True) + norm_eps) * moe_gain
    ).astype(jnp.bfloat16)
    flat_ids = route_ids.reshape(-1)
    onehot = (flat_ids[:, None] == jnp.arange(experts, dtype=jnp.int32)[None, :]).astype(jnp.int32)
    slot_index = jnp.sum(jnp.cumsum(onehot, axis=0) * onehot, axis=1) - 1
    target = flat_ids * capacity + slot_index
    source = jnp.arange(tokens * route_count, dtype=jnp.int32) // route_count
    slot_owner = jnp.full((experts * capacity,), tokens, jnp.int32).at[target].set(source)
    padded = jnp.concatenate([normed, jnp.zeros((1, model_width), jnp.bfloat16)], axis=0)
    outgoing = padded[slot_owner]
    gate_weight = w_gate[0]
    up_weight = w_up[0]
    down_weight = w_down[0]
    copies = jnp.broadcast_to(
        outgoing.reshape(experts, 1, capacity, model_width),
        (experts, lane_count, capacity, model_width),
    )
    arrived = lax.all_to_all(
        copies.reshape(experts * lane_count * capacity, model_width),
        ("ep", "tp"),
        split_axis=0,
        concat_axis=0,
        tiled=True,
    )
    gate_part = jnp.dot(arrived, gate_weight, preferred_element_type=jnp.float32)
    up_part = jnp.dot(arrived, up_weight, preferred_element_type=jnp.float32)
    hidden_grid = (
        (jax.nn.silu(gate_part) * up_part)
        .astype(jnp.bfloat16)
        .reshape(experts, lane_count, capacity, -1)
    )
    partial_value = jnp.einsum(
        "elcf,fd->lecd", hidden_grid, down_weight, preferred_element_type=jnp.float32
    )
    summed_rows = lax.psum_scatter(
        partial_value.reshape(lax.axis_size("tp") * (experts * capacity), model_width).astype(
            jnp.bfloat16
        ),
        "tp",
        scatter_dimension=0,
        tiled=True,
    )
    returned = lax.all_to_all(summed_rows, "ep", split_axis=0, concat_axis=0, tiled=True)
    picked_rows = returned[target].reshape(tokens, route_count, model_width)
    combined = jnp.sum(picked_rows.astype(jnp.float32) * route_weights[:, :, None], axis=1)
    return combined.astype(jnp.bfloat16)


def on_device(
    mix_query,
    mix_key,
    mix_value,
    mix_gate,
    log_decay,
    ret_gain,
    w_out,
    moe_in,
    route_ids,
    route_weights,
    moe_gain,
    w_gate,
    w_up,
    w_down,
):
    mix_out = mixer_half(mix_query, mix_key, mix_value, mix_gate, log_decay, ret_gain, w_out)
    moe_out = expert_half(moe_in, route_ids, route_weights, moe_gain, w_gate, w_up, w_down)
    return (mix_out, moe_out)


def solution(mesh):
    in_specs = (
        P("ep", "tp"),
        P("ep", "tp"),
        P("ep", "tp"),
        P("ep", "tp"),
        P("ep", "tp"),
        P("tp"),
        P(),
        P(("ep", "tp"), None),
        P(("ep", "tp"), None),
        P(("ep", "tp"), None),
        P(),
        P("ep", None, "tp"),
        P("ep", None, "tp"),
        P("ep", "tp", None),
    )
    out_specs = (P(("ep", "tp"), None), P(("ep", "tp"), None))
    return jax.shard_map(
        on_device, mesh=mesh, in_specs=in_specs, out_specs=out_specs, check_vma=False
    )
```

profile of v0, /device:TPU:0, one launch (start us, length us, event | category | flops | bytes accessed | tf_op | source)
XLA Modules:
  0.0 216.1 jit_solution(18138071127455803170)
XLA Ops:
  7.2 0.8 copy.77
  8.0 0.7 broadcast_multiply_fusion
  9.4 0.8 scatter_custom_fusion
  10.2 1.0 fusion.47
  11.2 1.0 fusion.49
  12.3 0.9 gather_fusion
  13.2 2.5 %broadcast_in_dim.95 = bf16[16,8,8,2048]{3,2,1,0:T(8,128)(2,1)} broadcast(bf16[16,8,2048]{2,1,0:T(8,128)(2,1)S(1)} %bitcast.134), dimensions={0,2,3} | broadcast | bytes 4718592 | tf_op jit(solution)/shard_map/broadcast_in_dim | solution.py:149
  15.7 11.7 %all-to-all-start.3 = ((bf16[128,8,2048]{2,1,0:T(8,128)(2,1)}), bf16[128,8,2048]{2,1,0:T(8,128)(2,1)}, u32[]{:S(2)}, u32[]{:S(2)}) async-start(bf16[128,8,2048]{2,1,0:T(8,128)(2,1)} %bitcast.126), calls=%async_computation.3 | async-start | bytes 8388608 | tf_op jit(solution)/shard_map/all_to_all | solution.py:153
  27.5 1.2 reduce-window.6
  29.6 0.6 slice.79
  31.0 3.3 %bitcast_convert_fusion = (f32[2048,1,256]{2,0,1:T(8,128)S(1)}, f32[2048,1,256]{2,0,1:T(8,128)}) fusion(bf16[2048,256]{1,0:T(8,128)(2,1)} %param.17, bf16[2048,256]{1,0:T(8,128)(2,1)} %param.16), kind=kLoop, calls=%fused_computation.57 | loop fusion | flops 1048576 | bytes 6291456 | tf_op jit(solution)/shard_map/reshape | solution.py:75
  34.3 45.7 %all-to-all-done.3 = bf16[128,8,2048]{2,1,0:T(8,128)(2,1)} async-done(((bf16[128,8,2048]{2,1,0:T(8,128)(2,1)}), bf16[128,8,2048]{2,1,0:T(8,128)(2,1)}, u32[]{:S(2)}, u32[]{:S(2)}) %all-to-all-start.3) | async-done | bytes 4194336 | tf_op jit(solution)/shard_map/all_to_all | solution.py:153
  80.0 0.6 broadcast_in_dim.87
  80.6 3.5 %all-to-all-start = ((bf16[16,1,1]{2,1,0:T(2,128)(2,1)}), bf16[16,1,1]{2,1,0:T(2,128)(2,1)S(1)}, u32[]{:S(2)}, u32[]{:S(2)}) async-start(bf16[16,1,1]{2,1,0:T(2,128)(2,1)} %broadcast_in_dim.87), calls=%async_computation | async-start | bytes 16384 | tf_op jit(solution)/shard_map/all_to_all | solution.py:15
  84.1 7.5 %fusion = f32[1024,896]{1,0:T(8,128)S(1)} fusion(bf16[128,8,2048]{2,1,0:T(8,128)(2,1)} %all-to-all-done.3, bf16[1,2048,896]{2,1,0:T(8,128)(2,1)} %param.28), kind=kOutput, calls=%fused_computation.6 | convolution fusion | flops 3758096384 | bytes 11534336 | tf_op jit(solution)/shard_map/dot_general | solution.py:161
  91.6 7.1 %multiply_convert_fusion.1 = bf16[1024,896]{1,0:T(8,128)(2,1)S(1)} fusion(f32[1024,896]{1,0:T(8,128)S(1)} %fusion, bf16[1,2048,896]{2,1,0:T(8,128)(2,1)S(1)} %copy-done.12, bf16[128,8,2048]{2,1,0:T(8,128)(2,1)} %all-to-all-done.3), kind=kOutput, calls=%fused_computation.16 | convolution fusion | flops 3763601408 | bytes 13369344 | tf_op jit(solution)/shard_map/dot_general | solution.py:160
  98.7 4.8 %convert_bitcast_fusion = bf16[8,16,8,2048]{3,2,0,1:T(8,128)(2,1)S(1)} fusion(bf16[16,8,8,896]{3,2,1,0:T(8,128)(2,1)S(1)} %bitcast.154, bf16[1,896,2048]{2,1,0:T(8,128)(2,1)S(1)} %copy-done.13), kind=kOutput, calls=%fused_computation.10 | convolution fusion | flops 3760193536 | bytes 9699328 | tf_op jit(solution)/shard_map/elcf,fd->lecd/dot_general | solution.py:167
  103.5 2.2 %copy.78 = bf16[8,16,8,2048]{3,2,1,0:T(8,128)(2,1)} copy(bf16[8,16,8,2048]{3,2,0,1:T(8,128)(2,1)S(1)} %convert_bitcast_fusion) | data formatting | bytes 8388608 | tf_op jit(solution)/shard_map/convert_element_type | solution.py:171
  105.8 7.8 %fusion.38 = (f32[2048,1,128]{2,0,1:T(8,128)S(1)}, f32[2048,1,128]{2,0,1:T(8,128)S(1)}, bf16[2048,1,128]{2,0,1:T(8,128)(2,1)}, bf16[2048,1,128]{2,0,1:T(8,128)(2,1)}) fusion(f32[2048,1,256]{2,0,1:T(8,128)S(1)} %get-tuple-element.95, f32[128]{0:T(128)S(1)} %multiply_power_fusion, f32[2048]{0:T(1024)S(1)} %add_convert_fusion, f32[2048,1,256]{2,0,1:T(8,128)} %get-tuple-element.96), kind=kLoop, calls=%fused_computation.53 | loop fusion | flops 3932160 | bytes 7348736 | tf_op jit(solution)/shard_map/sub | solution.py:54
  113.6 1.3 convolution_bitcast_fusion
  115.0 8.1 %while.13 = (s32[]{:T(128)}, f32[1,256,256]{2,1,0:T(8,128)S(1)}, f32[4,1,256,256]{3,2,1,0:T(8,128)}, f32[4,1]{0,1:T(1,128)S(1)}, f32[4,1,256,256]{3,2,1,0:T(8,128)S(1)}, /*index=5*/s32[]{:T(128)}, s32[]{:T(128)}) while((s32[]{:T(128)}, f32[1,256,256]{2,1,0:T(8,128)S(1)}, f32[4,1,256,256]{3,2,1,0:T(8,128)}, f32[4,1]{0,1:T(1,128)S(1)}, ...), condition=%wide.region_3.4_spmd.clone, body=%wide.region_2.3_spmd.clone.sunk | while | flops 262147 | bytes 1311340 | solution.py:101
  115.0 0.7 bitcast_dynamic-update-slice_fusion.2
  115.7 0.6 fusion.76
  116.3 0.7 bitcast_add_fusion.6
  117.0 0.7 bitcast_dynamic-update-slice_fusion.2
  118.4 0.7 bitcast_add_fusion.6
  119.1 0.7 bitcast_dynamic-update-slice_fusion.2
  120.4 0.7 bitcast_add_fusion.6
  121.1 0.7 bitcast_dynamic-update-slice_fusion.2
  121.8 0.6 fusion.76
  122.4 0.7 bitcast_add_fusion.6
  123.2 1.5 broadcast_in_dim.90
  124.7 7.2 %all-to-all-start.1 = ((bf16[16,1,256,256]{3,2,1,0:T(8,128)(2,1)}), bf16[16,1,256,256]{3,2,1,0:T(8,128)(2,1)S(1)}, u32[]{:S(2)}, u32[]{:S(2)}) async-start(bf16[16,1,256,256]{3,2,1,0:T(8,128)(2,1)} %broadcast_in_dim.90), calls=%async_computation.1 | async-start | bytes 4194304 | tf_op jit(solution)/shard_map/all_to_all | solution.py:15
  132.0 5.1 %fusion.33 = f32[4,512,256]{2,1,0:T(8,128)} fusion(bf16[4,512,256]{2,1,0:T(8,128)(2,1)S(1)} %bitcast.123, f32[4,512]{1,0:T(4,128)S(1)} %get-tuple-element.86, pred[512,512]{1,0:T(8,128)(4,1)S(1)} %iota_compare_fusion, bf16[4,512,128]{2,1,0:T(8,128)(2,1)} %bitcast.135, bf16[4,512,128]{2,1,0:T(8,128)(2,1)} %bitcast.137, f32[4,512,128]{2,1,0:T(8,128)} %bitcast.133, ...), kind=kOutput, calls=%fused_computation.47 | convolution fusion | flops 1082654720 | bytes 6561792 | tf_op jit(solution)/shard_map/nhij,njhe->nihe/dot_general | solution.py:90
  138.0 0.6 slice.86
  138.5 23.7 %all-to-all-done.1 = bf16[16,1,256,256]{3,2,1,0:T(8,128)(2,1)S(1)} async-done(((bf16[16,1,256,256]{3,2,1,0:T(8,128)(2,1)}), bf16[16,1,256,256]{3,2,1,0:T(8,128)(2,1)S(1)}, u32[]{:S(2)}, u32[]{:S(2)}) %all-to-all-start.1) | async-done | bytes 2097184 | tf_op jit(solution)/shard_map/all_to_all | solution.py:15
  163.5 0.9 fusion.50
  165.3 2.6 %fusion.18 = (f32[4,512]{1,0:T(4,128)S(1)}, f32[4,256,512]{1,2,0:T(8,128)S(1)}) fusion(f32[4,512]{1,0:T(4,128)S(1)} %exp.53, bf16[4,512,128]{2,1,0:T(8,128)(2,1)S(1)} %bitcast.136, bf16[4,512,128]{2,1,0:T(8,128)(2,1)S(1)} %bitcast.138, f32[4,1,256,256]{3,2,1,0:T(8,128)S(1)} %copy-done.8, f32[256,256]{1,0:T(8,128)S(1)} %fusion.50, f32[4]{0:T(128)S(1)} %fusion.56, ...), kind=kOutput, calls=%fused_computation.29 | convolution fusion | flops 1615329280 | bytes 6570000 | tf_op jit(solution)/shard_map/nihd,nhde->nihe/dot_general | solution.py:109
  168.0 1.7 fusion.22
  169.7 3.7 %all-to-all-start.2 = ((bf16[8,256,256]{2,1,0:T(8,128)(2,1)}), bf16[8,256,256]{2,1,0:T(8,128)(2,1)S(1)}, u32[]{:S(2)}, u32[]{:S(2)}) async-start(bf16[8,256,256]{2,1,0:T(8,128)(2,1)} %bitcast.33), calls=%async_computation.2 | async-start | bytes 2097152 | tf_op jit(solution)/shard_map/all_to_all | solution.py:118
  173.5 15.8 %all-to-all-done.2 = bf16[8,256,256]{2,1,0:T(8,128)(2,1)S(1)} async-done(((bf16[8,256,256]{2,1,0:T(8,128)(2,1)}), bf16[8,256,256]{2,1,0:T(8,128)(2,1)S(1)}, u32[]{:S(2)}, u32[]{:S(2)}) %all-to-all-start.2) | async-done | bytes 1048608 | tf_op jit(solution)/shard_map/all_to_all | solution.py:118
  189.2 1.0 copy-done.1
  190.2 1.5 copy.75
  191.7 3.6 %all-to-all-start.4 = ((bf16[16,8,2048]{2,1,0:T(8,128)(2,1)}), bf16[16,8,2048]{2,1,0:T(8,128)(2,1)S(1)}, u32[]{:S(2)}, u32[]{:S(2)}) async-start(bf16[16,8,2048]{2,1,0:T(8,128)(2,1)} %bitcast.141), calls=%async_computation.5 | async-start | bytes 1048576 | tf_op jit(solution)/shard_map/all_to_all | solution.py:178
  195.3 6.7 %convolution_convert_fusion = bf16[256,2048]{1,0:T(8,128)(2,1)} fusion(bf16[256,2048]{0,1:T(8,128)(2,1)S(1)} %bitcast.128, bf16[2048,2048]{1,0:T(8,128)(2,1)} %param.22), kind=kOutput, calls=%fused_computation.19 | convolution fusion | flops 2148007936 | bytes 10485760 | tf_op jit(solution)/shard_map/dot_general | solution.py:125
  202.0 4.8 %all-to-all-done.4 = bf16[16,8,2048]{2,1,0:T(8,128)(2,1)S(1)} async-done(((bf16[16,8,2048]{2,1,0:T(8,128)(2,1)}), bf16[16,8,2048]{2,1,0:T(8,128)(2,1)S(1)}, u32[]{:S(2)}, u32[]{:S(2)}) %all-to-all-start.4) | async-done | bytes 524320 | tf_op jit(solution)/shard_map/all_to_all | solution.py:178
  206.8 0.7 gather_fusion.1
  207.9 1.4 multiply_reduce_fusion
  (84 shorter events, 6.6 us)
Async XLA Ops:
  7.2 106.4 %copy-start = (bf16[2048,256]{1,0:T(8,128)(2,1)S(1)}, bf16[2048,256]{1,0:T(8,128)(2,1)}, u32[]{:S(2)}) copy-start(bf16[2048,256]{1,0:T(8,128)(2,1)} %param.18) | copy-start | bytes 3145732
  15.7 11.7 %copy-start.9 = (f32[2048,1]{0,1:T(1,128)S(1)}, f32[2048,1]{0,1:T(1,128)}, u32[]{:S(2)}) copy-start(f32[2048,1]{0,1:T(1,128)} %param.20) | copy-start | bytes 24580
  15.7 64.2 %all-to-all-start.3 = ((bf16[128,8,2048]{2,1,0:T(8,128)(2,1)}), bf16[128,8,2048]{2,1,0:T(8,128)(2,1)}, u32[]{:S(2)}, u32[]{:S(2)}) async-start(bf16[128,8,2048]{2,1,0:T(8,128)(2,1)} %bitcast.126), calls=%async_computation.3 | async-start | bytes 8388608 | tf_op jit(solution)/shard_map/all_to_all | solution.py:153
  80.6 42.6 %all-to-all-start = ((bf16[16,1,1]{2,1,0:T(2,128)(2,1)}), bf16[16,1,1]{2,1,0:T(2,128)(2,1)S(1)}, u32[]{:S(2)}, u32[]{:S(2)}) async-start(bf16[16,1,1]{2,1,0:T(2,128)(2,1)} %broadcast_in_dim.87), calls=%async_computation | async-start | bytes 16384 | tf_op jit(solution)/shard_map/all_to_all | solution.py:15
  84.0 107.7 %reduce-scatter.2.cloned.1.call-start = ((), (), s32[]{:S(2)}) async-start(), calls=%async_computation.6 | async-start | bytes 4718592 | tf_op jit(solution)/shard_map/reduce_scatter | solution.py:170
  84.1 7.5 %copy-start.12 = (bf16[1,2048,896]{2,1,0:T(8,128)(2,1)S(1)}, bf16[1,2048,896]{2,1,0:T(8,128)(2,1)}, u32[]{:S(2)}) copy-start(bf16[1,2048,896]{2,1,0:T(8,128)(2,1)} %param.27) | copy-start | bytes 11010052
  91.6 7.1 %copy-start.13 = (bf16[1,896,2048]{2,1,0:T(8,128)(2,1)S(1)}, bf16[1,896,2048]{2,1,0:T(8,128)(2,1)}, u32[]{:S(2)}) copy-start(bf16[1,896,2048]{2,1,0:T(8,128)(2,1)} %param.29) | copy-start | bytes 11010052
  113.6 1.3 copy-start.2
  113.6 1.4 copy-start.3
  124.7 37.6 %all-to-all-start.1 = ((bf16[16,1,256,256]{3,2,1,0:T(8,128)(2,1)}), bf16[16,1,256,256]{3,2,1,0:T(8,128)(2,1)S(1)}, u32[]{:S(2)}, u32[]{:S(2)}) async-start(bf16[16,1,256,256]{3,2,1,0:T(8,128)(2,1)} %broadcast_in_dim.90), calls=%async_computation.1 | async-start | bytes 4194304 | tf_op jit(solution)/shard_map/all_to_all | solution.py:15
  163.1 1.6 copy-start.4
  163.1 1.7 copy-start.5
  163.1 1.8 copy-start.6
  163.1 2.2 copy-start.8
  165.3 2.7 %copy-start.7 = (bf16[2048,256]{1,0:T(8,128)(2,1)S(1)}, bf16[2048,256]{1,0:T(8,128)(2,1)}, u32[]{:S(2)}) copy-start(bf16[2048,256]{1,0:T(8,128)(2,1)} %param.19) | copy-start | bytes 3145732
  165.3 2.7 %copy-start.10 = (f32[256]{0:T(256)S(1)}, f32[256]{0:T(256)}, u32[]{:S(2)}) copy-start(f32[256]{0:T(256)} %param.21) | copy-start | bytes 3076
  169.7 3.7 %copy-start.11 = (f32[32,2]{0,1:T(2,128)S(1)}, f32[32,2]{0,1:T(2,128)}, u32[]{:S(2)}) copy-start(f32[32,2]{0,1:T(2,128)} %param.25) | copy-start | bytes 772
  169.7 19.6 %all-to-all-start.2 = ((bf16[8,256,256]{2,1,0:T(8,128)(2,1)}), bf16[8,256,256]{2,1,0:T(8,128)(2,1)S(1)}, u32[]{:S(2)}, u32[]{:S(2)}) async-start(bf16[8,256,256]{2,1,0:T(8,128)(2,1)} %bitcast.33), calls=%async_computation.2 | async-start | bytes 2097152 | tf_op jit(solution)/shard_map/all_to_all | solution.py:118
  189.2 1.0 copy-start.1
  191.7 15.1 %all-to-all-start.4 = ((bf16[16,8,2048]{2,1,0:T(8,128)(2,1)}), bf16[16,8,2048]{2,1,0:T(8,128)(2,1)S(1)}, u32[]{:S(2)}, u32[]{:S(2)}) async-start(bf16[16,8,2048]{2,1,0:T(8,128)(2,1)} %bitcast.141), calls=%async_computation.5 | async-start | bytes 1048576 | tf_op jit(solution)/shard_map/all_to_all | solution.py:178
Sparse Core Ops, SparseCore 0:
  105.9 37.2 reduce-scatter.1
where the time goes:
time: 217 us; the launch traced here: 216 us
  waiting for transfers between devices  89.9 us (41%)
  matrix products  35.1 us (16%)
  starting transfers between devices  29.6 us (14%)
  other arithmetic  27 us (12%)
  local copies, waits for them, and re-layouts  19.1 us (9%)
  between operations  15.2 us (7%)
    all_to_all x1, waiting for transfers between devices, expert_half(): lax.all_to_all(copies.reshape(experts * lane_count * capacity, model_widt...  45.7 us
    all_to_all x2, waiting for transfers between devices, from_everyone(): return lax.all_to_all(copies, axis, split_axis=0, concat_axis=0, tiled=True)  23.7 us
    all_to_all x1, waiting for transfers between devices, mixer_half(): lax.all_to_all(heads_out.reshape(seq_rows, local_heads * HEAD_DIM), 'tp',...  15.8 us
    all_to_all x1, starting transfers between devices, expert_half(): lax.all_to_all(copies.reshape(experts * lane_count * capacity, model_widt...  11.7 us
    all_to_all x2, starting transfers between devices, from_everyone(): return lax.all_to_all(copies, axis, split_axis=0, concat_axis=0, tiled=True)  10.6 us
    sub x1, other arithmetic, rotate(): front * cosine - back * sine  7.82 us
    dot_general x1, matrix products, expert_half(): up_part = jnp.dot(arrived, up_weight, preferred_element_type=jnp.float32)  7.5 us
    dot_general x1, matrix products, expert_half(): jnp.dot(arrived, gate_weight, preferred_element_type=jnp.float32)  7.09 us
  transfers between devices with their start and end apart: 6, of which 4 were waited for; matrix products, arithmetic and copies ran while one was open for 31% of the time, Pallas kernels for 0%

commit v1 on v0

v1 whole, which is shorter than its diff:
```python
import functools

import jax
import jax.numpy as jnp
import numpy as np
from jax import lax
from jax.experimental import pallas as pl
from jax.experimental.pallas import tpu as pltpu
from jax.sharding import Mesh
from jax.sharding import PartitionSpec as P

HEAD_DIM = 256
HALF = HEAD_DIM // 2
BLOCK = 512
EXPERTS = 16
CAP = 8
SLOTS = EXPERTS * CAP
norm_eps = 1e-06

f32 = jnp.float32
bf16 = jnp.bfloat16

NT = (((1,), (1,)), ((), ()))
TN = (((0,), (0,)), ((), ()))


def mm(a, b):
    return jnp.dot(a, b, preferred_element_type=f32)


def shift(x, axis, by, size=4, wrap=True):
    pairs = [(j, (j + by) % size) for j in range(size) if wrap or 0 <= j + by < size]
    return lax.ppermute(x, axis, pairs)


def route_tables(ids):
    tokens = ids.shape[0]
    lane = lax.broadcasted_iota(jnp.int32, (tokens, EXPERTS), 1)
    first = (ids[:, 0:1] == lane).astype(f32)
    second = (ids[:, 1:2] == lane).astype(f32)
    both = first + second
    below = (
        lax.broadcasted_iota(jnp.int32, (tokens, tokens), 1)
        < lax.broadcasted_iota(jnp.int32, (tokens, tokens), 0)
    ).astype(f32)
    rank = mm(below, both)
    return first, second, both, rank


def pre_kernel(x_ref, ids_ref, gain_ref, out_ref):
    _, _, both, rank = route_tables(ids_ref[...])
    tokens = x_ref.shape[0]
    row = lax.broadcasted_iota(jnp.int32, (SLOTS, EXPERTS), 0)
    col = lax.broadcasted_iota(jnp.int32, (SLOTS, EXPERTS), 1)
    spread = (row // CAP == col).astype(f32)
    named = lax.dot_general(spread, both, NT, preferred_element_type=f32)
    ranks = lax.dot_general(spread, rank, NT, preferred_element_type=f32)
    slot = (lax.broadcasted_iota(jnp.int32, (SLOTS, tokens), 0) % CAP).astype(f32)
    pick = jnp.where((named > 0.5) & (jnp.abs(ranks - slot) < 0.5), 1.0, 0.0).astype(bf16)
    x = x_ref[...].astype(f32)
    scale = lax.rsqrt(jnp.mean(x * x, axis=-1, keepdims=True) + norm_eps)
    normed = (x * scale * gain_ref[...]).astype(bf16)
    out_ref[...] = mm(pick, normed).astype(bf16)


def combine_kernel(rows_ref, ids_ref, weights_ref, out_ref):
    first, second, _, rank = route_tables(ids_ref[...])
    tokens = ids_ref.shape[0]
    row = lax.broadcasted_iota(jnp.int32, (EXPERTS, SLOTS), 0)
    col = lax.broadcasted_iota(jnp.int32, (EXPERTS, SLOTS), 1)
    spread = (col // CAP == row).astype(f32)
    slot = (lax.broadcasted_iota(jnp.int32, (tokens, SLOTS), 1) % CAP).astype(f32)
    here = jnp.abs(mm(rank, spread) - slot) < 0.5
    rows = rows_ref[...]
    total = None
    for k, named in enumerate((first, second)):
        pick = jnp.where((mm(named, spread) > 0.5) & here, 1.0, 0.0).astype(bf16)
        part = mm(pick, rows) * weights_ref[:, k : k + 1]
        total = part if total is None else total + part
    out_ref[...] = total.astype(bf16)


def ffn_kernel(n_x, tile, *refs):
    xs = refs[:n_x]
    wg, wu, wd = refs[n_x : n_x + 3]
    outs = refs[n_x + 3 : -9]
    xbuf, gbuf, ubuf, dbuf, hbuf, obuf, xsem, wsem, osem = refs[-9:]
    ff = gbuf.shape[1]
    chunks = ff // 128
    per_out = n_x // len(outs)
    copies_w = []
    for j in range(chunks):
        cols = pl.ds(j * 128, 128)
        a = pltpu.make_async_copy(wg.at[:, cols], gbuf.at[:, cols], wsem.at[2 * j])
        b = pltpu.make_async_copy(wu.at[:, cols], ubuf.at[:, cols], wsem.at[2 * j + 1])
        copies_w.append((a, b))
    for c in copies_w[0]:
        c.start()
    copies_x = []
    for i in range(n_x):
        c = pltpu.make_async_copy(xs[i], xbuf.at[pl.ds(i * tile, tile)], xsem.at[i])
        c.start()
        copies_x.append(c)
    for pair in copies_w[1:]:
        for c in pair:
            c.start()
    down = pltpu.make_async_copy(wd, dbuf, wsem.at[2 * chunks])
    down.start()
    for j in range(chunks):
        for c in copies_w[j]:
            c.wait()
        w = jnp.concatenate(
            [gbuf[:, j * 128 : (j + 1) * 128], ubuf[:, j * 128 : (j + 1) * 128]], axis=1
        )
        step = 256
        for r in range(0, n_x * tile, step):
            if j == 0:
                for i in range(r // tile, (r + step) // tile):
                    copies_x[i].wait()
            both = mm(xbuf[r : r + step, :], w)
            gate, up = both[:, :128], both[:, 128:]
            hidden = gate * up / (1.0 + jnp.exp(-gate))
            hbuf[r : r + step, j * 128 : (j + 1) * 128] = hidden.astype(bf16)
    down.wait()
    outs_c = []
    for o in range(len(outs)):
        for i in range(per_out):
            r = (o * per_out + i) * tile
            if r % 256 == 0:
                obuf[r : r + 256, :] = mm(hbuf[r : r + 256, :], dbuf[...]).astype(bf16)
                last = pltpu.make_async_copy(
                    obuf.at[pl.ds(r, 256)], outs[o].at[pl.ds(i * tile, 256)], osem.at[r // 256]
                )
                last.start()
                outs_c.append(last)
    for c in outs_c:
        c.wait()


def ffn(xs, w_gate, w_up, w_down, n_out):
    n_x = len(xs)
    tile, width = xs[0].shape
    ff = w_gate.shape[1]
    rows = n_x * tile
    hbm = pl.BlockSpec(memory_space=pl.ANY)
    return pl.pallas_call(
        functools.partial(ffn_kernel, n_x, tile),
        out_shape=[jax.ShapeDtypeStruct((rows // n_out, width), bf16)] * n_out,
        in_specs=[hbm] * (n_x + 3),
        out_specs=[hbm] * n_out,
        scratch_shapes=[
            pltpu.VMEM((rows, width), bf16),
            pltpu.VMEM((width, ff), bf16),
            pltpu.VMEM((width, ff), bf16),
            pltpu.VMEM((ff, width), bf16),
            pltpu.VMEM((rows, ff), bf16),
            pltpu.VMEM((rows, width), bf16),
            pltpu.SemaphoreType.DMA((n_x,)),
            pltpu.SemaphoreType.DMA((2 * (ff // 128) + 1,)),
            pltpu.SemaphoreType.DMA((rows // 256,)),
        ],
        cost_estimate=pl.CostEstimate(
            flops=6 * rows * width * ff,
            bytes_accessed=2 * (3 * width * ff + 2 * rows * width),
            transcendentals=rows * ff,
        ),
        name="ffn",
    )(*xs, w_gate, w_up, w_down)


def local_kernel(
    base_ref, q_ref, k_ref, v_ref, ld_ref, cos_ref, sin_ref, kept_ref, qd_ref, send_ref, state, before
):
    b = pl.program_id(0)

    @pl.when(b == 0)
    def _():
        state[...] = jnp.zeros_like(state)
        before[...] = jnp.zeros_like(before)

    cos_base = base_ref[0, 0:1, :]
    sin_base = base_ref[0, 1:2, :]
    cos_t, sin_t = cos_ref[...], sin_ref[...]
    cosine = cos_t * cos_base - sin_t * sin_base
    sine = sin_t * cos_base + cos_t * sin_base

    def rotated(ref):
        front = ref[:, :HALF].astype(f32)
        back = ref[:, HALF:].astype(f32)
        return jnp.concatenate([front * cosine - back * sine, back * cosine + front * sine], axis=1)

    q = rotated(q_ref).astype(bf16)
    k = (rotated(k_ref) * HEAD_DIM ** (-0.5)).astype(bf16)
    v = v_ref[...]
    row = lax.broadcasted_iota(jnp.int32, (BLOCK, BLOCK), 0)
    col = lax.broadcasted_iota(jnp.int32, (BLOCK, BLOCK), 1)
    ld = ld_ref[0]
    cum = jnp.sum(jnp.where(row >= col, ld, 0.0), axis=1, keepdims=True)
    cum_row = jnp.sum(jnp.where(row == col, cum, 0.0), axis=0, keepdims=True)
    last = cum[BLOCK - 1 : BLOCK, :]

    q32 = q.astype(f32)
    begin = state[...].astype(bf16)
    carried = mm((q32 * jnp.exp(cum)).astype(bf16), begin)
    half = BLOCK // 2
    for r in range(2):
        lo, hi = r * half, (r + 1) * half
        scores = lax.dot_general(q[lo:hi], k[:hi], NT, preferred_element_type=f32)
        gap = cum[lo:hi] - cum_row[:, :hi]
        seen = (
            lax.broadcasted_iota(jnp.int32, (half, hi), 0) + lo
            >= lax.broadcasted_iota(jnp.int32, (half, hi), 1)
        )
        weights = jnp.where(seen, scores * jnp.exp(jnp.where(seen, gap, 0.0)), 0.0).astype(bf16)
        kept_ref[lo:hi, :] = mm(weights, v[:hi]) + carried[lo:hi]
    qd_ref[...] = (q32 * jnp.exp(cum + before[0:1, 0:1])).astype(bf16)
    kd = (k.astype(f32) * jnp.exp(last - cum)).astype(bf16)
    update = lax.dot_general(kd, v, TN, preferred_element_type=f32)
    state[...] = jnp.exp(last) * state[...] + update
    before[...] = before[...] + last

    @pl.when(b == pl.num_programs(0) - 1)
    def _():
        send_ref[0:HEAD_DIM, :] = state[...].astype(bf16)
        put_decay(send_ref, jnp.exp(before[...]))


def put_decay(ref, decay):
    high = decay.astype(bf16)
    low = (decay - high.astype(f32)).astype(bf16)
    ref[HEAD_DIM : HEAD_DIM + 8, :HALF] = jnp.broadcast_to(high, (8, HALF))
    ref[HEAD_DIM : HEAD_DIM + 8, HALF:] = jnp.broadcast_to(low, (8, HALF))


def get_decay(ref):
    tail = ref[HEAD_DIM : HEAD_DIM + 8, :].astype(f32)
    return tail[0:1, 0:1] + tail[0:1, HALF : HALF + 1]


def local_part(base, q, k, v, ld, cos_t, sin_t):
    rows = q.shape[0]
    blocks = rows // BLOCK
    seq = pl.BlockSpec((BLOCK, HEAD_DIM), lambda b: (b, 0))
    table = pl.BlockSpec((BLOCK, HALF), lambda b: (0, 0))
    return pl.pallas_call(
        local_kernel,
        grid=(blocks,),
        out_shape=[
            jax.ShapeDtypeStruct((rows, HEAD_DIM), f32),
            jax.ShapeDtypeStruct((rows, HEAD_DIM), bf16),
            jax.ShapeDtypeStruct((HEAD_DIM + 8, HEAD_DIM), bf16),
        ],
        in_specs=[
            pl.BlockSpec((1, 2, HALF), lambda b: (b, 0, 0)),
            seq,
            seq,
            seq,
            pl.BlockSpec((1, 1, BLOCK), lambda b: (b, 0, 0)),
            table,
            table,
        ],
        out_specs=[seq, seq, pl.BlockSpec((HEAD_DIM + 8, HEAD_DIM), lambda b: (0, 0))],
        scratch_shapes=[pltpu.VMEM((HEAD_DIM, HEAD_DIM), f32), pltpu.VMEM((8, HALF), f32)],
        compiler_params=pltpu.CompilerParams(dimension_semantics=("arbitrary",)),
        cost_estimate=pl.CostEstimate(
            flops=6 * 10**9, bytes_accessed=6 * 2**20, transcendentals=2**20
        ),
        name="local",
    )(base, q, k, v, ld, cos_t, sin_t)


def middle_kernel(x_ref, own_ref, one_ref, two_ref, three_ref, before_ref, send_ref):
    x = x_ref[0]
    refs = (own_ref, one_ref, two_ref, three_ref)
    place = [lax.rem(x - s + 4, 4) for s in range(4)]
    decay = [get_decay(r) for r in refs]
    into = jnp.zeros((HEAD_DIM, HEAD_DIM), f32)
    whole = jnp.zeros((HEAD_DIM, HEAD_DIM), f32)
    through = jnp.ones((1, 1), f32)
    for s in range(4):
        after_all = jnp.ones((1, 1), f32)
        for o in range(4):
            if o != s:
                after_all = after_all * jnp.where(place[o] > place[s], decay[o], 1.0)
        part = refs[s][0:HEAD_DIM, :].astype(f32)
        whole = whole + part * after_all
        if s:
            into = into + jnp.where(s <= x, through, 0.0) * part
            through = through * jnp.where(s <= x, decay[s], 1.0)
    before_ref[0:HEAD_DIM, :] = into
    before_ref[HEAD_DIM : HEAD_DIM + 8, :] = jnp.broadcast_to(through, (8, HEAD_DIM))
    send_ref[0:HEAD_DIM, :] = whole.astype(bf16)
    total = decay[0] * decay[1] * decay[2] * decay[3]
    put_decay(send_ref, jnp.broadcast_to(total, (8, HALF)))


def middle(x, own, one, two, three):
    return pl.pallas_call(
        middle_kernel,
        out_shape=[
            jax.ShapeDtypeStruct((HEAD_DIM + 8, HEAD_DIM), f32),
            jax.ShapeDtypeStruct((HEAD_DIM + 8, HEAD_DIM), bf16),
        ],
        in_specs=[pl.BlockSpec(memory_space=pltpu.SMEM)]
        + [pl.BlockSpec(memory_space=pltpu.VMEM)] * 4,
        out_specs=[pl.BlockSpec(memory_space=pltpu.VMEM)] * 2,
        cost_estimate=pl.CostEstimate(
            flops=5 * 10**8, bytes_accessed=10**6, transcendentals=0
        ),
        name="middle",
    )(x, own, one, two, three)


def finish_kernel(
    before_ref, one_ref, two_ref, three_ref, kept_ref, qd_ref, gate_ref, gain_ref, out_ref, start
):
    @pl.when(pl.program_id(0) == 0)
    def _():
        into = three_ref[0:HEAD_DIM, :].astype(f32)
        for ref in (two_ref, one_ref):
            into = ref[0:HEAD_DIM, :].astype(f32) + get_decay(ref) * into
        through = before_ref[HEAD_DIM : HEAD_DIM + 1, 0:1]
        start[...] = (before_ref[0:HEAD_DIM, :] + through * into).astype(bf16)

    retained = kept_ref[...] + mm(qd_ref[...], start[...])
    scale = lax.rsqrt(jnp.mean(retained * retained, axis=-1, keepdims=True) + norm_eps)
    gate = gate_ref[...].astype(f32)
    gate = gate / (1.0 + jnp.exp(-gate))
    out_ref[...] = (gate * retained * scale * gain_ref[...]).astype(bf16)


def finish(before, one, two, three, kept, qd, gate, gain):
    rows = qd.shape[0]
    seq = pl.BlockSpec((BLOCK, HEAD_DIM), lambda b: (b, 0))
    whole = pl.BlockSpec((HEAD_DIM + 8, HEAD_DIM), lambda b: (0, 0))
    return pl.pallas_call(
        finish_kernel,
        grid=(rows // BLOCK,),
        out_shape=jax.ShapeDtypeStruct((rows, HEAD_DIM), bf16),
        in_specs=[whole] * 4 + [seq] * 3 + [pl.BlockSpec((1, HEAD_DIM), lambda b: (0, 0))],
        out_specs=seq,
        scratch_shapes=[pltpu.VMEM((HEAD_DIM, HEAD_DIM), bf16)],
        compiler_params=pltpu.CompilerParams(dimension_semantics=("arbitrary",)),
        cost_estimate=pl.CostEstimate(
            flops=2 * 10**9, bytes_accessed=5 * 2**20, transcendentals=2**19
        ),
        name="finish",
    )(before, one, two, three, kept, qd, gate, gain)


def project_kernel(rows_ref, w_ref, out_ref, acc):
    s = pl.program_id(0)
    part = mm(rows_ref[...], w_ref[...])

    @pl.when(s == 0)
    def _():
        acc[...] = part

    @pl.when(s > 0)
    def _():
        acc[...] = acc[...] + part

    @pl.when(s == pl.num_programs(0) - 1)
    def _():
        out_ref[...] = acc[...].astype(bf16)


def project(pieces, w_out):
    parts = 8
    rows = pieces.shape[0] // parts
    width = w_out.shape[1]
    return pl.pallas_call(
        project_kernel,
        grid=(parts,),
        out_shape=jax.ShapeDtypeStruct((rows, width), bf16),
        in_specs=[
            pl.BlockSpec((rows, HEAD_DIM), lambda s: (s, 0)),
            pl.BlockSpec((HEAD_DIM, width), lambda s: (s, 0)),
        ],
        out_specs=pl.BlockSpec((rows, width), lambda s: (0, 0)),
        scratch_shapes=[pltpu.VMEM((rows, width), f32)],
        compiler_params=pltpu.CompilerParams(dimension_semantics=("arbitrary",)),
        cost_estimate=pl.CostEstimate(
            flops=4 * 10**9, bytes_accessed=10 * 2**20, transcendentals=0
        ),
        name="project",
    )(pieces, w_out)


def angle_tables():
    inverse = 10000.0 ** (-np.arange(HALF) * 2.0 / HEAD_DIM)
    angle = np.arange(BLOCK)[:, None] * inverse[None, :]
    return np.cos(angle).astype(np.float32), np.sin(angle).astype(np.float32)


def on_device(
    mix_query,
    mix_key,
    mix_value,
    mix_gate,
    log_decay,
    ret_gain,
    w_out,
    moe_in,
    route_ids,
    route_weights,
    moe_gain,
    w_gate,
    w_up,
    w_down,
):
    seq_rows = mix_query.shape[0]
    blocks = seq_rows // BLOCK
    width = moe_in.shape[1]
    ep = ("z", "x")
    tp = ("y", "core")

    outgoing = pl.pallas_call(
        pre_kernel,
        out_shape=jax.ShapeDtypeStruct((SLOTS, width), bf16),
        cost_estimate=pl.CostEstimate(flops=2 * 10**9, bytes_accessed=10**6, transcendentals=0),
        name="pre",
    )(moe_in, route_ids, moe_gain.reshape(1, -1))
    own = lax.all_to_all(outgoing, ep, split_axis=0, concat_axis=0, tiled=True)

    cos_t, sin_t = angle_tables()
    inverse = 10000.0 ** (-np.arange(HALF) * 2.0 / HEAD_DIM)
    first = lax.axis_index(ep) * seq_rows + BLOCK * jnp.arange(blocks, dtype=jnp.int32)
    angle = first.astype(f32)[:, None] * jnp.asarray(inverse, f32)[None, :]
    base = jnp.stack([jnp.cos(angle), jnp.sin(angle)], axis=1)
    kept, qd, end = local_part(
        base,
        mix_query,
        mix_key,
        mix_value,
        log_decay.reshape(blocks, 1, BLOCK),
        jnp.asarray(cos_t),
        jnp.asarray(sin_t),
    )
    by_x = [shift(end, "x", s) for s in (1, 2, 3)]
    x_index = lax.axis_index("x").astype(jnp.int32).reshape(1)
    before, whole = middle(x_index, end, *by_x)
    by_z = [shift(whole, "z", s, wrap=False) for s in (1, 2, 3)]
    heads_out = finish(before, *by_z, kept, qd, mix_gate, ret_gain.reshape(1, -1))
    pieces = lax.all_to_all(heads_out, tp, split_axis=0, concat_axis=0, tiled=True)

    half = own.shape[0] // 2
    up1 = shift(own, "y", 1)
    down1 = shift(own, "y", -1)
    far = jnp.concatenate([shift(up1[:half], "y", 1), shift(down1[half:], "y", -1)], axis=0)
    mine = [own, up1, down1, far]
    other = [shift(v, "core", 1, 2) for v in mine]
    keep, give = ffn(mine + other, w_gate[0], w_up[0], w_down[0], 2)
    got = shift(give, "core", 1, 2)
    sums = (keep.astype(f32) + got.astype(f32)).astype(bf16)
    n = own.shape[0]
    back = [
        sums[:n],
        shift(sums[n : 2 * n], "y", -1),
        shift(sums[2 * n : 3 * n], "y", 1),
        shift(sums[3 * n :], "y", 2),
    ]
    expert_rows = sum(v.astype(f32) for v in back).astype(bf16)
    returned = lax.all_to_all(expert_rows, ep, split_axis=0, concat_axis=0, tiled=True)
    mix_out = project(pieces, w_out)
    moe_out = pl.pallas_call(
        combine_kernel,
        out_shape=jax.ShapeDtypeStruct(moe_in.shape, bf16),
        cost_estimate=pl.CostEstimate(flops=10**9, bytes_accessed=10**6, transcendentals=0),
        name="combine",
    )(returned, route_ids, route_weights)
    return (mix_out, moe_out)


def solution(mesh):
    ep, tp = ("z", "x"), ("y", "core")
    every = ep + tp
    fine = Mesh(mesh.devices.reshape(4, 4, 4, 2), every)
    in_specs = (
        P(ep, tp),
        P(ep, tp),
        P(ep, tp),
        P(ep, tp),
        P(ep, tp),
        P(tp),
        P(),
        P(every, None),
        P(every, None),
        P(every, None),
        P(),
        P(ep, None, tp),
        P(ep, None, tp),
        P(ep, tp, None),
    )
    out_specs = (P(every, None), P(every, None))
    return jax.shard_map(
        on_device, mesh=fine, in_specs=in_specs, out_specs=out_specs, check_vma=False
    )
```

time: 217 us -> 160 us (0.74)
  Pallas kernels: 0 us -> 46.8 us
  waiting for transfers between devices: 89.9 us -> 45.6 us
  matrix products: 35.1 us -> 0 us
  other arithmetic: 27 us -> 6.18 us
  blocking collectives: 0 us -> 19.5 us
  between operations: 15.2 us -> 0.88 us
  local copies, waits for them, and re-layouts: 19.1 us -> 7.79 us
  starting transfers between devices: 29.6 us -> 32.4 us
    all_to_all x5 -> x2, waiting for transfers between devices: 89.9 us -> 5.84 us  [the longest x1 5.84 us: on_device(): lax.all_to_all(heads_out, tp, split_axis=0, concat_axis=0, tiled=True)]
    pallas_call x0 -> x7, Pallas kernels: none -> 46.8 us  [the longest x1 18.8 us: ffn(): pl.pallas_call(functools.partial(ffn_kernel, n_x, tile), out_shape=[jax.S...]
    ppermute x0 -> x18, waiting for transfers between devices: none -> 39.8 us  [shift(): return lax.ppermute(x, axis, pairs)]
    dot_general x7 -> x0, matrix products: 35.1 us -> none  [the longest x1 7.5 us: expert_half(): up_part = jnp.dot(arrived, up_weight, preferred_element_type=jnp.float32)]
    ppermute x0 -> x18, starting transfers between devices: none -> 23.7 us  [shift(): return lax.ppermute(x, axis, pairs)]
    all_to_all x5 -> x2, starting transfers between devices: 29.6 us -> 8.72 us  [the longest x1 4.81 us: on_device(): lax.all_to_all(expert_rows, ep, split_axis=0, concat_axis=0, tiled=True)]
    all_to_all x0 -> x1, blocking collectives: none -> 19.5 us  [on_device(): own = lax.all_to_all(outgoing, ep, split_axis=0, concat_axis=0, tiled=True)]
    sub x1 -> x0, other arithmetic: 7.82 us -> none  [rotate(): front * cosine - back * sine]
  transfers between devices with their start and end apart: 6 -> 20, of which waited for: 4 -> 8; matrix products, arithmetic and copies ran while one was open for 31% -> 5% of each run, Pallas kernels for 0% -> 15%
where the time goes in v1:
time: 160 us; the launch traced here: 159 us
  Pallas kernels  46.8 us (29%)
  waiting for transfers between devices  45.6 us (28%)
  starting transfers between devices  32.4 us (20%)
  blocking collectives  19.5 us (12%)
  local copies, waits for them, and re-layouts  7.79 us (5%)
  other arithmetic  6.18 us (4%)
    ppermute x18, waiting for transfers between devices, shift(): return lax.ppermute(x, axis, pairs)  39.8 us
    ppermute x18, starting transfers between devices, shift(): return lax.ppermute(x, axis, pairs)  23.7 us
    all_to_all x1, blocking collectives, on_device(): own = lax.all_to_all(outgoing, ep, split_axis=0, concat_axis=0, tiled=True)  19.5 us
    pallas_call x1, Pallas kernels, ffn(): pl.pallas_call(functools.partial(ffn_kernel, n_x, tile), out_shape=[jax.S...  18.8 us
    pallas_call x1, Pallas kernels, project(): pl.pallas_call(project_kernel, grid=(parts,), out_shape=jax.ShapeDtypeStr...  9.59 us
    pallas_call x1, Pallas kernels, local_part(): pl.pallas_call(local_kernel, grid=(blocks,), out_shape=[jax.ShapeDtypeStr...  6.54 us
    unnamed x41, local copies, waits for them, and re-layouts  6.46 us
    all_to_all x1, waiting for transfers between devices, on_device(): lax.all_to_all(heads_out, tp, split_axis=0, concat_axis=0, tiled=True)  5.84 us
  transfers between devices with their start and end apart: 20, of which 8 were waited for; matrix products, arithmetic and copies ran while one was open for 5% of the time, Pallas kernels for 15%

profile of v1, /device:TPU:0, one launch (start us, length us, event | category | flops | bytes accessed | tf_op | source)
XLA Modules:
  0.0 159.2 jit_solution(17388388378843734349)
XLA Ops:
  0.6 1.4 copy.23.ids_ref
  2.0 2.3 %pre.1 = bf16[128,2048]{1,0:T(8,128)(2,1)} custom-call(bf16[32,2048]{1,0:T(8,128)(2,1)} %x_ref.1, s32[32,2]{1,0:T(8,128)} %copy.23.ids_ref, f32[1,2048]{1,0:T(1,128)} %bitcast.27), custom_call_target="tpu_custom_call" | custom-call | flops 2000000000 | bytes 1000000 | tf_op jit(solution)/shard_map/pre/pallas_call | solution.py:418
  4.3 19.5 %all_to_all.33 = bf16[16,8,2048]{2,1,0:T(8,128)(2,1)S(1)} all-to-all(bf16[16,8,2048]{2,1,0:T(8,128)(2,1)} %bitcast.22), channel_id=1, replica_groups=mesh['z'=4,'x'=4,'y'=4,'core'=2] {'z','x'}, dimensions={0} | all-to-all | bytes 1048576 | tf_op jit(solution)/shard_map/all_to_all | solution.py:424
  23.8 1.6 collective-permute-start.6
  25.4 1.7 %collective-permute-start.7 = (bf16[128,2048]{1,0:T(8,128)(2,1)S(1)}, bf16[128,2048]{1,0:T(8,128)(2,1)S(1)}, u32[]{:S(2)}, u32[]{:S(2)}) collective-permute-start(bf16[128,2048]{1,0:T(8,128)(2,1)S(1)} %bitcast.18), channel_id=1, source_target_pairs={{0,6},{2,0},{4,2},{6,4},{1,7},{3,1},{5,3},{7,5},{8,14},{10,8},{12,... | collective-permute-start | bytes 1572872 | tf_op jit(solution)/shard_map/ppermute | solution.py:33
  27.1 10.3 %collective-permute-done.6.refs_1_ = bf16[128,2048]{1,0:T(8,128)(2,1)S(1)} collective-permute-done((bf16[128,2048]{1,0:T(8,128)(2,1)S(1)}, bf16[128,2048]{1,0:T(8,128)(2,1)S(1)}, u32[]{:S(2)}, u32[]{:S(2)}) %collective-permute-start.6) | collective-permute-done | bytes 524320 | tf_op jit(solution)/shard_map/ppermute | solution.py:33
  37.4 0.4 collective-permute-start.8
  37.8 3.0 %collective-permute-start.9 = (bf16[64,2048]{1,0:T(8,128)(2,1)S(1)}, bf16[64,2048]{1,0:T(8,128)(2,1)S(1)}, u32[]{:S(2)}, u32[]{:S(2)}) collective-permute-start(bf16[64,2048]{1,0:T(8,128)(2,1)S(1)} %slice.25), channel_id=1, source_target_pairs={{0,6},{2,0},{4,2},{6,4},{1,7},{3,1},{5,3},{7,5},{8,14},{10,8},{12,... | collective-permute-start | bytes 786440 | tf_op jit(solution)/shard_map/ppermute | solution.py:33
  40.8 0.5 collective-permute-start.11
  41.3 3.7 %collective-permute-done.8 = bf16[64,2048]{1,0:T(8,128)(2,1)S(1)} collective-permute-done((bf16[64,2048]{1,0:T(8,128)(2,1)S(1)}, bf16[64,2048]{1,0:T(8,128)(2,1)S(1)}, u32[]{:S(2)}, u32[]{:S(2)}) %collective-permute-start.8) | collective-permute-done | bytes 262176 | tf_op jit(solution)/shard_map/ppermute | solution.py:33
  45.1 0.3 collective-permute-start.13
  45.4 1.8 %collective-permute-done.13.refs_7_ = bf16[128,2048]{1,0:T(8,128)(2,1)S(1)} collective-permute-done((bf16[128,2048]{1,0:T(8,128)(2,1)S(1)}, bf16[128,2048]{1,0:T(8,128)(2,1)S(1)}, u32[]{:S(2)}, u32[]{:S(2)}) %collective-permute-start.13) | collective-permute-done | bytes 524320 | tf_op jit(solution)/shard_map/ppermute | solution.py:33
  47.3 0.8 copy-done.12
  48.2 18.8 %ffn.1 = (bf16[512,2048]{1,0:T(8,128)(2,1)}, bf16[512,2048]{1,0:T(8,128)(2,1)}) custom-call(bf16[128,2048]{1,0:T(8,128)(2,1)} %bitcast.20, bf16[128,2048]{1,0:T(8,128)(2,1)} %copy-done.4, bf16[128,2048]{1,0:T(8,128)(2,1)} %copy-done.5, bf16[128,2048]{1,0:T(8,128)(2,1)} %copy-done.6, bf16[128,2048]{1,0:T(8,128)(2,1)} %copy-done.9, ...), custom_call_target="tpu_custom_call" | custom-call | flops 11274289152 | bytes 19398656 | tf_op jit(solution)/shard_map/ffn/pallas_call | solution.py:146
  67.0 0.2 collective-permute-start.14
  67.2 0.1 mul.40
  67.3 0.1 multiply_cosine_fusion
  67.3 0.6 pad_maximum_fusion.base_ref
  67.9 6.5 %local.1 = (f32[2048,256]{1,0:T(8,128)}, bf16[2048,256]{1,0:T(8,128)(2,1)}, bf16[264,256]{1,0:T(8,128)(2,1)}) custom-call(f32[4,2,128]{2,1,0:T(2,128)} %pad_maximum_fusion.base_ref, bf16[2048,256]{1,0:T(8,128)(2,1)} %q_ref.1, bf16[2048,256]{1,0:T(8,128)(2,1)} %k_ref.1, bf16[2048,256]{1,0:T(8,128)(2,1)} %v_ref.1, f32[4,1,512]{2,1,0:T(1,128)} %bitcast.28, ...), custom_call_target="tpu_custom_call" | custom-call | flops 6000000000 | bytes 6291456 | tf_op jit(solution)/shard_map/local/pallas_call | solution.py:245
  74.5 0.6 collective-permute-start
  75.1 1.7 %collective-permute-start.1 = (bf16[264,256]{1,0:T(8,128)(2,1)}, bf16[264,256]{1,0:T(8,128)(2,1)S(1)}, u32[]{:S(2)}, u32[]{:S(2)}) collective-permute-start(bf16[264,256]{1,0:T(8,128)(2,1)} %get-tuple-element.9.own_ref), channel_id=1, source_target_pairs={{0,16},{8,24},{16,0},{24,8},{1,17},{9,25},{17,1},{25,9},{2,18},{10... | collective-permute-start | bytes 405512 | tf_op jit(solution)/shard_map/ppermute | solution.py:33
  76.8 1.3 collective-permute-start.2
  78.1 6.6 %collective-permute-done.one_ref = bf16[264,256]{1,0:T(8,128)(2,1)S(1)} collective-permute-done((bf16[264,256]{1,0:T(8,128)(2,1)}, bf16[264,256]{1,0:T(8,128)(2,1)S(1)}, u32[]{:S(2)}, u32[]{:S(2)}) %collective-permute-start) | collective-permute-done | bytes 135200 | tf_op jit(solution)/shard_map/ppermute | solution.py:33
  84.7 0.6 collective-permute-done.2.three_ref
  85.4 0.0 copy-done.17
  85.4 0.6 copy-done.18
  86.0 2.1 %middle.1 = (f32[264,256]{1,0:T(8,128)}, bf16[264,256]{1,0:T(8,128)(2,1)}) custom-call(s32[1]{0:T(128)} %bitcast.x_ref, bf16[264,256]{1,0:T(8,128)(2,1)} %get-tuple-element.9.own_ref, bf16[264,256]{1,0:T(8,128)(2,1)} %copy-done.16, bf16[264,256]{1,0:T(8,128)(2,1)} %copy-done.17, bf16[264,256]{1,0:T(8,128)(2,1)} %copy-done.18), custom_call_target="tpu_custom_call" | custom-call | flops 500000000 | bytes 1000000 | tf_op jit(solution)/shard_map/middle/pallas_call | solution.py:298
  88.1 1.9 %collective-permute-start.3 = (bf16[264,256]{1,0:T(8,128)(2,1)}, bf16[264,256]{1,0:T(8,128)(2,1)S(1)}, u32[]{:S(2)}, u32[]{:S(2)}) collective-permute-start(bf16[264,256]{1,0:T(8,128)(2,1)} %get-tuple-element.11), channel_id=1, source_target_pairs={{0,32},{32,64},{64,96},{1,33},{33,65},{65,97},{2,34},{34,66},{66,9... | collective-permute-start | bytes 405512 | tf_op jit(solution)/shard_map/ppermute | solution.py:33
  90.1 4.5 %collective-permute-start.4 = (bf16[264,256]{1,0:T(8,128)(2,1)}, bf16[264,256]{1,0:T(8,128)(2,1)S(1)}, u32[]{:S(2)}, u32[]{:S(2)}) collective-permute-start(bf16[264,256]{1,0:T(8,128)(2,1)} %get-tuple-element.11), channel_id=1, source_target_pairs={{0,64},{32,96},{1,65},{33,97},{2,66},{34,98},{3,67},{35,99},{4,68}... | collective-permute-start | bytes 405512 | tf_op jit(solution)/shard_map/ppermute | solution.py:33
  94.6 1.3 collective-permute-start.5
  95.9 1.4 copy-done
  97.3 3.0 %add_convert_fusion = bf16[512,2048]{1,0:T(8,128)(2,1)S(1)} fusion(bf16[512,2048]{1,0:T(8,128)(2,1)} %copy-done, bf16[512,2048]{1,0:T(8,128)(2,1)} %get-tuple-element.14), kind=kLoop, calls=%fused_computation | loop fusion | flops 4194304 | bytes 6291456 | tf_op jit(solution)/shard_map/convert_element_type | solution.py:455
  100.3 1.2 fusion.1
  101.5 3.3 %collective-permute-start.15 = (bf16[128,2048]{1,0:T(8,128)(2,1)}, bf16[128,2048]{1,0:T(8,128)(2,1)}, u32[]{:S(2)}, u32[]{:S(2)}) collective-permute-start(bf16[128,2048]{1,0:T(8,128)(2,1)} %get-tuple-element.16), channel_id=1, source_target_pairs={{0,6},{2,0},{4,2},{6,4},{1,7},{3,1},{5,3},{7,5},{8,14},{10,8},{12,... | collective-permute-start | bytes 1572872 | tf_op jit(solution)/shard_map/ppermute | solution.py:33
  104.8 1.5 collective-permute-start.17
  106.3 0.6 copy-done.14
  106.9 0.1 copy-done.15
  107.0 5.0 %finish.1 = bf16[2048,256]{1,0:T(8,128)(2,1)} custom-call(f32[264,256]{1,0:T(8,128)} %get-tuple-element.10.before_ref, bf16[264,256]{1,0:T(8,128)(2,1)} %copy-done.13, bf16[264,256]{1,0:T(8,128)(2,1)} %copy-done.14, bf16[264,256]{1,0:T(8,128)(2,1)} %copy-done.15, f32[2048,256]{1,0:T(8,128)} %get-tuple-element.12.kept_ref, ...), custom_call_target="tpu_custom_call" | custom-call | flops 2000000000 | bytes 5242880 | tf_op jit(solution)/shard_map/finish/pallas_call | solution.py:336
  112.0 3.9 %all-to-all-start = ((bf16[8,256,256]{2,1,0:T(8,128)(2,1)}), bf16[8,256,256]{2,1,0:T(8,128)(2,1)S(1)}, u32[]{:S(2)}, u32[]{:S(2)}) async-start(bf16[8,256,256]{2,1,0:T(8,128)(2,1)} %bitcast.16), calls=%async_computation | async-start | bytes 2097152 | tf_op jit(solution)/shard_map/all_to_all | solution.py:445
  115.9 13.6 %collective-permute-done.15 = bf16[128,2048]{1,0:T(8,128)(2,1)} collective-permute-done((bf16[128,2048]{1,0:T(8,128)(2,1)}, bf16[128,2048]{1,0:T(8,128)(2,1)}, u32[]{:S(2)}, u32[]{:S(2)}) %collective-permute-start.15) | collective-permute-done | bytes 524320 | tf_op jit(solution)/shard_map/ppermute | solution.py:33
  129.5 3.1 %collective-permute-done.16 = bf16[128,2048]{1,0:T(8,128)(2,1)} collective-permute-done((bf16[128,2048]{1,0:T(8,128)(2,1)}, bf16[128,2048]{1,0:T(8,128)(2,1)}, u32[]{:S(2)}, u32[]{:S(2)}) %collective-permute-start.16) | collective-permute-done | bytes 524320 | tf_op jit(solution)/shard_map/ppermute | solution.py:33
  132.6 2.5 %fusion = bf16[16,8,2048]{2,1,0:T(8,128)(2,1)} fusion(bf16[128,2048]{1,0:T(8,128)(2,1)} %collective-permute-done.17, bf16[128,2048]{1,0:T(8,128)(2,1)} %collective-permute-done.16, bf16[128,2048]{1,0:T(8,128)(2,1)} %collective-permute-done.15, bf16[512,2048]{1,0:T(8,128)(2,1)S(1)} %add_convert_fusion), kind=kLoop, calls=%fused_computation.2 | loop fusion | flops 2097152 | bytes 2621440 | tf_op jit(solution)/shard_map/all_to_all | solution.py:464
  135.1 5.8 %all-to-all-done = bf16[8,256,256]{2,1,0:T(8,128)(2,1)S(1)} async-done(((bf16[8,256,256]{2,1,0:T(8,128)(2,1)}), bf16[8,256,256]{2,1,0:T(8,128)(2,1)S(1)}, u32[]{:S(2)}, u32[]{:S(2)}) %all-to-all-start) | async-done | bytes 1048608 | tf_op jit(solution)/shard_map/all_to_all | solution.py:445
  140.9 4.8 %all-to-all-start.2 = ((bf16[16,8,2048]{2,1,0:T(8,128)(2,1)}), bf16[16,8,2048]{2,1,0:T(8,128)(2,1)S(1)}, u32[]{:S(2)}, u32[]{:S(2)}) async-start(bf16[16,8,2048]{2,1,0:T(8,128)(2,1)} %fusion), calls=%async_computation.2 | async-start | bytes 1048576 | tf_op jit(solution)/shard_map/all_to_all | solution.py:464
  145.7 0.7 copy.25.weights_ref
  146.4 9.6 %project.1 = bf16[256,2048]{1,0:T(8,128)(2,1)} custom-call(bf16[2048,256]{1,0:T(8,128)(2,1)} %bitcast.15, bf16[2048,2048]{1,0:T(8,128)(2,1)} %w_ref.1), custom_call_target="tpu_custom_call" | custom-call | flops 4000000000 | bytes 10485760 | tf_op jit(solution)/shard_map/project/pallas_call | solution.py:372
  156.0 0.8 copy-done.3
  156.8 2.4 %combine.1 = bf16[32,2048]{1,0:T(8,128)(2,1)} custom-call(bf16[128,2048]{1,0:T(8,128)(2,1)} %bitcast.21, s32[32,2]{1,0:T(8,128)} %copy.23.ids_ref, f32[32,2]{1,0:T(8,128)} %copy.25.weights_ref), custom_call_target="tpu_custom_call" | custom-call | flops 1000000000 | bytes 1000000 | tf_op jit(solution)/shard_map/combine/pallas_call | solution.py:466
  (51 shorter events, 0.2 us)
Async XLA Ops:
  23.8 24.3 %copy-start.2 = (bf16[16,8,2048]{2,1,0:T(8,128)(2,1)}, bf16[16,8,2048]{2,1,0:T(8,128)(2,1)S(1)}, u32[]{:S(2)}) copy-start(bf16[16,8,2048]{2,1,0:T(8,128)(2,1)S(1)} %all_to_all.33) | copy-start | bytes 1572868
  23.8 13.6 %collective-permute-start.6 = (bf16[128,2048]{1,0:T(8,128)(2,1)S(1)}, bf16[128,2048]{1,0:T(8,128)(2,1)S(1)}, u32[]{:S(2)}, u32[]{:S(2)}) collective-permute-start(bf16[128,2048]{1,0:T(8,128)(2,1)S(1)} %bitcast.17), channel_id=1, source_target_pairs={{0,2},{2,4},{4,6},{6,0},{1,3},{3,5},{5,7},{7,1},{8,10},{10,12},{12... | collective-permute-start | bytes 1572872 | tf_op jit(solution)/shard_map/ppermute | solution.py:33
  25.4 12.4 %collective-permute-start.7 = (bf16[128,2048]{1,0:T(8,128)(2,1)S(1)}, bf16[128,2048]{1,0:T(8,128)(2,1)S(1)}, u32[]{:S(2)}, u32[]{:S(2)}) collective-permute-start(bf16[128,2048]{1,0:T(8,128)(2,1)S(1)} %bitcast.18), channel_id=1, source_target_pairs={{0,6},{2,0},{4,2},{6,4},{1,7},{3,1},{5,3},{7,5},{8,14},{10,8},{12,... | collective-permute-start | bytes 1572872 | tf_op jit(solution)/shard_map/ppermute | solution.py:33
  37.4 10.8 %copy-start.4 = (bf16[128,2048]{1,0:T(8,128)(2,1)}, bf16[128,2048]{1,0:T(8,128)(2,1)S(1)}, u32[]{:S(2)}) copy-start(bf16[128,2048]{1,0:T(8,128)(2,1)S(1)} %collective-permute-done.6.refs_1_) | copy-start | bytes 1572868
  37.4 7.7 %collective-permute-start.8 = (bf16[64,2048]{1,0:T(8,128)(2,1)S(1)}, bf16[64,2048]{1,0:T(8,128)(2,1)S(1)}, u32[]{:S(2)}, u32[]{:S(2)}) collective-permute-start(bf16[64,2048]{1,0:T(8,128)(2,1)S(1)} %slice.24), channel_id=1, source_target_pairs={{0,2},{2,4},{4,6},{6,0},{1,3},{3,5},{5,7},{7,1},{8,10},{10,12},{12... | collective-permute-start | bytes 786440 | tf_op jit(solution)/shard_map/ppermute | solution.py:33
  37.8 10.4 %copy-start.5 = (bf16[128,2048]{1,0:T(8,128)(2,1)}, bf16[128,2048]{1,0:T(8,128)(2,1)S(1)}, u32[]{:S(2)}) copy-start(bf16[128,2048]{1,0:T(8,128)(2,1)S(1)} %collective-permute-done.7.refs_2_) | copy-start | bytes 1572868
  37.8 7.3 %collective-permute-start.9 = (bf16[64,2048]{1,0:T(8,128)(2,1)S(1)}, bf16[64,2048]{1,0:T(8,128)(2,1)S(1)}, u32[]{:S(2)}, u32[]{:S(2)}) collective-permute-start(bf16[64,2048]{1,0:T(8,128)(2,1)S(1)} %slice.25), channel_id=1, source_target_pairs={{0,6},{2,0},{4,2},{6,4},{1,7},{3,1},{5,3},{7,5},{8,14},{10,8},{12,... | collective-permute-start | bytes 786440 | tf_op jit(solution)/shard_map/ppermute | solution.py:33
  40.8 4.6 %collective-permute-start.10 = (bf16[128,2048]{1,0:T(8,128)(2,1)S(1)}, bf16[128,2048]{1,0:T(8,128)(2,1)S(1)}, u32[]{:S(2)}, u32[]{:S(2)}) collective-permute-start(bf16[128,2048]{1,0:T(8,128)(2,1)S(1)} %bitcast.19), channel_id=1, source_target_pairs={{0,1},{1,0},{2,3},{3,2},{4,5},{5,4},{6,7},{7,6},{8,9},{9,8},{10,11... | collective-permute-start | bytes 1572872 | tf_op jit(solution)/shard_map/ppermute | solution.py:33
  40.8 4.6 %collective-permute-start.11 = (bf16[128,2048]{1,0:T(8,128)(2,1)S(1)}, bf16[128,2048]{1,0:T(8,128)(2,1)S(1)}, u32[]{:S(2)}, u32[]{:S(2)}) collective-permute-start(bf16[128,2048]{1,0:T(8,128)(2,1)S(1)} %collective-permute-done.6.refs_1_), channel_id=1, source_target_pairs={{0,1},{1,0},{2,3},{3,2},{4,5},{5,4},{6,7},{7,6},{8,9},{9,8},{10,11... | collective-permute-start | bytes 1572872 | tf_op jit(solution)/shard_map/ppermute | solution.py:33
  41.3 4.1 %collective-permute-start.12 = (bf16[128,2048]{1,0:T(8,128)(2,1)S(1)}, bf16[128,2048]{1,0:T(8,128)(2,1)S(1)}, u32[]{:S(2)}, u32[]{:S(2)}) collective-permute-start(bf16[128,2048]{1,0:T(8,128)(2,1)S(1)} %collective-permute-done.7.refs_2_), channel_id=1, source_target_pairs={{0,1},{1,0},{2,3},{3,2},{4,5},{5,4},{6,7},{7,6},{8,9},{9,8},{10,11... | collective-permute-start | bytes 1572872 | tf_op jit(solution)/shard_map/ppermute | solution.py:33
  45.1 3.0 %copy-start.6 = (bf16[128,2048]{1,0:T(8,128)(2,1)}, bf16[128,2048]{1,0:T(8,128)(2,1)S(1)}, u32[]{:S(2)}) copy-start(bf16[128,2048]{1,0:T(8,128)(2,1)S(1)} %constant_dynamic-update-slice_fusion.refs_3_) | copy-start | bytes 1572868
  45.1 2.2 %collective-permute-start.13 = (bf16[128,2048]{1,0:T(8,128)(2,1)S(1)}, bf16[128,2048]{1,0:T(8,128)(2,1)S(1)}, u32[]{:S(2)}, u32[]{:S(2)}) collective-permute-start(bf16[128,2048]{1,0:T(8,128)(2,1)S(1)} %constant_dynamic-update-slice_fusion.refs_3_), channel_id=1, source_target_pairs={{0,1},{1,0},{2,3},{3,2},{4,5},{5,4},{6,7},{7,6},{8,9},{9,8},{10,11... | collective-permute-start | bytes 1572872 | tf_op jit(solution)/shard_map/ppermute | solution.py:33
  45.4 2.7 %copy-start.9 = (bf16[128,2048]{1,0:T(8,128)(2,1)}, bf16[128,2048]{1,0:T(8,128)(2,1)S(1)}, u32[]{:S(2)}) copy-start(bf16[128,2048]{1,0:T(8,128)(2,1)S(1)} %collective-permute-done.10.refs_4_) | copy-start | bytes 1572868
  45.4 2.7 %copy-start.10 = (bf16[128,2048]{1,0:T(8,128)(2,1)}, bf16[128,2048]{1,0:T(8,128)(2,1)S(1)}, u32[]{:S(2)}) copy-start(bf16[128,2048]{1,0:T(8,128)(2,1)S(1)} %collective-permute-done.11.refs_5_) | copy-start | bytes 1572868
  45.4 1.9 %copy-start.11 = (bf16[128,2048]{1,0:T(8,128)(2,1)}, bf16[128,2048]{1,0:T(8,128)(2,1)S(1)}, u32[]{:S(2)}) copy-start(bf16[128,2048]{1,0:T(8,128)(2,1)S(1)} %collective-permute-done.12.refs_6_) | copy-start | bytes 1572868
  47.3 0.8 copy-start.12
  48.1 19.1 %copy-start.8 = (f32[128]{0:T(128)S(1)}, f32[128]{0:T(128)}, u32[]{:S(2)}) copy-start(f32[128]{0:T(128)} %constant.21.clone) | copy-start | bytes 1540
  67.0 28.9 %collective-permute-start.14 = (bf16[512,2048]{1,0:T(8,128)(2,1)}, bf16[512,2048]{1,0:T(8,128)(2,1)S(1)}, u32[]{:S(2)}, u32[]{:S(2)}) collective-permute-start(bf16[512,2048]{1,0:T(8,128)(2,1)} %get-tuple-element.15), channel_id=1, source_target_pairs={{0,1},{1,0},{2,3},{3,2},{4,5},{5,4},{6,7},{7,6},{8,9},{9,8},{10,11... | collective-permute-start | bytes 6291464 | tf_op jit(solution)/shard_map/ppermute | solution.py:33
  74.5 10.2 %collective-permute-start = (bf16[264,256]{1,0:T(8,128)(2,1)}, bf16[264,256]{1,0:T(8,128)(2,1)S(1)}, u32[]{:S(2)}, u32[]{:S(2)}) collective-permute-start(bf16[264,256]{1,0:T(8,128)(2,1)} %get-tuple-element.9.own_ref), channel_id=1, source_target_pairs={{0,8},{8,16},{16,24},{24,0},{1,9},{9,17},{17,25},{25,1},{2,10},{10... | collective-permute-start | bytes 405512 | tf_op jit(solution)/shard_map/ppermute | solution.py:33
  75.1 9.6 %collective-permute-start.1 = (bf16[264,256]{1,0:T(8,128)(2,1)}, bf16[264,256]{1,0:T(8,128)(2,1)S(1)}, u32[]{:S(2)}, u32[]{:S(2)}) collective-permute-start(bf16[264,256]{1,0:T(8,128)(2,1)} %get-tuple-element.9.own_ref), channel_id=1, source_target_pairs={{0,16},{8,24},{16,0},{24,8},{1,17},{9,25},{17,1},{25,9},{2,18},{10... | collective-permute-start | bytes 405512 | tf_op jit(solution)/shard_map/ppermute | solution.py:33
  76.8 8.6 %collective-permute-start.2 = (bf16[264,256]{1,0:T(8,128)(2,1)}, bf16[264,256]{1,0:T(8,128)(2,1)S(1)}, u32[]{:S(2)}, u32[]{:S(2)}) collective-permute-start(bf16[264,256]{1,0:T(8,128)(2,1)} %get-tuple-element.9.own_ref), channel_id=1, source_target_pairs={{0,24},{8,0},{16,8},{24,16},{1,25},{9,1},{17,9},{25,17},{2,26},{10... | collective-permute-start | bytes 405512 | tf_op jit(solution)/shard_map/ppermute | solution.py:33
  84.7 0.7 copy-start.16
  84.7 0.7 copy-start.17
  85.3 0.7 copy-start.18
  88.1 16.7 %collective-permute-start.3 = (bf16[264,256]{1,0:T(8,128)(2,1)}, bf16[264,256]{1,0:T(8,128)(2,1)S(1)}, u32[]{:S(2)}, u32[]{:S(2)}) collective-permute-start(bf16[264,256]{1,0:T(8,128)(2,1)} %get-tuple-element.11), channel_id=1, source_target_pairs={{0,32},{32,64},{64,96},{1,33},{33,65},{65,97},{2,34},{34,66},{66,9... | collective-permute-start | bytes 405512 | tf_op jit(solution)/shard_map/ppermute | solution.py:33
  90.1 16.2 %collective-permute-start.4 = (bf16[264,256]{1,0:T(8,128)(2,1)}, bf16[264,256]{1,0:T(8,128)(2,1)S(1)}, u32[]{:S(2)}, u32[]{:S(2)}) collective-permute-start(bf16[264,256]{1,0:T(8,128)(2,1)} %get-tuple-element.11), channel_id=1, source_target_pairs={{0,64},{32,96},{1,65},{33,97},{2,66},{34,98},{3,67},{35,99},{4,68}... | collective-permute-start | bytes 405512 | tf_op jit(solution)/shard_map/ppermute | solution.py:33
  94.6 11.7 %collective-permute-start.5 = (bf16[264,256]{1,0:T(8,128)(2,1)}, bf16[264,256]{1,0:T(8,128)(2,1)S(1)}, u32[]{:S(2)}, u32[]{:S(2)}) collective-permute-start(bf16[264,256]{1,0:T(8,128)(2,1)} %get-tuple-element.11), channel_id=1, source_target_pairs={{0,96},{1,97},{2,98},{3,99},{4,100},{5,101},{6,102},{7,103},{8,104... | collective-permute-start | bytes 405512 | tf_op jit(solution)/shard_map/ppermute | solution.py:33
  95.9 1.4 copy-start
  101.5 28.0 %collective-permute-start.15 = (bf16[128,2048]{1,0:T(8,128)(2,1)}, bf16[128,2048]{1,0:T(8,128)(2,1)}, u32[]{:S(2)}, u32[]{:S(2)}) collective-permute-start(bf16[128,2048]{1,0:T(8,128)(2,1)} %get-tuple-element.16), channel_id=1, source_target_pairs={{0,6},{2,0},{4,2},{6,4},{1,7},{3,1},{5,3},{7,5},{8,14},{10,8},{12,... | collective-permute-start | bytes 1572872 | tf_op jit(solution)/shard_map/ppermute | solution.py:33
  104.8 27.8 %collective-permute-start.16 = (bf16[128,2048]{1,0:T(8,128)(2,1)}, bf16[128,2048]{1,0:T(8,128)(2,1)}, u32[]{:S(2)}, u32[]{:S(2)}) collective-permute-start(bf16[128,2048]{1,0:T(8,128)(2,1)} %get-tuple-element.18), channel_id=1, source_target_pairs={{0,2},{2,4},{4,6},{6,0},{1,3},{3,5},{5,7},{7,1},{8,10},{10,12},{12... | collective-permute-start | bytes 1572872 | tf_op jit(solution)/shard_map/ppermute | solution.py:33
  104.8 1.5 copy-start.13
  104.8 27.8 %collective-permute-start.17 = (bf16[128,2048]{1,0:T(8,128)(2,1)}, bf16[128,2048]{1,0:T(8,128)(2,1)}, u32[]{:S(2)}, u32[]{:S(2)}) collective-permute-start(bf16[128,2048]{1,0:T(8,128)(2,1)} %get-tuple-element.17), channel_id=1, source_target_pairs={{0,4},{2,6},{4,0},{6,2},{1,5},{3,7},{5,1},{7,3},{8,12},{10,14},{12... | collective-permute-start | bytes 1572872 | tf_op jit(solution)/shard_map/ppermute | solution.py:33
  106.3 0.7 copy-start.14
  106.3 0.7 copy-start.15
  112.0 28.9 %all-to-all-start = ((bf16[8,256,256]{2,1,0:T(8,128)(2,1)}), bf16[8,256,256]{2,1,0:T(8,128)(2,1)S(1)}, u32[]{:S(2)}, u32[]{:S(2)}) async-start(bf16[8,256,256]{2,1,0:T(8,128)(2,1)} %bitcast.16), calls=%async_computation | async-start | bytes 2097152 | tf_op jit(solution)/shard_map/all_to_all | solution.py:445
  115.9 29.8 %copy-start.7 = (f32[32,2]{0,1:T(2,128)S(1)}, f32[32,2]{0,1:T(2,128)}, u32[]{:S(2)}) copy-start(f32[32,2]{0,1:T(2,128)} %param.26) | copy-start | bytes 772
  140.9 5.5 %copy-start.1 = (bf16[8,256,256]{2,1,0:T(8,128)(2,1)}, bf16[8,256,256]{2,1,0:T(8,128)(2,1)S(1)}, u32[]{:S(2)}) copy-start(bf16[8,256,256]{2,1,0:T(8,128)(2,1)S(1)} %all-to-all-done) | copy-start | bytes 3145732
  140.9 15.1 %all-to-all-start.2 = ((bf16[16,8,2048]{2,1,0:T(8,128)(2,1)}), bf16[16,8,2048]{2,1,0:T(8,128)(2,1)S(1)}, u32[]{:S(2)}, u32[]{:S(2)}) async-start(bf16[16,8,2048]{2,1,0:T(8,128)(2,1)} %fusion), calls=%async_computation.2 | async-start | bytes 1048576 | tf_op jit(solution)/shard_map/all_to_all | solution.py:464
  156.0 0.8 copy-start.3

commit v2 on v1

--- a/solution.py
+++ b/solution.py
@@ -33,118 +33,113 @@
     return lax.ppermute(x, axis, pairs)
 
 
-def route_tables(ids):
-    tokens = ids.shape[0]
-    lane = lax.broadcasted_iota(jnp.int32, (tokens, EXPERTS), 1)
-    first = (ids[:, 0:1] == lane).astype(f32)
-    second = (ids[:, 1:2] == lane).astype(f32)
-    both = first + second
-    below = (
-        lax.broadcasted_iota(jnp.int32, (tokens, tokens), 1)
-        < lax.broadcasted_iota(jnp.int32, (tokens, tokens), 0)
+def after(x, *earlier):
+    return lax.optimization_barrier((x, *earlier))[0]
+
+
+def route_tables(ids_ref):
+    tokens = ids_ref.shape[1]
+    expert = lax.broadcasted_iota(jnp.int32, (EXPERTS, tokens), 0)
+    named = [(ids_ref[k : k + 1, :] == expert).astype(f32) for k in range(2)]
+    earlier = (
+        lax.broadcasted_iota(jnp.int32, (tokens, tokens), 0)
+        < lax.broadcasted_iota(jnp.int32, (tokens, tokens), 1)
     ).astype(f32)
-    rank = mm(below, both)
-    return first, second, both, rank
-
-
-def pre_kernel(x_ref, ids_ref, gain_ref, out_ref):
-    _, _, both, rank = route_tables(ids_ref[...])
-    tokens = x_ref.shape[0]
+    rank = mm(named[0] + named[1], earlier)
     row = lax.broadcasted_iota(jnp.int32, (SLOTS, EXPERTS), 0)
     col = lax.broadcasted_iota(jnp.int32, (SLOTS, EXPERTS), 1)
     spread = (row // CAP == col).astype(f32)
-    named = lax.dot_general(spread, both, NT, preferred_element_type=f32)
-    ranks = lax.dot_general(spread, rank, NT, preferred_element_type=f32)
     slot = (lax.broadcasted_iota(jnp.int32, (SLOTS, tokens), 0) % CAP).astype(f32)
-    pick = jnp.where((named > 0.5) & (jnp.abs(ranks - slot) < 0.5), 1.0, 0.0).astype(bf16)
+    here = jnp.abs(mm(spread, rank) - slot) < 0.5
+    return [jnp.where((mm(spread, n) > 0.5) & here, 1.0, 0.0) for n in named]
+
+
+def pre_kernel(x_ref, ids_ref, gain_ref, out_ref):
+    first, second = route_tables(ids_ref)
     x = x_ref[...].astype(f32)
     scale = lax.rsqrt(jnp.mean(x * x, axis=-1, keepdims=True) + norm_eps)
     normed = (x * scale * gain_ref[...]).astype(bf16)
-    out_ref[...] = mm(pick, normed).astype(bf16)
+    out_ref[...] = mm((first + second).astype(bf16), normed).astype(bf16)
 
 
 def combine_kernel(rows_ref, ids_ref, weights_ref, out_ref):
-    first, second, _, rank = route_tables(ids_ref[...])
-    tokens = ids_ref.shape[0]
-    row = lax.broadcasted_iota(jnp.int32, (EXPERTS, SLOTS), 0)
-    col = lax.broadcasted_iota(jnp.int32, (EXPERTS, SLOTS), 1)
-    spread = (col // CAP == row).astype(f32)
-    slot = (lax.broadcasted_iota(jnp.int32, (tokens, SLOTS), 1) % CAP).astype(f32)
-    here = jnp.abs(mm(rank, spread) - slot) < 0.5
+    tokens = ids_ref.shape[1]
     rows = rows_ref[...]
+    diagonal = lax.broadcasted_iota(jnp.int32, (tokens, tokens), 0) == lax.broadcasted_iota(
+        jnp.int32, (tokens, tokens), 1
+    )
     total = None
-    for k, named in enumerate((first, second)):
-        pick = jnp.where((mm(named, spread) > 0.5) & here, 1.0, 0.0).astype(bf16)
-        part = mm(pick, rows) * weights_ref[:, k : k + 1]
+    for k, pick in enumerate(route_tables(ids_ref)):
+        weight = jnp.sum(
+            jnp.where(diagonal, weights_ref[k : k + 1, :], 0.0), axis=1, keepdims=True
+        )
+        part = lax.dot_general(pick.astype(bf16), rows, TN, preferred_element_type=f32) * weight
         total = part if total is None else total + part
     out_ref[...] = total.astype(bf16)
 
 
-def ffn_kernel(n_x, tile, *refs):
+def ffn_kernel(n_x, tile, groups, *refs):
     xs = refs[:n_x]
     wg, wu, wd = refs[n_x : n_x + 3]
     outs = refs[n_x + 3 : -9]
     xbuf, gbuf, ubuf, dbuf, hbuf, obuf, xsem, wsem, osem = refs[-9:]
-    ff = gbuf.shape[1]
-    chunks = ff // 128
     per_out = n_x // len(outs)
     copies_w = []
-    for j in range(chunks):
-        cols = pl.ds(j * 128, 128)
+    for j, (lo, hi) in enumerate(groups):
+        cols = pl.ds(lo, hi - lo)
         a = pltpu.make_async_copy(wg.at[:, cols], gbuf.at[:, cols], wsem.at[2 * j])
         b = pltpu.make_async_copy(wu.at[:, cols], ubuf.at[:, cols], wsem.at[2 * j + 1])
         copies_w.append((a, b))
+    copies_x = [
+        pltpu.make_async_copy(xs[i], xbuf.at[pl.ds(i * tile, tile)], xsem.at[i])
+        for i in range(n_x)
+    ]
+    pair = 256 // tile
     for c in copies_w[0]:
         c.start()
-    copies_x = []
-    for i in range(n_x):
-        c = pltpu.make_async_copy(xs[i], xbuf.at[pl.ds(i * tile, tile)], xsem.at[i])
+    for c in copies_x:
         c.start()
-        copies_x.append(c)
-    for pair in copies_w[1:]:
-        for c in pair:
-            c.start()
-    down = pltpu.make_async_copy(wd, dbuf, wsem.at[2 * chunks])
+    for c in copies_w[1]:
+        c.start()
+    down = pltpu.make_async_copy(wd, dbuf, wsem.at[2 * len(groups)])
     down.start()
-    for j in range(chunks):
+    for j, (lo, hi) in enumerate(groups):
         for c in copies_w[j]:
             c.wait()
-        w = jnp.concatenate(
-            [gbuf[:, j * 128 : (j + 1) * 128], ubuf[:, j * 128 : (j + 1) * 128]], axis=1
-        )
-        step = 256
-        for r in range(0, n_x * tile, step):
+        for r in range(0, n_x * tile, 256):
             if j == 0:
-                for i in range(r // tile, (r + step) // tile):
+                for i in range(r // tile, r // tile + pair):
                     copies_x[i].wait()
-            both = mm(xbuf[r : r + step, :], w)
-            gate, up = both[:, :128], both[:, 128:]
-            hidden = gate * up / (1.0 + jnp.exp(-gate))
-            hbuf[r : r + step, j * 128 : (j + 1) * 128] = hidden.astype(bf16)
+            x = xbuf[r : r + 256, :]
+            for at in range(lo, hi, 128):
+                w = jnp.concatenate([gbuf[:, at : at + 128], ubuf[:, at : at + 128]], axis=1)
+                both = mm(x, w)
+                gate, up = both[:, :128], both[:, 128:]
+                hidden = gate * up / (1.0 + jnp.exp(-gate))
+                hbuf[r : r + 256, at : at + 128] = hidden.astype(bf16)
     down.wait()
-    outs_c = []
-    for o in range(len(outs)):
-        for i in range(per_out):
-            r = (o * per_out + i) * tile
-            if r % 256 == 0:
-                obuf[r : r + 256, :] = mm(hbuf[r : r + 256, :], dbuf[...]).astype(bf16)
-                last = pltpu.make_async_copy(
-                    obuf.at[pl.ds(r, 256)], outs[o].at[pl.ds(i * tile, 256)], osem.at[r // 256]
-                )
-                last.start()
-                outs_c.append(last)
-    for c in outs_c:
+    stores = []
+    for r in range(0, n_x * tile, 256):
+        obuf[r : r + 256, :] = mm(hbuf[r : r + 256, :], dbuf[...]).astype(bf16)
+        for i in range(r // tile, r // tile + pair):
+            to = outs[i // per_out].at[pl.ds((i % per_out) * tile, tile)]
+            c = pltpu.make_async_copy(obuf.at[pl.ds(i * tile, tile)], to, osem.at[i])
+            c.start()
+            stores.append(c)
+    for c in stores:
         c.wait()
 
 
-def ffn(xs, w_gate, w_up, w_down, n_out):
+def ffn(name, xs, w_gate, w_up, w_down, n_out):
     n_x = len(xs)
     tile, width = xs[0].shape
     ff = w_gate.shape[1]
     rows = n_x * tile
+    cut = 128 * ((ff // 128 + 1) // 2)
+    groups = ((0, cut), (cut, ff))
     hbm = pl.BlockSpec(memory_space=pl.ANY)
     return pl.pallas_call(
-        functools.partial(ffn_kernel, n_x, tile),
+        functools.partial(ffn_kernel, n_x, tile, groups),
         out_shape=[jax.ShapeDtypeStruct((rows // n_out, width), bf16)] * n_out,
         in_specs=[hbm] * (n_x + 3),
         out_specs=[hbm] * n_out,
@@ -156,15 +151,15 @@
             pltpu.VMEM((rows, ff), bf16),
             pltpu.VMEM((rows, width), bf16),
             pltpu.SemaphoreType.DMA((n_x,)),
-            pltpu.SemaphoreType.DMA((2 * (ff // 128) + 1,)),
-            pltpu.SemaphoreType.DMA((rows // 256,)),
+            pltpu.SemaphoreType.DMA((2 * len(groups) + 1,)),
+            pltpu.SemaphoreType.DMA((n_x,)),
         ],
         cost_estimate=pl.CostEstimate(
             flops=6 * rows * width * ff,
             bytes_accessed=2 * (3 * width * ff + 2 * rows * width),
             transcendentals=rows * ff,
         ),
-        name="ffn",
+        name=name,
     )(*xs, w_gate, w_up, w_down)
 
 
@@ -348,37 +343,30 @@
     )(before, one, two, three, kept, qd, gate, gain)
 
 
-def project_kernel(rows_ref, w_ref, out_ref, acc):
-    s = pl.program_id(0)
-    part = mm(rows_ref[...], w_ref[...])
-
-    @pl.when(s == 0)
-    def _():
-        acc[...] = part
-
-    @pl.when(s > 0)
-    def _():
-        acc[...] = acc[...] + part
-
-    @pl.when(s == pl.num_programs(0) - 1)
-    def _():
-        out_ref[...] = acc[...].astype(bf16)
+def project_kernel(rows_ref, w_ref, out_ref):
+    parts = w_ref.shape[0] // HEAD_DIM
+    rows = rows_ref.shape[0] // parts
+    total = None
+    for s in range(parts):
+        at = s * HEAD_DIM
+        part = mm(rows_ref[s * rows : (s + 1) * rows, :], w_ref[at : at + HEAD_DIM, :])
+        total = part if total is None else total + part
+    out_ref[...] = total.astype(bf16)
 
 
 def project(pieces, w_out):
-    parts = 8
-    rows = pieces.shape[0] // parts
-    width = w_out.shape[1]
+    whole, width = w_out.shape
+    rows = pieces.shape[0] * HEAD_DIM // whole
+    cols = 256
     return pl.pallas_call(
         project_kernel,
-        grid=(parts,),
+        grid=(width // cols,),
         out_shape=jax.ShapeDtypeStruct((rows, width), bf16),
         in_specs=[
-            pl.BlockSpec((rows, HEAD_DIM), lambda s: (s, 0)),
-            pl.BlockSpec((HEAD_DIM, width), lambda s: (s, 0)),
+            pl.BlockSpec(pieces.shape, lambda n: (0, 0)),
+            pl.BlockSpec((whole, cols), lambda n: (0, n)),
         ],
-        out_specs=pl.BlockSpec((rows, width), lambda s: (0, 0)),
-        scratch_shapes=[pltpu.VMEM((rows, width), f32)],
+        out_specs=pl.BlockSpec((rows, cols), lambda n: (0, n)),
         compiler_params=pltpu.CompilerParams(dimension_semantics=("arbitrary",)),
         cost_estimate=pl.CostEstimate(
             flops=4 * 10**9, bytes_accessed=10 * 2**20, transcendentals=0
@@ -415,12 +403,13 @@
     ep = ("z", "x")
     tp = ("y", "core")
 
+    ids = route_ids.T
     outgoing = pl.pallas_call(
         pre_kernel,
         out_shape=jax.ShapeDtypeStruct((SLOTS, width), bf16),
         cost_estimate=pl.CostEstimate(flops=2 * 10**9, bytes_accessed=10**6, transcendentals=0),
         name="pre",
-    )(moe_in, route_ids, moe_gain.reshape(1, -1))
+    )(moe_in, ids, moe_gain.reshape(1, -1))
     own = lax.all_to_all(outgoing, ep, split_axis=0, concat_axis=0, tiled=True)
 
     cos_t, sin_t = angle_tables()
@@ -430,7 +419,7 @@
     base = jnp.stack([jnp.cos(angle), jnp.sin(angle)], axis=1)
     kept, qd, end = local_part(
         base,
-        mix_query,
+        after(mix_query, outgoing),
         mix_key,
         mix_value,
         log_decay.reshape(blocks, 1, BLOCK),
@@ -438,29 +427,37 @@
         jnp.asarray(sin_t),
     )
     by_x = [shift(end, "x", s) for s in (1, 2, 3)]
+    own = after(own, end)
+
+    own_c = shift(own, "core", 1, 2)
+    up = shift(own, "y", 1)
+    down = shift(own, "y", -1)
+    far = shift(own, "y", 2)
     x_index = lax.axis_index("x").astype(jnp.int32).reshape(1)
     before, whole = middle(x_index, end, *by_x)
     by_z = [shift(whole, "z", s, wrap=False) for s in (1, 2, 3)]
-    heads_out = finish(before, *by_z, kept, qd, mix_gate, ret_gain.reshape(1, -1))
+    weights = (w_gate[0], w_up[0], w_down[0])
+    keep0, give0 = ffn("ffn0", [after(own, whole), own_c], *weights, 2)
+    got0 = shift(give0, "core", 1, 2)
+    heads_out = finish(
+        after(before, keep0), *by_z, kept, qd, mix_gate, ret_gain.reshape(1, -1)
+    )
     pieces = lax.all_to_all(heads_out, tp, split_axis=0, concat_axis=0, tiled=True)
 
-    half = own.shape[0] // 2
-    up1 = shift(own, "y", 1)
-    down1 = shift(own, "y", -1)
-    far = jnp.concatenate([shift(up1[:half], "y", 1), shift(down1[half:], "y", -1)], axis=0)
-    mine = [own, up1, down1, far]
-    other = [shift(v, "core", 1, 2) for v in mine]
-    keep, give = ffn(mine + other, w_gate[0], w_up[0], w_down[0], 2)
-    got = shift(give, "core", 1, 2)
-    sums = (keep.astype(f32) + got.astype(f32)).astype(bf16)
+    up_c = shift(up, "core", 1, 2)
+    down_c = shift(down, "core", 1, 2)
+    keep1, give1 = ffn("ffn1", [after(up, heads_out), down, up_c, down_c], *weights, 2)
+    got1 = shift(give1, "core", 1, 2)
+    far_c = shift(far, "core", 1, 2)
+    near = (keep1.astype(f32) + got1.astype(f32)).astype(bf16)
     n = own.shape[0]
-    back = [
-        sums[:n],
-        shift(sums[n : 2 * n], "y", -1),
-        shift(sums[2 * n : 3 * n], "y", 1),
-        shift(sums[3 * n :], "y", 2),
-    ]
-    expert_rows = sum(v.astype(f32) for v in back).astype(bf16)
+    back_up = shift(near[:n], "y", -1)
+    back_down = shift(near[n:], "y", 1)
+    keep2, give2 = ffn("ffn2", [after(far, near, pieces), far_c], *weights, 2)
+    got2 = shift(give2, "core", 1, 2)
+    back_far = shift((keep2.astype(f32) + got2.astype(f32)).astype(bf16), "y", 2)
+    parts = (keep0, got0, back_up, back_down, back_far)
+    expert_rows = sum(v.astype(f32) for v in parts).astype(bf16)
     returned = lax.all_to_all(expert_rows, ep, split_axis=0, concat_axis=0, tiled=True)
     mix_out = project(pieces, w_out)
     moe_out = pl.pallas_call(
@@ -468,7 +465,7 @@
         out_shape=jax.ShapeDtypeStruct(moe_in.shape, bf16),
         cost_estimate=pl.CostEstimate(flops=10**9, bytes_accessed=10**6, transcendentals=0),
         name="combine",
-    )(returned, route_ids, route_weights)
+    )(returned, ids, route_weights.T)
     return (mix_out, moe_out)
 
 

time: 160 us -> 161 us (level)
  blocking collectives: 19.5 us -> 0 us
  waiting for transfers between devices: 45.6 us -> 61.2 us
  Pallas kernels: 46.8 us -> 54.7 us
  local copies, waits for them, and re-layouts: 7.79 us -> 3.16 us
  starting transfers between devices: 32.4 us -> 35.4 us
    all_to_all x1 -> x0, blocking collectives: 19.5 us -> none  [on_device(): own = lax.all_to_all(outgoing, ep, split_axis=0, concat_axis=0, tiled=True)]
    all_to_all x0 -> x1, starting transfers between devices: none -> 7.99 us  [on_device(): own = lax.all_to_all(outgoing, ep, split_axis=0, concat_axis=0, tiled=True)]
    pallas_call x2 -> x4, Pallas kernels: 28.4 us -> 36.4 us  [the longest x3 27.7 us: ffn(): pl.pallas_call(functools.partial(ffn_kernel, n_x, tile, groups), out_shap...]
    ppermute x18 -> x19, waiting for transfers between devices: 39.8 us -> 46.7 us  [shift(): return lax.ppermute(x, axis, pairs)]
    all_to_all x0 -> x1, waiting for transfers between devices: none -> 4.19 us  [on_device(): own = lax.all_to_all(outgoing, ep, split_axis=0, concat_axis=0, tiled=True)]
    unnamed x41 -> x34, local copies, waits for them, and re-layouts: 6.46 us -> 3 us
    ppermute x18 -> x19, starting transfers between devices: 23.7 us -> 20.3 us  [shift(): return lax.ppermute(x, axis, pairs)]
    all_to_all x1, waiting for transfers between devices: 5.84 us -> 8.89 us  [on_device(): lax.all_to_all(heads_out, tp, split_axis=0, concat_axis=0, tiled=True)]
  transfers between devices with their start and end apart: 20 -> 22, of which waited for: 8 -> 8; matrix products, arithmetic and copies ran while one was open for 5% -> 2% of each run, Pallas kernels for 15% -> 19%
where the time goes in v2:
time: 161 us; the launch traced here: 160 us
  waiting for transfers between devices  61.2 us (38%)
  Pallas kernels  54.7 us (34%)
  starting transfers between devices  35.4 us (22%)
  other arithmetic  4.77 us (3%)
  local copies, waits for them, and re-layouts  3.16 us (2%)
    ppermute x19, waiting for transfers between devices, shift(): return lax.ppermute(x, axis, pairs)  46.7 us
    pallas_call x3, Pallas kernels, ffn(): pl.pallas_call(functools.partial(ffn_kernel, n_x, tile, groups), out_shap...  27.7 us
    ppermute x19, starting transfers between devices, shift(): return lax.ppermute(x, axis, pairs)  20.3 us
    all_to_all x1, waiting for transfers between devices, on_device(): lax.all_to_all(heads_out, tp, split_axis=0, concat_axis=0, tiled=True)  8.89 us
    pallas_call x1, Pallas kernels, project(): pl.pallas_call(project_kernel, grid=(width // cols,), out_shape=jax.Shape...  8.67 us
    all_to_all x1, starting transfers between devices, on_device(): own = lax.all_to_all(outgoing, ep, split_axis=0, concat_axis=0, tiled=True)  7.99 us
    pallas_call x1, Pallas kernels, local_part(): pl.pallas_call(local_kernel, grid=(blocks,), out_shape=[jax.ShapeDtypeStr...  6.56 us
    pallas_call x1, Pallas kernels, finish(): pl.pallas_call(finish_kernel, grid=(rows // BLOCK,), out_shape=jax.ShapeD...  5.06 us
  transfers between devices with their start and end apart: 22, of which 8 were waited for; matrix products, arithmetic and copies ran while one was open for 2% of the time, Pallas kernels for 19%

profile of v2, /device:TPU:0, one launch (start us, length us, event | category | flops | bytes accessed | tf_op | source)
XLA Modules:
  0.0 160.1 jit_solution(3509831273986880818)
XLA Ops:
  0.6 2.3 %pre.1 = bf16[128,2048]{1,0:T(8,128)(2,1)} custom-call(bf16[32,2048]{1,0:T(8,128)(2,1)} %x_ref.1, s32[2,32]{1,0:T(2,128)} %bitcast.39, f32[1,2048]{1,0:T(1,128)} %bitcast.36), custom_call_target="tpu_custom_call" | custom-call | flops 2000000000 | bytes 1000000 | tf_op jit(solution)/shard_map/pre/pallas_call | solution.py:407
  2.9 8.0 %all-to-all-start = ((bf16[16,8,2048]{2,1,0:T(8,128)(2,1)}), bf16[16,8,2048]{2,1,0:T(8,128)(2,1)S(1)}, u32[]{:S(2)}, u32[]{:S(2)}) async-start(bf16[16,8,2048]{2,1,0:T(8,128)(2,1)} %bitcast.33), calls=%async_computation | async-start | bytes 1048576 | tf_op jit(solution)/shard_map/all_to_all | solution.py:413
  10.9 0.1 mul.40
  11.0 0.1 multiply_cosine_fusion
  11.1 0.6 pad_maximum_fusion.base_ref
  11.7 6.6 %local.1 = (f32[2048,256]{1,0:T(8,128)}, bf16[2048,256]{1,0:T(8,128)(2,1)}, bf16[264,256]{1,0:T(8,128)(2,1)}) custom-call(f32[4,2,128]{2,1,0:T(2,128)} %pad_maximum_fusion.base_ref, bf16[2048,256]{1,0:T(8,128)(2,1)} %q_ref, bf16[2048,256]{1,0:T(8,128)(2,1)} %k_ref.1, bf16[2048,256]{1,0:T(8,128)(2,1)} %v_ref.1, f32[4,1,512]{2,1,0:T(1,128)} %bitcast.37, ...), custom_call_target="tpu_custom_call" | custom-call | flops 6000000000 | bytes 6291456 | tf_op jit(solution)/shard_map/local/pallas_call | solution.py:240
  18.2 4.2 %all-to-all-done = bf16[16,8,2048]{2,1,0:T(8,128)(2,1)S(1)} async-done(((bf16[16,8,2048]{2,1,0:T(8,128)(2,1)}), bf16[16,8,2048]{2,1,0:T(8,128)(2,1)S(1)}, u32[]{:S(2)}, u32[]{:S(2)}) %all-to-all-start) | async-done | bytes 524320 | tf_op jit(solution)/shard_map/all_to_all | solution.py:413
  22.4 1.6 collective-permute-start.8
  24.0 1.7 %collective-permute-start.9 = (bf16[128,2048]{1,0:T(8,128)(2,1)S(1)}, bf16[128,2048]{1,0:T(8,128)(2,1)S(1)}, u32[]{:S(2)}, u32[]{:S(2)}) collective-permute-start(bf16[128,2048]{1,0:T(8,128)(2,1)S(1)} %bitcast.27), channel_id=1, source_target_pairs={{0,6},{2,0},{4,2},{6,4},{1,7},{3,1},{5,3},{7,5},{8,14},{10,8},{12,... | collective-permute-start | bytes 1572872 | tf_op jit(solution)/shard_map/ppermute | solution.py:33
  25.7 0.6 collective-permute-start
  26.2 1.4 collective-permute-start.1
  27.7 8.3 %collective-permute-done.one_ref = bf16[264,256]{1,0:T(8,128)(2,1)S(1)} collective-permute-done((bf16[264,256]{1,0:T(8,128)(2,1)}, bf16[264,256]{1,0:T(8,128)(2,1)S(1)}, u32[]{:S(2)}, u32[]{:S(2)}) %collective-permute-start) | collective-permute-done | bytes 135200 | tf_op jit(solution)/shard_map/ppermute | solution.py:33
  36.0 0.1 collective-permute-start.10
  36.1 0.5 collective-permute-start.11
  36.6 4.7 %collective-permute-done.2.three_ref = bf16[264,256]{1,0:T(8,128)(2,1)S(1)} collective-permute-done((bf16[264,256]{1,0:T(8,128)(2,1)}, bf16[264,256]{1,0:T(8,128)(2,1)S(1)}, u32[]{:S(2)}, u32[]{:S(2)}) %collective-permute-start.2) | collective-permute-done | bytes 135200 | tf_op jit(solution)/shard_map/ppermute | solution.py:33
  41.4 0.6 copy-done.15
  42.0 2.1 %middle.1 = (f32[264,256]{1,0:T(8,128)}, bf16[264,256]{1,0:T(8,128)(2,1)}) custom-call(s32[1]{0:T(128)} %bitcast.x_ref, bf16[264,256]{1,0:T(8,128)(2,1)} %get-tuple-element.20.own_ref, bf16[264,256]{1,0:T(8,128)(2,1)} %copy-done.11, bf16[264,256]{1,0:T(8,128)(2,1)} %copy-done.12, bf16[264,256]{1,0:T(8,128)(2,1)} %copy-done.15), custom_call_target="tpu_custom_call" | custom-call | flops 500000000 | bytes 1000000 | tf_op jit(solution)/shard_map/middle/pallas_call | solution.py:293
  44.2 1.3 collective-permute-start.4
  45.4 4.8 %collective-permute-start.5 = (bf16[264,256]{1,0:T(8,128)(2,1)}, bf16[264,256]{1,0:T(8,128)(2,1)S(1)}, u32[]{:S(2)}, u32[]{:S(2)}) collective-permute-start(bf16[264,256]{1,0:T(8,128)(2,1)} %get-tuple-element.23), channel_id=1, source_target_pairs={{0,64},{32,96},{1,65},{33,97},{2,66},{34,98},{3,67},{35,99},{4,68}... | collective-permute-start | bytes 405512 | tf_op jit(solution)/shard_map/ppermute | solution.py:33
  50.3 1.5 collective-permute-start.6
  51.8 8.5 %ffn0.1 = (bf16[128,2048]{1,0:T(8,128)(2,1)}, bf16[128,2048]{1,0:T(8,128)(2,1)}) custom-call(bf16[128,2048]{1,0:T(8,128)(2,1)} %bitcast.29, bf16[128,2048]{1,0:T(8,128)(2,1)} %copy-done.3, bf16[2048,896]{1,0:T(8,128)(2,1)} %bitcast.17, bf16[2048,896]{1,0:T(8,128)(2,1)} %bitcast.20, bf16[896,2048]{1,0:T(8,128)(2,1)} %bitcast.23), custom_call_target="tpu_custom_call" | custom-call | flops 2818572288 | bytes 13107200 | tf_op jit(solution)/shard_map/ffn0/pallas_call | solution.py:141
  60.4 0.6 copy-done.13
  61.0 0.0 copy-done.14
  61.1 5.1 %finish.1 = bf16[2048,256]{1,0:T(8,128)(2,1)} custom-call(f32[264,256]{1,0:T(8,128)} %get-tuple-element.26.before_ref, bf16[264,256]{1,0:T(8,128)(2,1)} %copy-done.13, bf16[264,256]{1,0:T(8,128)(2,1)} %copy-done.14, bf16[264,256]{1,0:T(8,128)(2,1)} %copy-done.16, f32[2048,256]{1,0:T(8,128)} %get-tuple-element.27.kept_ref, ...), custom_call_target="tpu_custom_call" | custom-call | flops 2000000000 | bytes 5242880 | tf_op jit(solution)/shard_map/finish/pallas_call | solution.py:331
  66.2 0.8 copy-done.10
  67.0 10.3 %ffn1.1 = (bf16[256,2048]{1,0:T(8,128)(2,1)}, bf16[256,2048]{1,0:T(8,128)(2,1)}) custom-call(bf16[128,2048]{1,0:T(8,128)(2,1)} %copy-done.8, bf16[128,2048]{1,0:T(8,128)(2,1)} %copy-done.9, bf16[128,2048]{1,0:T(8,128)(2,1)} %copy-done.10, bf16[128,2048]{1,0:T(8,128)(2,1)} %collective-permute-done.11.refs_3_, bf16[2048,896]{1,0:T(8,128)(2,1)} %bitcast.18, ...), custom_call_target="tpu_custom_call" | custom-call | flops 5637144576 | bytes 15204352 | tf_op jit(solution)/shard_map/ffn1/pallas_call | solution.py:141
  77.3 0.1 collective-permute-start.12
  77.4 2.1 %collective-permute-start.15 = (bf16[128,2048]{1,0:T(8,128)(2,1)S(1)}, bf16[128,2048]{1,0:T(8,128)(2,1)}, u32[]{:S(2)}, u32[]{:S(2)}) collective-permute-start(bf16[128,2048]{1,0:T(8,128)(2,1)S(1)} %bitcast.30), channel_id=1, source_target_pairs={{0,4},{2,6},{4,0},{6,2},{1,5},{3,7},{5,1},{7,3},{8,12},{10,14},{12... | collective-permute-start | bytes 1572872 | tf_op jit(solution)/shard_map/ppermute | solution.py:33
  79.4 3.6 %all-to-all-start.1 = ((bf16[8,256,256]{2,1,0:T(8,128)(2,1)}), bf16[8,256,256]{2,1,0:T(8,128)(2,1)S(1)}, u32[]{:S(2)}, u32[]{:S(2)}) async-start(bf16[8,256,256]{2,1,0:T(8,128)(2,1)} %bitcast.32), calls=%async_computation.1 | async-start | bytes 2097152 | tf_op jit(solution)/shard_map/all_to_all | solution.py:445
  83.0 11.0 %collective-permute-done.15.refs_0_ = bf16[128,2048]{1,0:T(8,128)(2,1)} collective-permute-done((bf16[128,2048]{1,0:T(8,128)(2,1)S(1)}, bf16[128,2048]{1,0:T(8,128)(2,1)}, u32[]{:S(2)}, u32[]{:S(2)}) %collective-permute-start.15) | collective-permute-done | bytes 524320 | tf_op jit(solution)/shard_map/ppermute | solution.py:33
  94.0 1.6 %add_convert_fusion = bf16[256,2048]{1,0:T(8,128)(2,1)S(1)} fusion(bf16[256,2048]{1,0:T(8,128)(2,1)S(1)} %collective-permute-done.12, bf16[256,2048]{1,0:T(8,128)(2,1)} %get-tuple-element.31), kind=kLoop, calls=%fused_computation | loop fusion | flops 2097152 | bytes 3145728 | tf_op jit(solution)/shard_map/convert_element_type | solution.py:452
  95.6 8.9 %all-to-all-done.1 = bf16[8,256,256]{2,1,0:T(8,128)(2,1)S(1)} async-done(((bf16[8,256,256]{2,1,0:T(8,128)(2,1)}), bf16[8,256,256]{2,1,0:T(8,128)(2,1)S(1)}, u32[]{:S(2)}, u32[]{:S(2)}) %all-to-all-start.1) | async-done | bytes 1048608 | tf_op jit(solution)/shard_map/all_to_all | solution.py:445
  104.5 8.9 %ffn2.1 = (bf16[128,2048]{1,0:T(8,128)(2,1)}, bf16[128,2048]{1,0:T(8,128)(2,1)}) custom-call(bf16[128,2048]{1,0:T(8,128)(2,1)} %collective-permute-done.15.refs_0_, bf16[128,2048]{1,0:T(8,128)(2,1)} %collective-permute-done.16.refs_1_, bf16[2048,896]{1,0:T(8,128)(2,1)} %bitcast.19, bf16[2048,896]{1,0:T(8,128)(2,1)} %bitcast.22, bf16[896,2048]{1,0:T(8,128)(2,1)} %bitcast.25), custom_call_target="tpu_custom_call" | custom-call | flops 2818572288 | bytes 13107200 | tf_op jit(solution)/shard_map/ffn2/pallas_call | solution.py:141
  113.4 0.1 collective-permute-start.17
  113.5 0.5 collective-permute-start.7
  114.0 0.1 fusion.1
  114.1 1.9 %collective-permute-start.13 = (bf16[128,2048]{1,0:T(8,128)(2,1)S(1)}, bf16[128,2048]{1,0:T(8,128)(2,1)S(1)}, u32[]{:S(2)}, u32[]{:S(2)}) collective-permute-start(bf16[128,2048]{1,0:T(8,128)(2,1)S(1)} %get-tuple-element.36), channel_id=1, source_target_pairs={{0,6},{2,0},{4,2},{6,4},{1,7},{3,1},{5,3},{7,5},{8,14},{10,8},{12,... | collective-permute-start | bytes 1572872 | tf_op jit(solution)/shard_map/ppermute | solution.py:33
  116.0 0.2 collective-permute-start.14
  116.2 1.2 add_convert_fusion.2
  117.4 2.1 %collective-permute-start.18 = (bf16[128,2048]{1,0:T(8,128)(2,1)S(1)}, bf16[128,2048]{1,0:T(8,128)(2,1)S(1)}, u32[]{:S(2)}, u32[]{:S(2)}) collective-permute-start(bf16[128,2048]{1,0:T(8,128)(2,1)S(1)} %add_convert_fusion.2), channel_id=1, source_target_pairs={{0,4},{2,6},{4,0},{6,2},{1,5},{3,7},{5,1},{7,3},{8,12},{10,14},{12... | collective-permute-start | bytes 1572872 | tf_op jit(solution)/shard_map/ppermute | solution.py:33
  119.5 19.2 %collective-permute-done.13 = bf16[128,2048]{1,0:T(8,128)(2,1)S(1)} collective-permute-done((bf16[128,2048]{1,0:T(8,128)(2,1)S(1)}, bf16[128,2048]{1,0:T(8,128)(2,1)S(1)}, u32[]{:S(2)}, u32[]{:S(2)}) %collective-permute-start.13) | collective-permute-done | bytes 524320 | tf_op jit(solution)/shard_map/ppermute | solution.py:33
  138.7 3.4 %collective-permute-done.14 = bf16[128,2048]{1,0:T(8,128)(2,1)S(1)} collective-permute-done((bf16[128,2048]{1,0:T(8,128)(2,1)S(1)}, bf16[128,2048]{1,0:T(8,128)(2,1)S(1)}, u32[]{:S(2)}, u32[]{:S(2)}) %collective-permute-start.14) | collective-permute-done | bytes 524320 | tf_op jit(solution)/shard_map/ppermute | solution.py:33
  142.1 1.3 fusion
  143.4 3.6 %all-to-all-start.2 = ((bf16[16,8,2048]{2,1,0:T(8,128)(2,1)}), bf16[16,8,2048]{2,1,0:T(8,128)(2,1)S(1)}, u32[]{:S(2)}, u32[]{:S(2)}) async-start(bf16[16,8,2048]{2,1,0:T(8,128)(2,1)} %fusion), calls=%async_computation.2 | async-start | bytes 1048576 | tf_op jit(solution)/shard_map/all_to_all | solution.py:461
  147.0 8.7 %project.1 = bf16[256,2048]{1,0:T(8,128)(2,1)} custom-call(bf16[2048,256]{1,0:T(8,128)(2,1)} %bitcast.31, bf16[2048,2048]{1,0:T(8,128)(2,1)} %w_ref.1), custom_call_target="tpu_custom_call" | custom-call | flops 4000000000 | bytes 10485760 | tf_op jit(solution)/shard_map/project/pallas_call | solution.py:361
  155.7 1.4 all-to-all-done.2
  157.0 0.8 copy-done.4
  157.8 2.3 %combine.1 = bf16[32,2048]{1,0:T(8,128)(2,1)} custom-call(bf16[128,2048]{1,0:T(8,128)(2,1)} %bitcast.34, s32[2,32]{1,0:T(2,128)} %bitcast.40, f32[2,32]{1,0:T(2,128)} %bitcast.41), custom_call_target="tpu_custom_call" | custom-call | flops 1000000000 | bytes 1000000 | tf_op jit(solution)/shard_map/combine/pallas_call | solution.py:463
  (47 shorter events, 0.1 us)
Async XLA Ops:
  0.6 10.4 %copy-start.6 = (f32[128]{0:T(128)S(1)}, f32[128]{0:T(128)}, u32[]{:S(2)}) copy-start(f32[128]{0:T(128)} %constant.21.clone) | copy-start | bytes 1540
  2.9 19.5 %all-to-all-start = ((bf16[16,8,2048]{2,1,0:T(8,128)(2,1)}), bf16[16,8,2048]{2,1,0:T(8,128)(2,1)S(1)}, u32[]{:S(2)}, u32[]{:S(2)}) async-start(bf16[16,8,2048]{2,1,0:T(8,128)(2,1)} %bitcast.33), calls=%async_computation | async-start | bytes 1048576 | tf_op jit(solution)/shard_map/all_to_all | solution.py:413
  22.4 29.4 %copy-start = (bf16[16,8,2048]{2,1,0:T(8,128)(2,1)}, bf16[16,8,2048]{2,1,0:T(8,128)(2,1)S(1)}, u32[]{:S(2)}) copy-start(bf16[16,8,2048]{2,1,0:T(8,128)(2,1)S(1)} %all-to-all-done) | copy-start | bytes 1572868
  22.4 13.6 %collective-permute-start.8 = (bf16[128,2048]{1,0:T(8,128)(2,1)S(1)}, bf16[128,2048]{1,0:T(8,128)(2,1)S(1)}, u32[]{:S(2)}, u32[]{:S(2)}) collective-permute-start(bf16[128,2048]{1,0:T(8,128)(2,1)S(1)} %bitcast.26), channel_id=1, source_target_pairs={{0,2},{2,4},{4,6},{6,0},{1,3},{3,5},{5,7},{7,1},{8,10},{10,12},{12... | collective-permute-start | bytes 1572872 | tf_op jit(solution)/shard_map/ppermute | solution.py:33
  24.0 12.1 %collective-permute-start.9 = (bf16[128,2048]{1,0:T(8,128)(2,1)S(1)}, bf16[128,2048]{1,0:T(8,128)(2,1)S(1)}, u32[]{:S(2)}, u32[]{:S(2)}) collective-permute-start(bf16[128,2048]{1,0:T(8,128)(2,1)S(1)} %bitcast.27), channel_id=1, source_target_pairs={{0,6},{2,0},{4,2},{6,4},{1,7},{3,1},{5,3},{7,5},{8,14},{10,8},{12,... | collective-permute-start | bytes 1572872 | tf_op jit(solution)/shard_map/ppermute | solution.py:33
  25.7 24.6 %collective-permute-start.3 = (bf16[128,2048]{1,0:T(8,128)(2,1)S(1)}, bf16[128,2048]{1,0:T(8,128)(2,1)S(1)}, u32[]{:S(2)}, u32[]{:S(2)}) collective-permute-start(bf16[128,2048]{1,0:T(8,128)(2,1)S(1)} %bitcast.28), channel_id=1, source_target_pairs={{0,1},{1,0},{2,3},{3,2},{4,5},{5,4},{6,7},{7,6},{8,9},{9,8},{10,11... | collective-permute-start | bytes 1572872 | tf_op jit(solution)/shard_map/ppermute | solution.py:33
  25.7 10.3 %collective-permute-start = (bf16[264,256]{1,0:T(8,128)(2,1)}, bf16[264,256]{1,0:T(8,128)(2,1)S(1)}, u32[]{:S(2)}, u32[]{:S(2)}) collective-permute-start(bf16[264,256]{1,0:T(8,128)(2,1)} %get-tuple-element.20.own_ref), channel_id=1, source_target_pairs={{0,8},{8,16},{16,24},{24,0},{1,9},{9,17},{17,25},{25,1},{2,10},{10... | collective-permute-start | bytes 405512 | tf_op jit(solution)/shard_map/ppermute | solution.py:33
  26.2 10.4 %collective-permute-start.1 = (bf16[264,256]{1,0:T(8,128)(2,1)}, bf16[264,256]{1,0:T(8,128)(2,1)S(1)}, u32[]{:S(2)}, u32[]{:S(2)}) collective-permute-start(bf16[264,256]{1,0:T(8,128)(2,1)} %get-tuple-element.20.own_ref), channel_id=1, source_target_pairs={{0,16},{8,24},{16,0},{24,8},{1,17},{9,25},{17,1},{25,9},{2,18},{10... | collective-permute-start | bytes 405512 | tf_op jit(solution)/shard_map/ppermute | solution.py:33
  36.0 5.4 %copy-start.11 = (bf16[264,256]{1,0:T(8,128)(2,1)}, bf16[264,256]{1,0:T(8,128)(2,1)S(1)}, u32[]{:S(2)}) copy-start(bf16[264,256]{1,0:T(8,128)(2,1)S(1)} %collective-permute-done.one_ref) | copy-start | bytes 405508
  36.0 5.3 %collective-permute-start.2 = (bf16[264,256]{1,0:T(8,128)(2,1)}, bf16[264,256]{1,0:T(8,128)(2,1)S(1)}, u32[]{:S(2)}, u32[]{:S(2)}) collective-permute-start(bf16[264,256]{1,0:T(8,128)(2,1)} %get-tuple-element.20.own_ref), channel_id=1, source_target_pairs={{0,24},{8,0},{16,8},{24,16},{1,25},{9,1},{17,9},{25,17},{2,26},{10... | collective-permute-start | bytes 405512 | tf_op jit(solution)/shard_map/ppermute | solution.py:33
  36.0 24.3 %copy-start.8 = (bf16[128,2048]{1,0:T(8,128)(2,1)}, bf16[128,2048]{1,0:T(8,128)(2,1)S(1)}, u32[]{:S(2)}) copy-start(bf16[128,2048]{1,0:T(8,128)(2,1)S(1)} %collective-permute-done.8.refs_0_) | copy-start | bytes 1572868
  36.0 30.1 %collective-permute-start.10 = (bf16[128,2048]{1,0:T(8,128)(2,1)S(1)}, bf16[128,2048]{1,0:T(8,128)(2,1)S(1)}, u32[]{:S(2)}, u32[]{:S(2)}) collective-permute-start(bf16[128,2048]{1,0:T(8,128)(2,1)S(1)} %collective-permute-done.8.refs_0_), channel_id=1, source_target_pairs={{0,1},{1,0},{2,3},{3,2},{4,5},{5,4},{6,7},{7,6},{8,9},{9,8},{10,11... | collective-permute-start | bytes 1572872 | tf_op jit(solution)/shard_map/ppermute | solution.py:33
  36.1 24.2 %copy-start.9 = (bf16[128,2048]{1,0:T(8,128)(2,1)}, bf16[128,2048]{1,0:T(8,128)(2,1)S(1)}, u32[]{:S(2)}) copy-start(bf16[128,2048]{1,0:T(8,128)(2,1)S(1)} %collective-permute-done.9.refs_1_) | copy-start | bytes 1572868
  36.1 30.1 %collective-permute-start.11 = (bf16[128,2048]{1,0:T(8,128)(2,1)S(1)}, bf16[128,2048]{1,0:T(8,128)(2,1)}, u32[]{:S(2)}, u32[]{:S(2)}) collective-permute-start(bf16[128,2048]{1,0:T(8,128)(2,1)S(1)} %collective-permute-done.9.refs_1_), channel_id=1, source_target_pairs={{0,1},{1,0},{2,3},{3,2},{4,5},{5,4},{6,7},{7,6},{8,9},{9,8},{10,11... | collective-permute-start | bytes 1572872 | tf_op jit(solution)/shard_map/ppermute | solution.py:33
  36.6 4.7 %copy-start.12 = (bf16[264,256]{1,0:T(8,128)(2,1)}, bf16[264,256]{1,0:T(8,128)(2,1)S(1)}, u32[]{:S(2)}) copy-start(bf16[264,256]{1,0:T(8,128)(2,1)S(1)} %collective-permute-done.1.two_ref) | copy-start | bytes 405508
  41.3 0.7 copy-start.15
  44.2 16.2 %collective-permute-start.4 = (bf16[264,256]{1,0:T(8,128)(2,1)}, bf16[264,256]{1,0:T(8,128)(2,1)S(1)}, u32[]{:S(2)}, u32[]{:S(2)}) collective-permute-start(bf16[264,256]{1,0:T(8,128)(2,1)} %get-tuple-element.23), channel_id=1, source_target_pairs={{0,32},{32,64},{64,96},{1,33},{33,65},{65,97},{2,34},{34,66},{66,9... | collective-permute-start | bytes 405512 | tf_op jit(solution)/shard_map/ppermute | solution.py:33
  45.4 14.9 %collective-permute-start.5 = (bf16[264,256]{1,0:T(8,128)(2,1)}, bf16[264,256]{1,0:T(8,128)(2,1)S(1)}, u32[]{:S(2)}, u32[]{:S(2)}) collective-permute-start(bf16[264,256]{1,0:T(8,128)(2,1)} %get-tuple-element.23), channel_id=1, source_target_pairs={{0,64},{32,96},{1,65},{33,97},{2,66},{34,98},{3,67},{35,99},{4,68}... | collective-permute-start | bytes 405512 | tf_op jit(solution)/shard_map/ppermute | solution.py:33
  50.3 1.5 copy-start.3
  50.3 10.1 %collective-permute-start.6 = (bf16[264,256]{1,0:T(8,128)(2,1)}, bf16[264,256]{1,0:T(8,128)(2,1)S(1)}, u32[]{:S(2)}, u32[]{:S(2)}) collective-permute-start(bf16[264,256]{1,0:T(8,128)(2,1)} %get-tuple-element.23), channel_id=1, source_target_pairs={{0,96},{1,97},{2,98},{3,99},{4,100},{5,101},{6,102},{7,103},{8,104... | collective-permute-start | bytes 405512 | tf_op jit(solution)/shard_map/ppermute | solution.py:33
  60.4 0.7 copy-start.13
  60.4 0.7 copy-start.14
  60.4 0.7 copy-start.16
  66.2 11.2 %copy-start.1 = (bf16[16,8,2048]{2,1,0:T(8,128)(2,1)S(1)}, bf16[16,8,2048]{2,1,0:T(8,128)(2,1)}, u32[]{:S(2)}) copy-start(bf16[16,8,2048]{2,1,0:T(8,128)(2,1)} %copy-done) | copy-start | bytes 1572868
  66.2 0.8 copy-start.10
  77.3 16.7 %collective-permute-start.12 = (bf16[256,2048]{1,0:T(8,128)(2,1)}, bf16[256,2048]{1,0:T(8,128)(2,1)S(1)}, u32[]{:S(2)}, u32[]{:S(2)}) collective-permute-start(bf16[256,2048]{1,0:T(8,128)(2,1)} %get-tuple-element.32), channel_id=1, source_target_pairs={{0,1},{1,0},{2,3},{3,2},{4,5},{5,4},{6,7},{7,6},{8,9},{9,8},{10,11... | collective-permute-start | bytes 3145736 | tf_op jit(solution)/shard_map/ppermute | solution.py:33
  77.4 16.6 %collective-permute-start.15 = (bf16[128,2048]{1,0:T(8,128)(2,1)S(1)}, bf16[128,2048]{1,0:T(8,128)(2,1)}, u32[]{:S(2)}, u32[]{:S(2)}) collective-permute-start(bf16[128,2048]{1,0:T(8,128)(2,1)S(1)} %bitcast.30), channel_id=1, source_target_pairs={{0,4},{2,6},{4,0},{6,2},{1,5},{3,7},{5,1},{7,3},{8,12},{10,14},{12... | collective-permute-start | bytes 1572872 | tf_op jit(solution)/shard_map/ppermute | solution.py:33
  79.4 25.0 %all-to-all-start.1 = ((bf16[8,256,256]{2,1,0:T(8,128)(2,1)}), bf16[8,256,256]{2,1,0:T(8,128)(2,1)S(1)}, u32[]{:S(2)}, u32[]{:S(2)}) async-start(bf16[8,256,256]{2,1,0:T(8,128)(2,1)} %bitcast.32), calls=%async_computation.1 | async-start | bytes 2097152 | tf_op jit(solution)/shard_map/all_to_all | solution.py:445
  94.0 10.5 %collective-permute-start.16 = (bf16[128,2048]{1,0:T(8,128)(2,1)}, bf16[128,2048]{1,0:T(8,128)(2,1)}, u32[]{:S(2)}, u32[]{:S(2)}) collective-permute-start(bf16[128,2048]{1,0:T(8,128)(2,1)} %collective-permute-done.15.refs_0_), channel_id=1, source_target_pairs={{0,1},{1,0},{2,3},{3,2},{4,5},{5,4},{6,7},{7,6},{8,9},{9,8},{10,11... | collective-permute-start | bytes 1572872 | tf_op jit(solution)/shard_map/ppermute | solution.py:33
  104.5 8.9 %copy-start.2 = (bf16[8,256,256]{2,1,0:T(8,128)(2,1)}, bf16[8,256,256]{2,1,0:T(8,128)(2,1)S(1)}, u32[]{:S(2)}) copy-start(bf16[8,256,256]{2,1,0:T(8,128)(2,1)S(1)} %all-to-all-done.1) | copy-start | bytes 3145732
  104.5 9.0 %copy-start.7 = (bf16[128,2048]{1,0:T(8,128)(2,1)S(1)}, bf16[128,2048]{1,0:T(8,128)(2,1)}, u32[]{:S(2)}) copy-start(bf16[128,2048]{1,0:T(8,128)(2,1)} %get-tuple-element.29) | copy-start | bytes 1572868
  113.4 28.7 %copy-start.5 = (bf16[128,2048]{1,0:T(8,128)(2,1)S(1)}, bf16[128,2048]{1,0:T(8,128)(2,1)}, u32[]{:S(2)}) copy-start(bf16[128,2048]{1,0:T(8,128)(2,1)} %get-tuple-element.25) | copy-start | bytes 1572868
  113.4 2.8 %collective-permute-start.17 = (bf16[128,2048]{1,0:T(8,128)(2,1)}, bf16[128,2048]{1,0:T(8,128)(2,1)S(1)}, u32[]{:S(2)}, u32[]{:S(2)}) collective-permute-start(bf16[128,2048]{1,0:T(8,128)(2,1)} %get-tuple-element.35), channel_id=1, source_target_pairs={{0,1},{1,0},{2,3},{3,2},{4,5},{5,4},{6,7},{7,6},{8,9},{9,8},{10,11... | collective-permute-start | bytes 1572872 | tf_op jit(solution)/shard_map/ppermute | solution.py:33
  113.5 5.9 %collective-permute-start.7 = (bf16[128,2048]{1,0:T(8,128)(2,1)S(1)}, bf16[128,2048]{1,0:T(8,128)(2,1)S(1)}, u32[]{:S(2)}, u32[]{:S(2)}) collective-permute-start(bf16[128,2048]{1,0:T(8,128)(2,1)S(1)} %copy-done.7), channel_id=1, source_target_pairs={{0,1},{1,0},{2,3},{3,2},{4,5},{5,4},{6,7},{7,6},{8,9},{9,8},{10,11... | collective-permute-start | bytes 1572872 | tf_op jit(solution)/shard_map/ppermute | solution.py:33
  114.1 24.6 %collective-permute-start.13 = (bf16[128,2048]{1,0:T(8,128)(2,1)S(1)}, bf16[128,2048]{1,0:T(8,128)(2,1)S(1)}, u32[]{:S(2)}, u32[]{:S(2)}) collective-permute-start(bf16[128,2048]{1,0:T(8,128)(2,1)S(1)} %get-tuple-element.36), channel_id=1, source_target_pairs={{0,6},{2,0},{4,2},{6,4},{1,7},{3,1},{5,3},{7,5},{8,14},{10,8},{12,... | collective-permute-start | bytes 1572872 | tf_op jit(solution)/shard_map/ppermute | solution.py:33
  116.0 26.1 %collective-permute-start.14 = (bf16[128,2048]{1,0:T(8,128)(2,1)S(1)}, bf16[128,2048]{1,0:T(8,128)(2,1)S(1)}, u32[]{:S(2)}, u32[]{:S(2)}) collective-permute-start(bf16[128,2048]{1,0:T(8,128)(2,1)S(1)} %get-tuple-element.37), channel_id=1, source_target_pairs={{0,2},{2,4},{4,6},{6,0},{1,3},{3,5},{5,7},{7,1},{8,10},{10,12},{12... | collective-permute-start | bytes 1572872 | tf_op jit(solution)/shard_map/ppermute | solution.py:33
  117.4 24.7 %collective-permute-start.18 = (bf16[128,2048]{1,0:T(8,128)(2,1)S(1)}, bf16[128,2048]{1,0:T(8,128)(2,1)S(1)}, u32[]{:S(2)}, u32[]{:S(2)}) collective-permute-start(bf16[128,2048]{1,0:T(8,128)(2,1)S(1)} %add_convert_fusion.2), channel_id=1, source_target_pairs={{0,4},{2,6},{4,0},{6,2},{1,5},{3,7},{5,1},{7,3},{8,12},{10,14},{12... | collective-permute-start | bytes 1572872 | tf_op jit(solution)/shard_map/ppermute | solution.py:33
  143.4 13.6 %all-to-all-start.2 = ((bf16[16,8,2048]{2,1,0:T(8,128)(2,1)}), bf16[16,8,2048]{2,1,0:T(8,128)(2,1)S(1)}, u32[]{:S(2)}, u32[]{:S(2)}) async-start(bf16[16,8,2048]{2,1,0:T(8,128)(2,1)} %fusion), calls=%async_computation.2 | async-start | bytes 1048576 | tf_op jit(solution)/shard_map/all_to_all | solution.py:461
  157.0 0.8 copy-start.4

commit v3 on v2

--- a/solution.py
+++ b/solution.py
@@ -9,6 +9,7 @@
 from jax.sharding import Mesh
 from jax.sharding import PartitionSpec as P
 
+
 HEAD_DIM = 256
 HALF = HEAD_DIM // 2
 BLOCK = 512
@@ -16,6 +17,7 @@
 CAP = 8
 SLOTS = EXPERTS * CAP
 norm_eps = 1e-06
+
 
 f32 = jnp.float32
 bf16 = jnp.bfloat16
@@ -130,7 +132,7 @@
         c.wait()
 
 
-def ffn(name, xs, w_gate, w_up, w_down, n_out):
+def ffn(xs, w_gate, w_up, w_down, n_out):
     n_x = len(xs)
     tile, width = xs[0].shape
     ff = w_gate.shape[1]
@@ -159,7 +161,6 @@
             bytes_accessed=2 * (3 * width * ff + 2 * rows * width),
             transcendentals=rows * ff,
         ),
-        name=name,
     )(*xs, w_gate, w_up, w_down)
 
 
@@ -429,34 +430,31 @@
     by_x = [shift(end, "x", s) for s in (1, 2, 3)]
     own = after(own, end)
 
-    own_c = shift(own, "core", 1, 2)
     up = shift(own, "y", 1)
     down = shift(own, "y", -1)
     far = shift(own, "y", 2)
+    own_c = shift(own, "core", 1, 2)
     x_index = lax.axis_index("x").astype(jnp.int32).reshape(1)
     before, whole = middle(x_index, end, *by_x)
     by_z = [shift(whole, "z", s, wrap=False) for s in (1, 2, 3)]
-    weights = (w_gate[0], w_up[0], w_down[0])
-    keep0, give0 = ffn("ffn0", [after(own, whole), own_c], *weights, 2)
-    got0 = shift(give0, "core", 1, 2)
-    heads_out = finish(
-        after(before, keep0), *by_z, kept, qd, mix_gate, ret_gain.reshape(1, -1)
-    )
-    pieces = lax.all_to_all(heads_out, tp, split_axis=0, concat_axis=0, tiled=True)
-
     up_c = shift(up, "core", 1, 2)
     down_c = shift(down, "core", 1, 2)
-    keep1, give1 = ffn("ffn1", [after(up, heads_out), down, up_c, down_c], *weights, 2)
+    weights = (w_gate[0], w_up[0], w_down[0])
+    n = own.shape[0]
+    keep1, give1 = ffn([own, up, down, own_c, up_c, down_c], *weights, 2)
     got1 = shift(give1, "core", 1, 2)
     far_c = shift(far, "core", 1, 2)
     near = (keep1.astype(f32) + got1.astype(f32)).astype(bf16)
-    n = own.shape[0]
-    back_up = shift(near[:n], "y", -1)
-    back_down = shift(near[n:], "y", 1)
-    keep2, give2 = ffn("ffn2", [after(far, near, pieces), far_c], *weights, 2)
+    back_up = shift(near[n : 2 * n], "y", -1)
+    back_down = shift(near[2 * n :], "y", 1)
+    keep2, give2 = ffn([after(far, near), far_c], *weights, 2)
     got2 = shift(give2, "core", 1, 2)
     back_far = shift((keep2.astype(f32) + got2.astype(f32)).astype(bf16), "y", 2)
-    parts = (keep0, got0, back_up, back_down, back_far)
+    heads_out = finish(
+        before, *by_z, kept, qd, mix_gate, ret_gain.reshape(1, -1)
+    )
+    pieces = lax.all_to_all(heads_out, tp, split_axis=0, concat_axis=0, tiled=True)
+    parts = (near[:n], back_up, back_down, back_far)
     expert_rows = sum(v.astype(f32) for v in parts).astype(bf16)
     returned = lax.all_to_all(expert_rows, ep, split_axis=0, concat_axis=0, tiled=True)
     mix_out = project(pieces, w_out)
@@ -490,6 +488,7 @@
         P(ep, tp, None),
     )
     out_specs = (P(every, None), P(every, None))
+
     return jax.shard_map(
         on_device, mesh=fine, in_specs=in_specs, out_specs=out_specs, check_vma=False
     )

time: 161 us -> 150 us (0.932)
  waiting for transfers between devices: 61.2 us -> 49.7 us
  Pallas kernels: 54.7 us -> 49.7 us
  local copies, waits for them, and re-layouts: 3.16 us -> 5.01 us
  starting transfers between devices: 35.4 us -> 37.2 us
    ppermute x19 -> x18, waiting for transfers between devices: 46.7 us -> 36.1 us  [shift(): return lax.ppermute(x, axis, pairs)]
    pallas_call x3 -> x2, Pallas kernels: 27.7 us -> 22.6 us  [ffn(): pl.pallas_call(functools.partial(ffn_kernel, n_x, tile, groups), out_shap...]
    ppermute x19 -> x18, starting transfers between devices: 20.3 us -> 21.8 us  [shift(): return lax.ppermute(x, axis, pairs)]
    unnamed x34 -> x38, local copies, waits for them, and re-layouts: 3 us -> 3.89 us
  transfers between devices with their start and end apart: 22 -> 21, of which waited for: 8 -> 10; matrix products, arithmetic and copies ran while one was open for 2% -> 5% of each run, Pallas kernels for 19% -> 21%
where the time goes in v3:
time: 150 us; the launch traced here: 149 us
  Pallas kernels  49.7 us (33%)
  waiting for transfers between devices  49.7 us (33%)
  starting transfers between devices  37.2 us (25%)
  other arithmetic  6.17 us (4%)
  local copies, waits for them, and re-layouts  5.01 us (3%)
    ppermute x18, waiting for transfers between devices, shift(): return lax.ppermute(x, axis, pairs)  36.1 us
    pallas_call x2, Pallas kernels, ffn(): pl.pallas_call(functools.partial(ffn_kernel, n_x, tile, groups), out_shap...  22.6 us
    ppermute x18, starting transfers between devices, shift(): return lax.ppermute(x, axis, pairs)  21.8 us
    pallas_call x1, Pallas kernels, project(): pl.pallas_call(project_kernel, grid=(width // cols,), out_shape=jax.Shape...  8.67 us
    all_to_all x1, starting transfers between devices, on_device(): own = lax.all_to_all(outgoing, ep, split_axis=0, concat_axis=0, tiled=True)  7.99 us
    all_to_all x1, waiting for transfers between devices, on_device(): lax.all_to_all(heads_out, tp, split_axis=0, concat_axis=0, tiled=True)  7.39 us
    pallas_call x1, Pallas kernels, local_part(): pl.pallas_call(local_kernel, grid=(blocks,), out_shape=[jax.ShapeDtypeStr...  6.56 us
    pallas_call x1, Pallas kernels, finish(): pl.pallas_call(finish_kernel, grid=(rows // BLOCK,), out_shape=jax.ShapeD...  5.05 us
  transfers between devices with their start and end apart: 21, of which 10 were waited for; matrix products, arithmetic and copies ran while one was open for 5% of the time, Pallas kernels for 21%

profile of v3, /device:TPU:0, one launch (start us, length us, event | category | flops | bytes accessed | tf_op | source)
XLA Modules:
  0.0 148.7 jit_solution(7238881061467823018)
XLA Ops:
  0.6 2.3 %pre.1 = bf16[128,2048]{1,0:T(8,128)(2,1)} custom-call(bf16[32,2048]{1,0:T(8,128)(2,1)} %x_ref.1, s32[2,32]{1,0:T(2,128)} %bitcast.36, f32[1,2048]{1,0:T(1,128)} %bitcast.33), custom_call_target="tpu_custom_call" | custom-call | flops 2000000000 | bytes 1000000 | tf_op jit(solution)/shard_map/pre/pallas_call | solution.py:408
  2.9 8.0 %all-to-all-start.1 = ((bf16[16,8,2048]{2,1,0:T(8,128)(2,1)}), bf16[16,8,2048]{2,1,0:T(8,128)(2,1)S(1)}, u32[]{:S(2)}, u32[]{:S(2)}) async-start(bf16[16,8,2048]{2,1,0:T(8,128)(2,1)} %bitcast.30), calls=%async_computation.1 | async-start | bytes 1048576 | tf_op jit(solution)/shard_map/all_to_all | solution.py:414
  11.1 0.6 pad_maximum_fusion.base_ref
  11.7 6.6 %local.1 = (f32[2048,256]{1,0:T(8,128)}, bf16[2048,256]{1,0:T(8,128)(2,1)}, bf16[264,256]{1,0:T(8,128)(2,1)}) custom-call(f32[4,2,128]{2,1,0:T(2,128)} %pad_maximum_fusion.base_ref, bf16[2048,256]{1,0:T(8,128)(2,1)} %q_ref, bf16[2048,256]{1,0:T(8,128)(2,1)} %k_ref.1, bf16[2048,256]{1,0:T(8,128)(2,1)} %v_ref.1, f32[4,1,512]{2,1,0:T(1,128)} %bitcast.34, ...), custom_call_target="tpu_custom_call" | custom-call | flops 6000000000 | bytes 6291456 | tf_op jit(solution)/shard_map/local/pallas_call | solution.py:241
  18.2 4.2 %all-to-all-done.1 = bf16[16,8,2048]{2,1,0:T(8,128)(2,1)S(1)} async-done(((bf16[16,8,2048]{2,1,0:T(8,128)(2,1)}), bf16[16,8,2048]{2,1,0:T(8,128)(2,1)S(1)}, u32[]{:S(2)}, u32[]{:S(2)}) %all-to-all-start.1) | async-done | bytes 524320 | tf_op jit(solution)/shard_map/all_to_all | solution.py:414
  22.4 1.6 %collective-permute-start.6 = (bf16[128,2048]{1,0:T(8,128)(2,1)S(1)}, bf16[128,2048]{1,0:T(8,128)(2,1)S(1)}, u32[]{:S(2)}, u32[]{:S(2)}) collective-permute-start(bf16[128,2048]{1,0:T(8,128)(2,1)S(1)} %bitcast.25), channel_id=1, source_target_pairs={{0,2},{2,4},{4,6},{6,0},{1,3},{3,5},{5,7},{7,1},{8,10},{10,12},{12... | collective-permute-start | bytes 1572872 | tf_op jit(solution)/shard_map/ppermute | solution.py:35
  24.0 1.7 %collective-permute-start.7 = (bf16[128,2048]{1,0:T(8,128)(2,1)S(1)}, bf16[128,2048]{1,0:T(8,128)(2,1)S(1)}, u32[]{:S(2)}, u32[]{:S(2)}) collective-permute-start(bf16[128,2048]{1,0:T(8,128)(2,1)S(1)} %bitcast.26), channel_id=1, source_target_pairs={{0,6},{2,0},{4,2},{6,4},{1,7},{3,1},{5,3},{7,5},{8,14},{10,8},{12,... | collective-permute-start | bytes 1572872 | tf_op jit(solution)/shard_map/ppermute | solution.py:35
  25.7 10.3 %collective-permute-done.6.refs_1_ = bf16[128,2048]{1,0:T(8,128)(2,1)S(1)} collective-permute-done((bf16[128,2048]{1,0:T(8,128)(2,1)S(1)}, bf16[128,2048]{1,0:T(8,128)(2,1)S(1)}, u32[]{:S(2)}, u32[]{:S(2)}) %collective-permute-start.6) | collective-permute-done | bytes 524320 | tf_op jit(solution)/shard_map/ppermute | solution.py:35
  36.0 0.5 collective-permute-start.10
  36.5 1.4 collective-permute-done.9.refs_4_
  37.9 0.7 collective-permute-done.10.refs_5_
  38.7 0.1 copy-done.10
  38.7 0.7 copy-done.11
  39.5 14.2 %shard_map.176 = (bf16[384,2048]{1,0:T(8,128)(2,1)}, bf16[384,2048]{1,0:T(8,128)(2,1)}) custom-call(bf16[128,2048]{1,0:T(8,128)(2,1)} %bitcast.28, bf16[128,2048]{1,0:T(8,128)(2,1)} %copy-done.7, bf16[128,2048]{1,0:T(8,128)(2,1)} %copy-done.8, bf16[128,2048]{1,0:T(8,128)(2,1)} %copy-done.9, bf16[128,2048]{1,0:T(8,128)(2,1)} %copy-done.10, ...), custom_call_target="tpu_custom_call" | custom-call | flops 8455716864 | bytes 17301504 | tf_op jit(solution)/shard_map/pallas_call | solution.py:143
  53.6 0.2 collective-permute-start.11
  53.9 2.2 %collective-permute-start.14 = (bf16[128,2048]{1,0:T(8,128)(2,1)}, bf16[128,2048]{1,0:T(8,128)(2,1)S(1)}, u32[]{:S(2)}, u32[]{:S(2)}) collective-permute-start(bf16[128,2048]{1,0:T(8,128)(2,1)} %bitcast.29), channel_id=1, source_target_pairs={{0,4},{2,6},{4,0},{6,2},{1,5},{3,7},{5,1},{7,3},{8,12},{10,14},{12... | collective-permute-start | bytes 1572872 | tf_op jit(solution)/shard_map/ppermute | solution.py:35
  56.0 0.6 collective-permute-start
  56.6 1.7 %collective-permute-start.1 = (bf16[264,256]{1,0:T(8,128)(2,1)S(1)}, bf16[264,256]{1,0:T(8,128)(2,1)S(1)}, u32[]{:S(2)}, u32[]{:S(2)}) collective-permute-start(bf16[264,256]{1,0:T(8,128)(2,1)S(1)} %copy-done.12), channel_id=1, source_target_pairs={{0,16},{8,24},{16,0},{24,8},{1,17},{9,25},{17,1},{25,9},{2,18},{10... | collective-permute-start | bytes 405512 | tf_op jit(solution)/shard_map/ppermute | solution.py:35
  58.3 1.2 collective-permute-start.2
  59.4 10.3 %collective-permute-done.14.refs_0_ = bf16[128,2048]{1,0:T(8,128)(2,1)S(1)} collective-permute-done((bf16[128,2048]{1,0:T(8,128)(2,1)}, bf16[128,2048]{1,0:T(8,128)(2,1)S(1)}, u32[]{:S(2)}, u32[]{:S(2)}) %collective-permute-start.14) | collective-permute-done | bytes 524320 | tf_op jit(solution)/shard_map/ppermute | solution.py:35
  69.8 2.2 %add_convert_fusion = bf16[384,2048]{1,0:T(8,128)(2,1)S(1)} fusion(bf16[384,2048]{1,0:T(8,128)(2,1)S(1)} %collective-permute-done.11, bf16[384,2048]{1,0:T(8,128)(2,1)} %get-tuple-element.21), kind=kLoop, calls=%fused_computation | loop fusion | flops 3145728 | bytes 4718592 | tf_op jit(solution)/shard_map/convert_element_type | solution.py:447
  72.0 0.8 copy-done.3
  72.8 8.5 %shard_map.177 = (bf16[128,2048]{1,0:T(8,128)(2,1)}, bf16[128,2048]{1,0:T(8,128)(2,1)}) custom-call(bf16[128,2048]{1,0:T(8,128)(2,1)} %copy-done.2, bf16[128,2048]{1,0:T(8,128)(2,1)} %copy-done.3, bf16[2048,896]{1,0:T(8,128)(2,1)} %bitcast.18, bf16[2048,896]{1,0:T(8,128)(2,1)} %bitcast.20, bf16[896,2048]{1,0:T(8,128)(2,1)} %bitcast.22), custom_call_target="tpu_custom_call" | custom-call | flops 2818572288 | bytes 13107200 | tf_op jit(solution)/shard_map/pallas_call | solution.py:143
  81.3 0.4 collective-permute-start.16
  81.7 0.7 copy-done.17
  82.5 2.2 %middle.1 = (f32[264,256]{1,0:T(8,128)}, bf16[264,256]{1,0:T(8,128)(2,1)}) custom-call(s32[1]{0:T(128)} %bitcast.x_ref, bf16[264,256]{1,0:T(8,128)(2,1)} %get-tuple-element.15.own_ref, bf16[264,256]{1,0:T(8,128)(2,1)} %copy-done.13, bf16[264,256]{1,0:T(8,128)(2,1)} %copy-done.15, bf16[264,256]{1,0:T(8,128)(2,1)} %copy-done.17), custom_call_target="tpu_custom_call" | custom-call | flops 500000000 | bytes 1000000 | tf_op jit(solution)/shard_map/middle/pallas_call | solution.py:294
  84.7 1.9 %collective-permute-start.3 = (bf16[264,256]{1,0:T(8,128)(2,1)}, bf16[264,256]{1,0:T(8,128)(2,1)S(1)}, u32[]{:S(2)}, u32[]{:S(2)}) collective-permute-start(bf16[264,256]{1,0:T(8,128)(2,1)} %get-tuple-element.17), channel_id=1, source_target_pairs={{0,32},{32,64},{64,96},{1,33},{33,65},{65,97},{2,34},{34,66},{66,9... | collective-permute-start | bytes 405512 | tf_op jit(solution)/shard_map/ppermute | solution.py:35
  86.6 4.5 %collective-permute-start.4 = (bf16[264,256]{1,0:T(8,128)(2,1)}, bf16[264,256]{1,0:T(8,128)(2,1)S(1)}, u32[]{:S(2)}, u32[]{:S(2)}) collective-permute-start(bf16[264,256]{1,0:T(8,128)(2,1)} %get-tuple-element.17), channel_id=1, source_target_pairs={{0,64},{32,96},{1,65},{33,97},{2,66},{34,98},{3,67},{35,99},{4,68}... | collective-permute-start | bytes 405512 | tf_op jit(solution)/shard_map/ppermute | solution.py:35
  91.1 1.3 collective-permute-start.5
  92.4 1.1 fusion.1
  93.5 0.8 collective-permute-start.13
  94.3 2.4 %collective-permute-start.12 = (bf16[128,2048]{1,0:T(8,128)(2,1)}, bf16[128,2048]{1,0:T(8,128)(2,1)}, u32[]{:S(2)}, u32[]{:S(2)}) collective-permute-start(bf16[128,2048]{1,0:T(8,128)(2,1)} %get-tuple-element.26), channel_id=1, source_target_pairs={{0,6},{2,0},{4,2},{6,4},{1,7},{3,1},{5,3},{7,5},{8,14},{10,8},{12,... | collective-permute-start | bytes 1572872 | tf_op jit(solution)/shard_map/ppermute | solution.py:35
  96.7 0.9 add_convert_fusion.2
  97.7 1.0 collective-permute-start.17
  98.7 0.6 copy-done.16
  99.3 0.1 copy-done.18
  99.4 5.1 %finish.1 = bf16[2048,256]{1,0:T(8,128)(2,1)} custom-call(f32[264,256]{1,0:T(8,128)} %get-tuple-element.16.before_ref, bf16[264,256]{1,0:T(8,128)(2,1)} %copy-done.14, bf16[264,256]{1,0:T(8,128)(2,1)} %copy-done.16, bf16[264,256]{1,0:T(8,128)(2,1)} %copy-done.18, f32[2048,256]{1,0:T(8,128)} %get-tuple-element.18.kept_ref, ...), custom_call_target="tpu_custom_call" | custom-call | flops 2000000000 | bytes 5242880 | tf_op jit(solution)/shard_map/finish/pallas_call | solution.py:332
  104.4 3.8 %all-to-all-start = ((bf16[8,256,256]{2,1,0:T(8,128)(2,1)}), bf16[8,256,256]{2,1,0:T(8,128)(2,1)S(1)}, u32[]{:S(2)}, u32[]{:S(2)}) async-start(bf16[8,256,256]{2,1,0:T(8,128)(2,1)} %bitcast.24), calls=%async_computation | async-start | bytes 2097152 | tf_op jit(solution)/shard_map/all_to_all | solution.py:456
  108.3 1.0 collective-permute-done.13
  109.3 11.9 %collective-permute-done.12 = bf16[128,2048]{1,0:T(8,128)(2,1)} collective-permute-done((bf16[128,2048]{1,0:T(8,128)(2,1)}, bf16[128,2048]{1,0:T(8,128)(2,1)}, u32[]{:S(2)}, u32[]{:S(2)}) %collective-permute-start.12) | collective-permute-done | bytes 524320 | tf_op jit(solution)/shard_map/ppermute | solution.py:35
  121.2 0.4 collective-permute-done.17
  121.6 2.4 %fusion = bf16[16,8,2048]{2,1,0:T(8,128)(2,1)} fusion(bf16[128,2048]{1,0:T(8,128)(2,1)} %collective-permute-done.17, bf16[128,2048]{1,0:T(8,128)(2,1)S(1)} %collective-permute-done.13, bf16[128,2048]{1,0:T(8,128)(2,1)} %collective-permute-done.12, bf16[384,2048]{1,0:T(8,128)(2,1)S(1)} %add_convert_fusion), kind=kLoop, calls=%fused_computation.3 | loop fusion | flops 2097152 | bytes 2621440 | tf_op jit(solution)/shard_map/all_to_all | solution.py:459
  123.9 7.4 %all-to-all-done = bf16[8,256,256]{2,1,0:T(8,128)(2,1)S(1)} async-done(((bf16[8,256,256]{2,1,0:T(8,128)(2,1)}), bf16[8,256,256]{2,1,0:T(8,128)(2,1)S(1)}, u32[]{:S(2)}, u32[]{:S(2)}) %all-to-all-start) | async-done | bytes 1048608 | tf_op jit(solution)/shard_map/all_to_all | solution.py:456
  131.3 3.6 %all-to-all-start.2 = ((bf16[16,8,2048]{2,1,0:T(8,128)(2,1)}), bf16[16,8,2048]{2,1,0:T(8,128)(2,1)S(1)}, u32[]{:S(2)}, u32[]{:S(2)}) async-start(bf16[16,8,2048]{2,1,0:T(8,128)(2,1)} %fusion), calls=%async_computation.2 | async-start | bytes 1048576 | tf_op jit(solution)/shard_map/all_to_all | solution.py:459
  134.9 8.7 %project.1 = bf16[256,2048]{1,0:T(8,128)(2,1)} custom-call(bf16[2048,256]{1,0:T(8,128)(2,1)} %bitcast.23, bf16[2048,2048]{1,0:T(8,128)(2,1)} %w_ref.1), custom_call_target="tpu_custom_call" | custom-call | flops 4000000000 | bytes 10485760 | tf_op jit(solution)/shard_map/project/pallas_call | solution.py:362
  143.6 2.0 %all-to-all-done.2 = bf16[16,8,2048]{2,1,0:T(8,128)(2,1)S(1)} async-done(((bf16[16,8,2048]{2,1,0:T(8,128)(2,1)}), bf16[16,8,2048]{2,1,0:T(8,128)(2,1)S(1)}, u32[]{:S(2)}, u32[]{:S(2)}) %all-to-all-start.2) | async-done | bytes 524320 | tf_op jit(solution)/shard_map/all_to_all | solution.py:459
  145.6 0.8 copy-done.5
  146.4 2.3 %combine.1 = bf16[32,2048]{1,0:T(8,128)(2,1)} custom-call(bf16[128,2048]{1,0:T(8,128)(2,1)} %bitcast.31, s32[2,32]{1,0:T(2,128)} %bitcast.37, f32[2,32]{1,0:T(2,128)} %bitcast.38), custom_call_target="tpu_custom_call" | custom-call | flops 1000000000 | bytes 1000000 | tf_op jit(solution)/shard_map/combine/pallas_call | solution.py:461
  (48 shorter events, 0.3 us)
Async XLA Ops:
  0.6 10.4 %copy-start.6 = (f32[128]{0:T(128)S(1)}, f32[128]{0:T(128)}, u32[]{:S(2)}) copy-start(f32[128]{0:T(128)} %constant.21.clone) | copy-start | bytes 1540
  2.9 19.5 %all-to-all-start.1 = ((bf16[16,8,2048]{2,1,0:T(8,128)(2,1)}), bf16[16,8,2048]{2,1,0:T(8,128)(2,1)S(1)}, u32[]{:S(2)}, u32[]{:S(2)}) async-start(bf16[16,8,2048]{2,1,0:T(8,128)(2,1)} %bitcast.30), calls=%async_computation.1 | async-start | bytes 1048576 | tf_op jit(solution)/shard_map/all_to_all | solution.py:414
  22.4 16.2 %copy-start.4 = (bf16[16,8,2048]{2,1,0:T(8,128)(2,1)}, bf16[16,8,2048]{2,1,0:T(8,128)(2,1)S(1)}, u32[]{:S(2)}) copy-start(bf16[16,8,2048]{2,1,0:T(8,128)(2,1)S(1)} %all-to-all-done.1) | copy-start | bytes 1572868
  22.4 13.5 %collective-permute-start.6 = (bf16[128,2048]{1,0:T(8,128)(2,1)S(1)}, bf16[128,2048]{1,0:T(8,128)(2,1)S(1)}, u32[]{:S(2)}, u32[]{:S(2)}) collective-permute-start(bf16[128,2048]{1,0:T(8,128)(2,1)S(1)} %bitcast.25), channel_id=1, source_target_pairs={{0,2},{2,4},{4,6},{6,0},{1,3},{3,5},{5,7},{7,1},{8,10},{10,12},{12... | collective-permute-start | bytes 1572872 | tf_op jit(solution)/shard_map/ppermute | solution.py:35
  24.0 12.0 %collective-permute-start.7 = (bf16[128,2048]{1,0:T(8,128)(2,1)S(1)}, bf16[128,2048]{1,0:T(8,128)(2,1)S(1)}, u32[]{:S(2)}, u32[]{:S(2)}) collective-permute-start(bf16[128,2048]{1,0:T(8,128)(2,1)S(1)} %bitcast.26), channel_id=1, source_target_pairs={{0,6},{2,0},{4,2},{6,4},{1,7},{3,1},{5,3},{7,5},{8,14},{10,8},{12,... | collective-permute-start | bytes 1572872 | tf_op jit(solution)/shard_map/ppermute | solution.py:35
  25.7 10.8 %collective-permute-start.8 = (bf16[128,2048]{1,0:T(8,128)(2,1)S(1)}, bf16[128,2048]{1,0:T(8,128)(2,1)S(1)}, u32[]{:S(2)}, u32[]{:S(2)}) collective-permute-start(bf16[128,2048]{1,0:T(8,128)(2,1)S(1)} %bitcast.27), channel_id=1, source_target_pairs={{0,1},{1,0},{2,3},{3,2},{4,5},{5,4},{6,7},{7,6},{8,9},{9,8},{10,11... | collective-permute-start | bytes 1572872 | tf_op jit(solution)/shard_map/ppermute | solution.py:35
  36.0 2.7 %copy-start.7 = (bf16[128,2048]{1,0:T(8,128)(2,1)}, bf16[128,2048]{1,0:T(8,128)(2,1)S(1)}, u32[]{:S(2)}) copy-start(bf16[128,2048]{1,0:T(8,128)(2,1)S(1)} %collective-permute-done.6.refs_1_) | copy-start | bytes 1572868
  36.0 1.9 %collective-permute-start.9 = (bf16[128,2048]{1,0:T(8,128)(2,1)S(1)}, bf16[128,2048]{1,0:T(8,128)(2,1)S(1)}, u32[]{:S(2)}, u32[]{:S(2)}) collective-permute-start(bf16[128,2048]{1,0:T(8,128)(2,1)S(1)} %collective-permute-done.6.refs_1_), channel_id=1, source_target_pairs={{0,1},{1,0},{2,3},{3,2},{4,5},{5,4},{6,7},{7,6},{8,9},{9,8},{10,11... | collective-permute-start | bytes 1572872 | tf_op jit(solution)/shard_map/ppermute | solution.py:35
  36.0 2.6 %copy-start.8 = (bf16[128,2048]{1,0:T(8,128)(2,1)}, bf16[128,2048]{1,0:T(8,128)(2,1)S(1)}, u32[]{:S(2)}) copy-start(bf16[128,2048]{1,0:T(8,128)(2,1)S(1)} %collective-permute-done.7.refs_2_) | copy-start | bytes 1572868
  36.0 2.6 %collective-permute-start.10 = (bf16[128,2048]{1,0:T(8,128)(2,1)S(1)}, bf16[128,2048]{1,0:T(8,128)(2,1)S(1)}, u32[]{:S(2)}, u32[]{:S(2)}) collective-permute-start(bf16[128,2048]{1,0:T(8,128)(2,1)S(1)} %collective-permute-done.7.refs_2_), channel_id=1, source_target_pairs={{0,1},{1,0},{2,3},{3,2},{4,5},{5,4},{6,7},{7,6},{8,9},{9,8},{10,11... | collective-permute-start | bytes 1572872 | tf_op jit(solution)/shard_map/ppermute | solution.py:35
  36.5 2.2 %copy-start.9 = (bf16[128,2048]{1,0:T(8,128)(2,1)}, bf16[128,2048]{1,0:T(8,128)(2,1)S(1)}, u32[]{:S(2)}) copy-start(bf16[128,2048]{1,0:T(8,128)(2,1)S(1)} %collective-permute-done.8.refs_3_) | copy-start | bytes 1572868
  37.9 0.9 copy-start.10
  38.6 0.8 copy-start.11
  39.5 16.6 %copy-start.12 = (bf16[264,256]{1,0:T(8,128)(2,1)S(1)}, bf16[264,256]{1,0:T(8,128)(2,1)}, u32[]{:S(2)}) copy-start(bf16[264,256]{1,0:T(8,128)(2,1)} %get-tuple-element.15.own_ref) | copy-start | bytes 405508
  53.6 16.1 %collective-permute-start.11 = (bf16[384,2048]{1,0:T(8,128)(2,1)}, bf16[384,2048]{1,0:T(8,128)(2,1)S(1)}, u32[]{:S(2)}, u32[]{:S(2)}) collective-permute-start(bf16[384,2048]{1,0:T(8,128)(2,1)} %get-tuple-element.22), channel_id=1, source_target_pairs={{0,1},{1,0},{2,3},{3,2},{4,5},{5,4},{6,7},{7,6},{8,9},{9,8},{10,11... | collective-permute-start | bytes 4718600 | tf_op jit(solution)/shard_map/ppermute | solution.py:35
  53.9 15.9 %collective-permute-start.14 = (bf16[128,2048]{1,0:T(8,128)(2,1)}, bf16[128,2048]{1,0:T(8,128)(2,1)S(1)}, u32[]{:S(2)}, u32[]{:S(2)}) collective-permute-start(bf16[128,2048]{1,0:T(8,128)(2,1)} %bitcast.29), channel_id=1, source_target_pairs={{0,4},{2,6},{4,0},{6,2},{1,5},{3,7},{5,1},{7,3},{8,12},{10,14},{12... | collective-permute-start | bytes 1572872 | tf_op jit(solution)/shard_map/ppermute | solution.py:35
  56.0 25.7 %collective-permute-start = (bf16[264,256]{1,0:T(8,128)(2,1)S(1)}, bf16[264,256]{1,0:T(8,128)(2,1)S(1)}, u32[]{:S(2)}, u32[]{:S(2)}) collective-permute-start(bf16[264,256]{1,0:T(8,128)(2,1)S(1)} %copy-done.12), channel_id=1, source_target_pairs={{0,8},{8,16},{16,24},{24,0},{1,9},{9,17},{17,25},{25,1},{2,10},{10... | collective-permute-start | bytes 405512 | tf_op jit(solution)/shard_map/ppermute | solution.py:35
  56.6 25.1 %collective-permute-start.1 = (bf16[264,256]{1,0:T(8,128)(2,1)S(1)}, bf16[264,256]{1,0:T(8,128)(2,1)S(1)}, u32[]{:S(2)}, u32[]{:S(2)}) collective-permute-start(bf16[264,256]{1,0:T(8,128)(2,1)S(1)} %copy-done.12), channel_id=1, source_target_pairs={{0,16},{8,24},{16,0},{24,8},{1,17},{9,25},{17,1},{25,9},{2,18},{10... | collective-permute-start | bytes 405512 | tf_op jit(solution)/shard_map/ppermute | solution.py:35
  58.3 23.5 %collective-permute-start.2 = (bf16[264,256]{1,0:T(8,128)(2,1)S(1)}, bf16[264,256]{1,0:T(8,128)(2,1)S(1)}, u32[]{:S(2)}, u32[]{:S(2)}) collective-permute-start(bf16[264,256]{1,0:T(8,128)(2,1)S(1)} %copy-done.12), channel_id=1, source_target_pairs={{0,24},{8,0},{16,8},{24,16},{1,25},{9,1},{17,9},{25,17},{2,26},{10... | collective-permute-start | bytes 405512 | tf_op jit(solution)/shard_map/ppermute | solution.py:35
  69.8 2.2 %copy-start.2 = (bf16[128,2048]{1,0:T(8,128)(2,1)}, bf16[128,2048]{1,0:T(8,128)(2,1)S(1)}, u32[]{:S(2)}) copy-start(bf16[128,2048]{1,0:T(8,128)(2,1)S(1)} %collective-permute-done.14.refs_0_) | copy-start | bytes 1572868
  69.8 2.2 %collective-permute-start.15 = (bf16[128,2048]{1,0:T(8,128)(2,1)S(1)}, bf16[128,2048]{1,0:T(8,128)(2,1)S(1)}, u32[]{:S(2)}, u32[]{:S(2)}) collective-permute-start(bf16[128,2048]{1,0:T(8,128)(2,1)S(1)} %collective-permute-done.14.refs_0_), channel_id=1, source_target_pairs={{0,1},{1,0},{2,3},{3,2},{4,5},{5,4},{6,7},{7,6},{8,9},{9,8},{10,11... | collective-permute-start | bytes 1572872 | tf_op jit(solution)/shard_map/ppermute | solution.py:35
  72.0 0.8 copy-start.3
  81.3 13.0 %collective-permute-start.16 = (bf16[128,2048]{1,0:T(8,128)(2,1)}, bf16[128,2048]{1,0:T(8,128)(2,1)S(1)}, u32[]{:S(2)}, u32[]{:S(2)}) collective-permute-start(bf16[128,2048]{1,0:T(8,128)(2,1)} %get-tuple-element.25), channel_id=1, source_target_pairs={{0,1},{1,0},{2,3},{3,2},{4,5},{5,4},{6,7},{7,6},{8,9},{9,8},{10,11... | collective-permute-start | bytes 1572872 | tf_op jit(solution)/shard_map/ppermute | solution.py:35
  81.7 0.7 copy-start.13
  81.7 0.8 copy-start.15
  81.7 0.7 copy-start.17
  82.5 14.2 %copy-start.1 = (bf16[128,2048]{1,0:T(8,128)(2,1)S(1)}, bf16[128,2048]{1,0:T(8,128)(2,1)}, u32[]{:S(2)}) copy-start(bf16[128,2048]{1,0:T(8,128)(2,1)} %get-tuple-element.24) | copy-start | bytes 1572868
  84.7 13.0 %collective-permute-start.3 = (bf16[264,256]{1,0:T(8,128)(2,1)}, bf16[264,256]{1,0:T(8,128)(2,1)S(1)}, u32[]{:S(2)}, u32[]{:S(2)}) collective-permute-start(bf16[264,256]{1,0:T(8,128)(2,1)} %get-tuple-element.17), channel_id=1, source_target_pairs={{0,32},{32,64},{64,96},{1,33},{33,65},{65,97},{2,34},{34,66},{66,9... | collective-permute-start | bytes 405512 | tf_op jit(solution)/shard_map/ppermute | solution.py:35
  86.6 12.1 %collective-permute-start.4 = (bf16[264,256]{1,0:T(8,128)(2,1)}, bf16[264,256]{1,0:T(8,128)(2,1)S(1)}, u32[]{:S(2)}, u32[]{:S(2)}) collective-permute-start(bf16[264,256]{1,0:T(8,128)(2,1)} %get-tuple-element.17), channel_id=1, source_target_pairs={{0,64},{32,96},{1,65},{33,97},{2,66},{34,98},{3,67},{35,99},{4,68}... | collective-permute-start | bytes 405512 | tf_op jit(solution)/shard_map/ppermute | solution.py:35
  91.1 7.5 %collective-permute-start.5 = (bf16[264,256]{1,0:T(8,128)(2,1)}, bf16[264,256]{1,0:T(8,128)(2,1)S(1)}, u32[]{:S(2)}, u32[]{:S(2)}) collective-permute-start(bf16[264,256]{1,0:T(8,128)(2,1)} %get-tuple-element.17), channel_id=1, source_target_pairs={{0,96},{1,97},{2,98},{3,99},{4,100},{5,101},{6,102},{7,103},{8,104... | collective-permute-start | bytes 405512 | tf_op jit(solution)/shard_map/ppermute | solution.py:35
  93.5 15.8 %collective-permute-start.13 = (bf16[128,2048]{1,0:T(8,128)(2,1)}, bf16[128,2048]{1,0:T(8,128)(2,1)S(1)}, u32[]{:S(2)}, u32[]{:S(2)}) collective-permute-start(bf16[128,2048]{1,0:T(8,128)(2,1)} %get-tuple-element.27), channel_id=1, source_target_pairs={{0,2},{2,4},{4,6},{6,0},{1,3},{3,5},{5,7},{7,1},{8,10},{10,12},{12... | collective-permute-start | bytes 1572872 | tf_op jit(solution)/shard_map/ppermute | solution.py:35
  94.3 26.9 %collective-permute-start.12 = (bf16[128,2048]{1,0:T(8,128)(2,1)}, bf16[128,2048]{1,0:T(8,128)(2,1)}, u32[]{:S(2)}, u32[]{:S(2)}) collective-permute-start(bf16[128,2048]{1,0:T(8,128)(2,1)} %get-tuple-element.26), channel_id=1, source_target_pairs={{0,6},{2,0},{4,2},{6,4},{1,7},{3,1},{5,3},{7,5},{8,14},{10,8},{12,... | collective-permute-start | bytes 1572872 | tf_op jit(solution)/shard_map/ppermute | solution.py:35
  97.7 1.0 copy-start.14
  97.7 23.9 %collective-permute-start.17 = (bf16[128,2048]{1,0:T(8,128)(2,1)}, bf16[128,2048]{1,0:T(8,128)(2,1)}, u32[]{:S(2)}, u32[]{:S(2)}) collective-permute-start(bf16[128,2048]{1,0:T(8,128)(2,1)} %add_convert_fusion.2), channel_id=1, source_target_pairs={{0,4},{2,6},{4,0},{6,2},{1,5},{3,7},{5,1},{7,3},{8,12},{10,14},{12... | collective-permute-start | bytes 1572872 | tf_op jit(solution)/shard_map/ppermute | solution.py:35
  98.6 0.6 copy-start.16
  98.7 0.7 copy-start.18
  104.4 26.9 %all-to-all-start = ((bf16[8,256,256]{2,1,0:T(8,128)(2,1)}), bf16[8,256,256]{2,1,0:T(8,128)(2,1)S(1)}, u32[]{:S(2)}, u32[]{:S(2)}) async-start(bf16[8,256,256]{2,1,0:T(8,128)(2,1)} %bitcast.24), calls=%async_computation | async-start | bytes 2097152 | tf_op jit(solution)/shard_map/all_to_all | solution.py:456
  131.3 3.6 %copy-start = (bf16[8,256,256]{2,1,0:T(8,128)(2,1)}, bf16[8,256,256]{2,1,0:T(8,128)(2,1)S(1)}, u32[]{:S(2)}) copy-start(bf16[8,256,256]{2,1,0:T(8,128)(2,1)S(1)} %all-to-all-done) | copy-start | bytes 3145732
  131.3 14.3 %all-to-all-start.2 = ((bf16[16,8,2048]{2,1,0:T(8,128)(2,1)}), bf16[16,8,2048]{2,1,0:T(8,128)(2,1)S(1)}, u32[]{:S(2)}, u32[]{:S(2)}) async-start(bf16[16,8,2048]{2,1,0:T(8,128)(2,1)} %fusion), calls=%async_computation.2 | async-start | bytes 1048576 | tf_op jit(solution)/shard_map/all_to_all | solution.py:459
  145.6 0.8 copy-start.5

commit v4 on v3

--- a/solution.py
+++ b/solution.py
@@ -19,6 +19,8 @@
 norm_eps = 1e-06
 
 
+FFN_VMEM = 30 * 2**20
+
 f32 = jnp.float32
 bf16 = jnp.bfloat16
 
@@ -33,6 +35,10 @@
 def shift(x, axis, by, size=4, wrap=True):
     pairs = [(j, (j + by) % size) for j in range(size) if wrap or 0 <= j + by < size]
     return lax.ppermute(x, axis, pairs)
+
+
+def vm(x):
+    return pltpu.with_memory_space_constraint(x, pltpu.VMEM)
 
 
 def after(x, *earlier):
@@ -80,88 +86,50 @@
     out_ref[...] = total.astype(bf16)
 
 
-def ffn_kernel(n_x, tile, groups, *refs):
+def ffn_kernel(n_x, *refs):
     xs = refs[:n_x]
     wg, wu, wd = refs[n_x : n_x + 3]
-    outs = refs[n_x + 3 : -9]
-    xbuf, gbuf, ubuf, dbuf, hbuf, obuf, xsem, wsem, osem = refs[-9:]
-    per_out = n_x // len(outs)
-    copies_w = []
-    for j, (lo, hi) in enumerate(groups):
-        cols = pl.ds(lo, hi - lo)
-        a = pltpu.make_async_copy(wg.at[:, cols], gbuf.at[:, cols], wsem.at[2 * j])
-        b = pltpu.make_async_copy(wu.at[:, cols], ubuf.at[:, cols], wsem.at[2 * j + 1])
-        copies_w.append((a, b))
-    copies_x = [
-        pltpu.make_async_copy(xs[i], xbuf.at[pl.ds(i * tile, tile)], xsem.at[i])
-        for i in range(n_x)
-    ]
-    pair = 256 // tile
-    for c in copies_w[0]:
-        c.start()
-    for c in copies_x:
-        c.start()
-    for c in copies_w[1]:
-        c.start()
-    down = pltpu.make_async_copy(wd, dbuf, wsem.at[2 * len(groups)])
-    down.start()
-    for j, (lo, hi) in enumerate(groups):
-        for c in copies_w[j]:
-            c.wait()
-        for r in range(0, n_x * tile, 256):
-            if j == 0:
-                for i in range(r // tile, r // tile + pair):
-                    copies_x[i].wait()
-            x = xbuf[r : r + 256, :]
-            for at in range(lo, hi, 128):
-                w = jnp.concatenate([gbuf[:, at : at + 128], ubuf[:, at : at + 128]], axis=1)
-                both = mm(x, w)
-                gate, up = both[:, :128], both[:, 128:]
-                hidden = gate * up / (1.0 + jnp.exp(-gate))
-                hbuf[r : r + 256, at : at + 128] = hidden.astype(bf16)
-    down.wait()
-    stores = []
-    for r in range(0, n_x * tile, 256):
-        obuf[r : r + 256, :] = mm(hbuf[r : r + 256, :], dbuf[...]).astype(bf16)
-        for i in range(r // tile, r // tile + pair):
-            to = outs[i // per_out].at[pl.ds((i % per_out) * tile, tile)]
-            c = pltpu.make_async_copy(obuf.at[pl.ds(i * tile, tile)], to, osem.at[i])
-            c.start()
-            stores.append(c)
-    for c in stores:
-        c.wait()
-
-
-def ffn(xs, w_gate, w_up, w_down, n_out):
-    n_x = len(xs)
-    tile, width = xs[0].shape
-    ff = w_gate.shape[1]
+    outs = refs[n_x + 3 : -1]
+    hbuf = refs[-1]
+    tile = xs[0].shape[0]
+    for i in range(n_x):
+        x = xs[i][...]
+        for at in range(0, hbuf.shape[1], 128):
+            w = jnp.concatenate([wg[:, at : at + 128], wu[:, at : at + 128]], axis=1)
+            both = mm(x, w)
+            gate, up = both[:, :128], both[:, 128:]
+            hidden = gate * up / (1.0 + jnp.exp(-gate))
+            hbuf[i * tile : (i + 1) * tile, at : at + 128] = hidden.astype(bf16)
+    keep = len(outs) - 1
+    for i in range(n_x):
+        out = mm(hbuf[i * tile : (i + 1) * tile, :], wd[...]).astype(bf16)
+        if i < keep:
+            outs[i][...] = out
+        else:
+            at = (i - keep) * tile
+            outs[keep][at : at + tile, :] = out
+
+
+def ffn(keep, give, weights):
+    n_x = len(keep) + len(give)
+    tile, width = keep[0].shape
+    ff = weights[0].shape[1]
     rows = n_x * tile
-    cut = 128 * ((ff // 128 + 1) // 2)
-    groups = ((0, cut), (cut, ff))
-    hbm = pl.BlockSpec(memory_space=pl.ANY)
+    in_vmem = pl.BlockSpec(memory_space=pltpu.VMEM)
     return pl.pallas_call(
-        functools.partial(ffn_kernel, n_x, tile, groups),
-        out_shape=[jax.ShapeDtypeStruct((rows // n_out, width), bf16)] * n_out,
-        in_specs=[hbm] * (n_x + 3),
-        out_specs=[hbm] * n_out,
-        scratch_shapes=[
-            pltpu.VMEM((rows, width), bf16),
-            pltpu.VMEM((width, ff), bf16),
-            pltpu.VMEM((width, ff), bf16),
-            pltpu.VMEM((ff, width), bf16),
-            pltpu.VMEM((rows, ff), bf16),
-            pltpu.VMEM((rows, width), bf16),
-            pltpu.SemaphoreType.DMA((n_x,)),
-            pltpu.SemaphoreType.DMA((2 * len(groups) + 1,)),
-            pltpu.SemaphoreType.DMA((n_x,)),
-        ],
+        functools.partial(ffn_kernel, n_x),
+        out_shape=[pltpu.VMEM((tile, width), bf16)] * len(keep)
+        + [pltpu.VMEM((len(give) * tile, width), bf16)],
+        in_specs=[in_vmem] * (n_x + 3),
+        out_specs=[in_vmem] * (len(keep) + 1),
+        scratch_shapes=[pltpu.VMEM((rows, ff), bf16)],
+        compiler_params=pltpu.CompilerParams(vmem_limit_bytes=FFN_VMEM),
         cost_estimate=pl.CostEstimate(
             flops=6 * rows * width * ff,
             bytes_accessed=2 * (3 * width * ff + 2 * rows * width),
             transcendentals=rows * ff,
         ),
-    )(*xs, w_gate, w_up, w_down)
+    )(*[vm(x) for x in (*keep, *give)], *[vm(w) for w in weights])
 
 
 def local_kernel(
@@ -441,20 +409,23 @@
     down_c = shift(down, "core", 1, 2)
     weights = (w_gate[0], w_up[0], w_down[0])
     n = own.shape[0]
-    keep1, give1 = ffn([own, up, down, own_c, up_c, down_c], *weights, 2)
+    *keep, give1 = ffn([own, up, down], [own_c, up_c, down_c], weights)
     got1 = shift(give1, "core", 1, 2)
     far_c = shift(far, "core", 1, 2)
-    near = (keep1.astype(f32) + got1.astype(f32)).astype(bf16)
-    back_up = shift(near[n : 2 * n], "y", -1)
-    back_down = shift(near[2 * n :], "y", 1)
-    keep2, give2 = ffn([after(far, near), far_c], *weights, 2)
+    near = [
+        (k.astype(f32) + got1[i * n : (i + 1) * n].astype(f32)).astype(bf16)
+        for i, k in enumerate(keep)
+    ]
+    back_up = shift(near[1], "y", -1)
+    back_down = shift(near[2], "y", 1)
+    keep2, give2 = ffn([after(far, near[2])], [far_c], weights)
     got2 = shift(give2, "core", 1, 2)
     back_far = shift((keep2.astype(f32) + got2.astype(f32)).astype(bf16), "y", 2)
     heads_out = finish(
         before, *by_z, kept, qd, mix_gate, ret_gain.reshape(1, -1)
     )
     pieces = lax.all_to_all(heads_out, tp, split_axis=0, concat_axis=0, tiled=True)
-    parts = (near[:n], back_up, back_down, back_far)
+    parts = (near[0], back_up, back_down, back_far)
     expert_rows = sum(v.astype(f32) for v in parts).astype(bf16)
     returned = lax.all_to_all(expert_rows, ep, split_axis=0, concat_axis=0, tiled=True)
     mix_out = project(pieces, w_out)

time: 150 us -> 153 us (1.020)
  Pallas kernels: 49.7 us -> 39.8 us
  waiting for transfers between devices: 49.7 us -> 58.4 us
  local copies, waits for them, and re-layouts: 5.01 us -> 8.32 us
  starting transfers between devices: 37.2 us -> 38.8 us
    ppermute x18, waiting for transfers between devices: 36.1 us -> 46.2 us  [shift(): return lax.ppermute(x, axis, pairs)]
    pallas_call x2, Pallas kernels: 22.6 us -> 12.9 us  [ffn(): pl.pallas_call(functools.partial(ffn_kernel, n_x), out_shape=[pltpu.VMEM(...]
    unnamed x38 -> x26, local copies, waits for them, and re-layouts: 3.89 us -> 8.25 us
  transfers between devices with their start and end apart: 21 -> 21, of which waited for: 10 -> 13; matrix products, arithmetic and copies ran while one was open for 5% -> 4% of each run, Pallas kernels for 21% -> 15%
where the time goes in v4:
time: 153 us; the launch traced here: 152 us
  waiting for transfers between devices  58.4 us (38%)
  Pallas kernels  39.8 us (26%)
  starting transfers between devices  38.8 us (25%)
  local copies, waits for them, and re-layouts  8.32 us (5%)
  other arithmetic  5.66 us (4%)
    ppermute x18, waiting for transfers between devices, shift(): return lax.ppermute(x, axis, pairs)  46.2 us
    ppermute x18, starting transfers between devices, shift(): return lax.ppermute(x, axis, pairs)  21.8 us
    pallas_call x2, Pallas kernels, ffn(): pl.pallas_call(functools.partial(ffn_kernel, n_x), out_shape=[pltpu.VMEM(...  12.9 us
    pallas_call x1, Pallas kernels, project(): pl.pallas_call(project_kernel, grid=(width // cols,), out_shape=jax.Shape...  8.67 us
    unnamed x26, local copies, waits for them, and re-layouts  8.25 us
    all_to_all x1, starting transfers between devices, on_device(): own = lax.all_to_all(outgoing, ep, split_axis=0, concat_axis=0, tiled=True)  7.99 us
    all_to_all x1, waiting for transfers between devices, on_device(): lax.all_to_all(heads_out, tp, split_axis=0, concat_axis=0, tiled=True)  6.63 us
    pallas_call x1, Pallas kernels, local_part(): pl.pallas_call(local_kernel, grid=(blocks,), out_shape=[jax.ShapeDtypeStr...  6.55 us
  transfers between devices with their start and end apart: 21, of which 13 were waited for; matrix products, arithmetic and copies ran while one was open for 4% of the time, Pallas kernels for 15%

profile of v4, /device:TPU:0, one launch (start us, length us, event | category | flops | bytes accessed | tf_op | source)
XLA Modules:
  0.0 151.9 jit_solution(12617692323500942264)
XLA Ops:
  0.6 2.3 %pre.1 = bf16[128,2048]{1,0:T(8,128)(2,1)} custom-call(bf16[32,2048]{1,0:T(8,128)(2,1)} %x_ref.1, s32[2,32]{1,0:T(2,128)} %bitcast.35, f32[1,2048]{1,0:T(1,128)} %bitcast.32), custom_call_target="tpu_custom_call" | custom-call | flops 2000000000 | bytes 1000000 | tf_op jit(solution)/shard_map/pre/pallas_call | solution.py:376
  2.9 8.0 %all-to-all-start.1 = ((bf16[16,8,2048]{2,1,0:T(8,128)(2,1)}), bf16[16,8,2048]{2,1,0:T(8,128)(2,1)S(1)}, u32[]{:S(2)}, u32[]{:S(2)}) async-start(bf16[16,8,2048]{2,1,0:T(8,128)(2,1)} %bitcast.29), calls=%async_computation.1 | async-start | bytes 1048576 | tf_op jit(solution)/shard_map/all_to_all | solution.py:382
  11.1 0.6 pad_maximum_fusion.base_ref
  11.7 6.5 %local.1 = (f32[2048,256]{1,0:T(8,128)}, bf16[2048,256]{1,0:T(8,128)(2,1)}, bf16[264,256]{1,0:T(8,128)(2,1)}) custom-call(f32[4,2,128]{2,1,0:T(2,128)} %pad_maximum_fusion.base_ref, bf16[2048,256]{1,0:T(8,128)(2,1)} %q_ref, bf16[2048,256]{1,0:T(8,128)(2,1)} %k_ref.1, bf16[2048,256]{1,0:T(8,128)(2,1)} %v_ref.1, f32[4,1,512]{2,1,0:T(1,128)} %bitcast.33, ...), custom_call_target="tpu_custom_call" | custom-call | flops 6000000000 | bytes 6291456 | tf_op jit(solution)/shard_map/local/pallas_call | solution.py:209
  18.2 4.2 %all-to-all-done.1 = bf16[16,8,2048]{2,1,0:T(8,128)(2,1)S(1)} async-done(((bf16[16,8,2048]{2,1,0:T(8,128)(2,1)}), bf16[16,8,2048]{2,1,0:T(8,128)(2,1)S(1)}, u32[]{:S(2)}, u32[]{:S(2)}) %all-to-all-start.1) | async-done | bytes 524320 | tf_op jit(solution)/shard_map/all_to_all | solution.py:382
  22.4 1.6 %collective-permute-start.6 = (bf16[128,2048]{1,0:T(8,128)(2,1)S(1)}, bf16[128,2048]{1,0:T(8,128)(2,1)S(1)}, u32[]{:S(2)}, u32[]{:S(2)}) collective-permute-start(bf16[128,2048]{1,0:T(8,128)(2,1)S(1)} %bitcast.23), channel_id=1, source_target_pairs={{0,2},{2,4},{4,6},{6,0},{1,3},{3,5},{5,7},{7,1},{8,10},{10,12},{12... | collective-permute-start | bytes 1572872 | tf_op jit(solution)/shard_map/ppermute | solution.py:37
  24.0 1.7 %collective-permute-start.7 = (bf16[128,2048]{1,0:T(8,128)(2,1)S(1)}, bf16[128,2048]{1,0:T(8,128)(2,1)S(1)}, u32[]{:S(2)}, u32[]{:S(2)}) collective-permute-start(bf16[128,2048]{1,0:T(8,128)(2,1)S(1)} %bitcast.24), channel_id=1, source_target_pairs={{0,6},{2,0},{4,2},{6,4},{1,7},{3,1},{5,3},{7,5},{8,14},{10,8},{12,... | collective-permute-start | bytes 1572872 | tf_op jit(solution)/shard_map/ppermute | solution.py:37
  25.7 10.3 %collective-permute-done.6.refs_1_ = bf16[128,2048]{1,0:T(8,128)(2,1)S(1)} collective-permute-done((bf16[128,2048]{1,0:T(8,128)(2,1)S(1)}, bf16[128,2048]{1,0:T(8,128)(2,1)S(1)}, u32[]{:S(2)}, u32[]{:S(2)}) %collective-permute-start.6) | collective-permute-done | bytes 524320 | tf_op jit(solution)/shard_map/ppermute | solution.py:37
  36.0 0.5 collective-permute-start.10
  36.5 1.4 collective-permute-done.9.refs_4_
  37.9 0.7 collective-permute-done.10.refs_5_
  38.6 2.0 %copy-done = bf16[1,2048,896]{2,1,0:T(8,128)(2,1)S(1)} copy-done((bf16[1,2048,896]{2,1,0:T(8,128)(2,1)S(1)}, bf16[1,2048,896]{2,1,0:T(8,128)(2,1)}, u32[]{:S(2)}) %copy-start) | copy-done | bytes 3670040
  40.7 2.0 %copy-done.2 = bf16[1,2048,896]{2,1,0:T(8,128)(2,1)S(1)} copy-done((bf16[1,2048,896]{2,1,0:T(8,128)(2,1)S(1)}, bf16[1,2048,896]{2,1,0:T(8,128)(2,1)}, u32[]{:S(2)}) %copy-start.2) | copy-done | bytes 3670040
  42.7 2.0 %copy-done.3 = bf16[1,896,2048]{2,1,0:T(8,128)(2,1)S(1)} copy-done((bf16[1,896,2048]{2,1,0:T(8,128)(2,1)S(1)}, bf16[1,896,2048]{2,1,0:T(8,128)(2,1)}, u32[]{:S(2)}) %copy-start.3) | copy-done | bytes 3670040
  44.8 9.6 %shard_map.176 = (bf16[128,2048]{1,0:T(8,128)(2,1)S(1)}, bf16[128,2048]{1,0:T(8,128)(2,1)S(1)}, bf16[128,2048]{1,0:T(8,128)(2,1)S(1)}, bf16[384,2048]{1,0:T(8,128)(2,1)S(1)}) custom-call(bf16[128,2048]{1,0:T(8,128)(2,1)S(1)} %bitcast.26, bf16[128,2048]{1,0:T(8,128)(2,1)S(1)} %collective-permute-done.6.refs_1_, ...), custom_call_target="tpu_custom_call" | custom-call | flops 8455716864 | bytes 17301504 | tf_op jit(solution)/shard_map/pallas_call | solution.py:119
  54.3 0.2 collective-permute-start.11
  54.6 2.2 %collective-permute-start.14 = (bf16[128,2048]{1,0:T(8,128)(2,1)S(1)}, bf16[128,2048]{1,0:T(8,128)(2,1)S(1)}, u32[]{:S(2)}, u32[]{:S(2)}) collective-permute-start(bf16[128,2048]{1,0:T(8,128)(2,1)S(1)} %bitcast.27), channel_id=1, source_target_pairs={{0,4},{2,6},{4,0},{6,2},{1,5},{3,7},{5,1},{7,3},{8,12},{10,14},{12... | collective-permute-start | bytes 1572872 | tf_op jit(solution)/shard_map/ppermute | solution.py:37
  56.7 13.5 %collective-permute-done.14.refs_0_ = bf16[128,2048]{1,0:T(8,128)(2,1)S(1)} collective-permute-done((bf16[128,2048]{1,0:T(8,128)(2,1)S(1)}, bf16[128,2048]{1,0:T(8,128)(2,1)S(1)}, u32[]{:S(2)}, u32[]{:S(2)}) %collective-permute-start.14) | collective-permute-done | bytes 524320 | tf_op jit(solution)/shard_map/ppermute | solution.py:37
  70.3 1.4 add_convert_fusion.3
  71.7 0.5 collective-permute-done.15.refs_1_
  72.2 3.3 %shard_map.177 = (bf16[128,2048]{1,0:T(8,128)(2,1)S(1)}, bf16[128,2048]{1,0:T(8,128)(2,1)S(1)}) custom-call(bf16[128,2048]{1,0:T(8,128)(2,1)S(1)} %collective-permute-done.14.refs_0_, bf16[128,2048]{1,0:T(8,128)(2,1)S(1)} %collective-permute-done.15.refs_1_, bf16[2048,896]{1,0:T(8,128)(2,1)S(1)} %bitcast.18, bf16[2048,896]{1,0:T(8,128)(2,1)S(1)} %bitcast.20, ...), custom_call_target="tpu_custom_call" | custom-call | flops 2818572288 | bytes 13107200 | tf_op jit(solution)/shard_map/pallas_call | solution.py:119
  75.7 0.6 collective-permute-start
  76.3 1.7 %collective-permute-start.1 = (bf16[264,256]{1,0:T(8,128)(2,1)S(1)}, bf16[264,256]{1,0:T(8,128)(2,1)S(1)}, u32[]{:S(2)}, u32[]{:S(2)}) collective-permute-start(bf16[264,256]{1,0:T(8,128)(2,1)S(1)} %copy-done.6), channel_id=1, source_target_pairs={{0,16},{8,24},{16,0},{24,8},{1,17},{9,25},{17,1},{25,9},{2,18},{10... | collective-permute-start | bytes 405512 | tf_op jit(solution)/shard_map/ppermute | solution.py:37
  78.0 1.2 collective-permute-start.2
  79.1 6.6 %collective-permute-done.one_ref = bf16[264,256]{1,0:T(8,128)(2,1)S(1)} collective-permute-done((bf16[264,256]{1,0:T(8,128)(2,1)S(1)}, bf16[264,256]{1,0:T(8,128)(2,1)S(1)}, u32[]{:S(2)}, u32[]{:S(2)}) %collective-permute-start) | collective-permute-done | bytes 135200 | tf_op jit(solution)/shard_map/ppermute | solution.py:37
  85.7 0.6 collective-permute-done.2.three_ref
  86.3 0.7 copy-done.12
  87.0 2.2 %middle.1 = (f32[264,256]{1,0:T(8,128)}, bf16[264,256]{1,0:T(8,128)(2,1)}) custom-call(s32[1]{0:T(128)} %bitcast.x_ref, bf16[264,256]{1,0:T(8,128)(2,1)} %get-tuple-element.17.own_ref, bf16[264,256]{1,0:T(8,128)(2,1)} %copy-done.10, bf16[264,256]{1,0:T(8,128)(2,1)} %copy-done.11, bf16[264,256]{1,0:T(8,128)(2,1)} %copy-done.12), custom_call_target="tpu_custom_call" | custom-call | flops 500000000 | bytes 1000000 | tf_op jit(solution)/shard_map/middle/pallas_call | solution.py:262
  89.1 1.8 %collective-permute-start.3 = (bf16[264,256]{1,0:T(8,128)(2,1)}, bf16[264,256]{1,0:T(8,128)(2,1)S(1)}, u32[]{:S(2)}, u32[]{:S(2)}) collective-permute-start(bf16[264,256]{1,0:T(8,128)(2,1)} %get-tuple-element.19), channel_id=1, source_target_pairs={{0,32},{32,64},{64,96},{1,33},{33,65},{65,97},{2,34},{34,66},{66,9... | collective-permute-start | bytes 405512 | tf_op jit(solution)/shard_map/ppermute | solution.py:37
  91.0 4.6 %collective-permute-start.4 = (bf16[264,256]{1,0:T(8,128)(2,1)}, bf16[264,256]{1,0:T(8,128)(2,1)S(1)}, u32[]{:S(2)}, u32[]{:S(2)}) collective-permute-start(bf16[264,256]{1,0:T(8,128)(2,1)} %get-tuple-element.19), channel_id=1, source_target_pairs={{0,64},{32,96},{1,65},{33,97},{2,66},{34,98},{3,67},{35,99},{4,68}... | collective-permute-start | bytes 405512 | tf_op jit(solution)/shard_map/ppermute | solution.py:37
  95.5 1.3 collective-permute-start.5
  96.8 0.9 collective-permute-start.13
  97.8 2.4 %collective-permute-start.12 = (bf16[128,2048]{1,0:T(8,128)(2,1)}, bf16[128,2048]{1,0:T(8,128)(2,1)}, u32[]{:S(2)}, u32[]{:S(2)}) collective-permute-start(bf16[128,2048]{1,0:T(8,128)(2,1)} %get-tuple-element.30), channel_id=1, source_target_pairs={{0,6},{2,0},{4,2},{6,4},{1,7},{3,1},{5,3},{7,5},{8,14},{10,8},{12,... | collective-permute-start | bytes 1572872 | tf_op jit(solution)/shard_map/ppermute | solution.py:37
  100.1 1.2 add_convert_fusion.1
  101.3 1.0 collective-permute-start.17
  102.4 0.6 copy-done.8
  103.1 5.0 %finish.1 = bf16[2048,256]{1,0:T(8,128)(2,1)} custom-call(f32[264,256]{1,0:T(8,128)} %get-tuple-element.18.before_ref, bf16[264,256]{1,0:T(8,128)(2,1)} %copy-done.7, bf16[264,256]{1,0:T(8,128)(2,1)} %copy-done.8, bf16[264,256]{1,0:T(8,128)(2,1)} %copy-done.9, f32[2048,256]{1,0:T(8,128)} %get-tuple-element.20.kept_ref, ...), custom_call_target="tpu_custom_call" | custom-call | flops 2000000000 | bytes 5242880 | tf_op jit(solution)/shard_map/finish/pallas_call | solution.py:300
  108.1 4.2 %all-to-all-start = ((bf16[8,256,256]{2,1,0:T(8,128)(2,1)}), bf16[8,256,256]{2,1,0:T(8,128)(2,1)}, u32[]{:S(2)}, u32[]{:S(2)}) async-start(bf16[8,256,256]{2,1,0:T(8,128)(2,1)} %bitcast.28), calls=%async_computation | async-start | bytes 2097152 | tf_op jit(solution)/shard_map/all_to_all | solution.py:427
  112.4 0.4 collective-permute-done.13
  112.8 10.7 %collective-permute-done.12 = bf16[128,2048]{1,0:T(8,128)(2,1)} collective-permute-done((bf16[128,2048]{1,0:T(8,128)(2,1)}, bf16[128,2048]{1,0:T(8,128)(2,1)}, u32[]{:S(2)}, u32[]{:S(2)}) %collective-permute-start.12) | collective-permute-done | bytes 524320 | tf_op jit(solution)/shard_map/ppermute | solution.py:37
  123.5 1.3 collective-permute-done.17
  124.8 2.4 %fusion = bf16[16,8,2048]{2,1,0:T(8,128)(2,1)} fusion(bf16[128,2048]{1,0:T(8,128)(2,1)S(1)} %collective-permute-done.17, bf16[128,2048]{1,0:T(8,128)(2,1)} %collective-permute-done.13, bf16[128,2048]{1,0:T(8,128)(2,1)} %collective-permute-done.12, bf16[128,2048]{1,0:T(8,128)(2,1)S(1)} %get-tuple-element.23, bf16[384,2048]{1,0:T(8,128)(2,1)S(1)} %collective-permute-done.11), kind=kLoop, calls=%fused_computation.5 | loop fusion | flops 3145728 | bytes 3145728 | tf_op jit(solution)/shard_map/all_to_all | solution.py:430
  127.2 6.6 %all-to-all-done = bf16[8,256,256]{2,1,0:T(8,128)(2,1)} async-done(((bf16[8,256,256]{2,1,0:T(8,128)(2,1)}), bf16[8,256,256]{2,1,0:T(8,128)(2,1)}, u32[]{:S(2)}, u32[]{:S(2)}) %all-to-all-start) | async-done | bytes 1048608 | tf_op jit(solution)/shard_map/all_to_all | solution.py:427
  133.9 4.8 %all-to-all-start.2 = ((bf16[16,8,2048]{2,1,0:T(8,128)(2,1)}), bf16[16,8,2048]{2,1,0:T(8,128)(2,1)S(1)}, u32[]{:S(2)}, u32[]{:S(2)}) async-start(bf16[16,8,2048]{2,1,0:T(8,128)(2,1)} %fusion), calls=%async_computation.2 | async-start | bytes 1048576 | tf_op jit(solution)/shard_map/all_to_all | solution.py:430
  138.7 8.7 %project.1 = bf16[256,2048]{1,0:T(8,128)(2,1)} custom-call(bf16[2048,256]{1,0:T(8,128)(2,1)} %bitcast.7.rows_ref, bf16[2048,2048]{1,0:T(8,128)(2,1)} %w_ref.1), custom_call_target="tpu_custom_call" | custom-call | flops 4000000000 | bytes 10485760 | tf_op jit(solution)/shard_map/project/pallas_call | solution.py:330
  147.4 1.4 all-to-all-done.2
  148.8 0.8 copy-done.4
  149.6 2.3 %combine.1 = bf16[32,2048]{1,0:T(8,128)(2,1)} custom-call(bf16[128,2048]{1,0:T(8,128)(2,1)} %bitcast.30, s32[2,32]{1,0:T(2,128)} %bitcast.36, f32[2,32]{1,0:T(2,128)} %bitcast.37), custom_call_target="tpu_custom_call" | custom-call | flops 1000000000 | bytes 1000000 | tf_op jit(solution)/shard_map/combine/pallas_call | solution.py:432
  (35 shorter events, 0.5 us)
Async XLA Ops:
  0.6 10.4 %copy-start.5 = (f32[128]{0:T(128)S(1)}, f32[128]{0:T(128)}, u32[]{:S(2)}) copy-start(f32[128]{0:T(128)} %constant.21.clone) | copy-start | bytes 1540
  2.9 19.5 %all-to-all-start.1 = ((bf16[16,8,2048]{2,1,0:T(8,128)(2,1)}), bf16[16,8,2048]{2,1,0:T(8,128)(2,1)S(1)}, u32[]{:S(2)}, u32[]{:S(2)}) async-start(bf16[16,8,2048]{2,1,0:T(8,128)(2,1)} %bitcast.29), calls=%async_computation.1 | async-start | bytes 1048576 | tf_op jit(solution)/shard_map/all_to_all | solution.py:382
  22.4 13.5 %collective-permute-start.6 = (bf16[128,2048]{1,0:T(8,128)(2,1)S(1)}, bf16[128,2048]{1,0:T(8,128)(2,1)S(1)}, u32[]{:S(2)}, u32[]{:S(2)}) collective-permute-start(bf16[128,2048]{1,0:T(8,128)(2,1)S(1)} %bitcast.23), channel_id=1, source_target_pairs={{0,2},{2,4},{4,6},{6,0},{1,3},{3,5},{5,7},{7,1},{8,10},{10,12},{12... | collective-permute-start | bytes 1572872 | tf_op jit(solution)/shard_map/ppermute | solution.py:37
  24.0 12.0 %collective-permute-start.7 = (bf16[128,2048]{1,0:T(8,128)(2,1)S(1)}, bf16[128,2048]{1,0:T(8,128)(2,1)S(1)}, u32[]{:S(2)}, u32[]{:S(2)}) collective-permute-start(bf16[128,2048]{1,0:T(8,128)(2,1)S(1)} %bitcast.24), channel_id=1, source_target_pairs={{0,6},{2,0},{4,2},{6,4},{1,7},{3,1},{5,3},{7,5},{8,14},{10,8},{12,... | collective-permute-start | bytes 1572872 | tf_op jit(solution)/shard_map/ppermute | solution.py:37
  25.7 10.8 %collective-permute-start.8 = (bf16[128,2048]{1,0:T(8,128)(2,1)S(1)}, bf16[128,2048]{1,0:T(8,128)(2,1)S(1)}, u32[]{:S(2)}, u32[]{:S(2)}) collective-permute-start(bf16[128,2048]{1,0:T(8,128)(2,1)S(1)} %bitcast.25), channel_id=1, source_target_pairs={{0,1},{1,0},{2,3},{3,2},{4,5},{5,4},{6,7},{7,6},{8,9},{9,8},{10,11... | collective-permute-start | bytes 1572872 | tf_op jit(solution)/shard_map/ppermute | solution.py:37
  36.0 1.9 %collective-permute-start.9 = (bf16[128,2048]{1,0:T(8,128)(2,1)S(1)}, bf16[128,2048]{1,0:T(8,128)(2,1)S(1)}, u32[]{:S(2)}, u32[]{:S(2)}) collective-permute-start(bf16[128,2048]{1,0:T(8,128)(2,1)S(1)} %collective-permute-done.6.refs_1_), channel_id=1, source_target_pairs={{0,1},{1,0},{2,3},{3,2},{4,5},{5,4},{6,7},{7,6},{8,9},{9,8},{10,11... | collective-permute-start | bytes 1572872 | tf_op jit(solution)/shard_map/ppermute | solution.py:37
  36.0 2.6 %collective-permute-start.10 = (bf16[128,2048]{1,0:T(8,128)(2,1)S(1)}, bf16[128,2048]{1,0:T(8,128)(2,1)S(1)}, u32[]{:S(2)}, u32[]{:S(2)}) collective-permute-start(bf16[128,2048]{1,0:T(8,128)(2,1)S(1)} %collective-permute-done.7.refs_2_), channel_id=1, source_target_pairs={{0,1},{1,0},{2,3},{3,2},{4,5},{5,4},{6,7},{7,6},{8,9},{9,8},{10,11... | collective-permute-start | bytes 1572872 | tf_op jit(solution)/shard_map/ppermute | solution.py:37
  38.6 2.0 %copy-start = (bf16[1,2048,896]{2,1,0:T(8,128)(2,1)S(1)}, bf16[1,2048,896]{2,1,0:T(8,128)(2,1)}, u32[]{:S(2)}) copy-start(bf16[1,2048,896]{2,1,0:T(8,128)(2,1)} %param.28) | copy-start | bytes 11010052
  40.7 2.0 %copy-start.2 = (bf16[1,2048,896]{2,1,0:T(8,128)(2,1)S(1)}, bf16[1,2048,896]{2,1,0:T(8,128)(2,1)}, u32[]{:S(2)}) copy-start(bf16[1,2048,896]{2,1,0:T(8,128)(2,1)} %param.29) | copy-start | bytes 11010052
  42.7 2.0 %copy-start.3 = (bf16[1,896,2048]{2,1,0:T(8,128)(2,1)S(1)}, bf16[1,896,2048]{2,1,0:T(8,128)(2,1)}, u32[]{:S(2)}) copy-start(bf16[1,896,2048]{2,1,0:T(8,128)(2,1)} %param.30) | copy-start | bytes 11010052
  44.8 27.4 %copy-start.1 = (bf16[1,2048,896]{2,1,0:T(8,128)(2,1)S(1)}, bf16[1,2048,896]{2,1,0:T(8,128)(2,1)}, u32[]{:S(2)}) copy-start(bf16[1,2048,896]{2,1,0:T(8,128)(2,1)} %param.28) | copy-start | bytes 11010052
  54.3 15.9 %collective-permute-start.11 = (bf16[384,2048]{1,0:T(8,128)(2,1)S(1)}, bf16[384,2048]{1,0:T(8,128)(2,1)S(1)}, u32[]{:S(2)}, u32[]{:S(2)}) collective-permute-start(bf16[384,2048]{1,0:T(8,128)(2,1)S(1)} %get-tuple-element.24), channel_id=1, source_target_pairs={{0,1},{1,0},{2,3},{3,2},{4,5},{5,4},{6,7},{7,6},{8,9},{9,8},{10,11... | collective-permute-start | bytes 4718600 | tf_op jit(solution)/shard_map/ppermute | solution.py:37
  54.6 15.7 %collective-permute-start.14 = (bf16[128,2048]{1,0:T(8,128)(2,1)S(1)}, bf16[128,2048]{1,0:T(8,128)(2,1)S(1)}, u32[]{:S(2)}, u32[]{:S(2)}) collective-permute-start(bf16[128,2048]{1,0:T(8,128)(2,1)S(1)} %bitcast.27), channel_id=1, source_target_pairs={{0,4},{2,6},{4,0},{6,2},{1,5},{3,7},{5,1},{7,3},{8,12},{10,14},{12... | collective-permute-start | bytes 1572872 | tf_op jit(solution)/shard_map/ppermute | solution.py:37
  70.3 1.9 %collective-permute-start.15 = (bf16[128,2048]{1,0:T(8,128)(2,1)S(1)}, bf16[128,2048]{1,0:T(8,128)(2,1)S(1)}, u32[]{:S(2)}, u32[]{:S(2)}) collective-permute-start(bf16[128,2048]{1,0:T(8,128)(2,1)S(1)} %collective-permute-done.14.refs_0_), channel_id=1, source_target_pairs={{0,1},{1,0},{2,3},{3,2},{4,5},{5,4},{6,7},{7,6},{8,9},{9,8},{10,11... | collective-permute-start | bytes 1572872 | tf_op jit(solution)/shard_map/ppermute | solution.py:37
  71.7 4.0 %copy-start.6 = (bf16[264,256]{1,0:T(8,128)(2,1)S(1)}, bf16[264,256]{1,0:T(8,128)(2,1)}, u32[]{:S(2)}) copy-start(bf16[264,256]{1,0:T(8,128)(2,1)} %get-tuple-element.17.own_ref) | copy-start | bytes 405508
  75.5 22.3 %collective-permute-start.16 = (bf16[128,2048]{1,0:T(8,128)(2,1)S(1)}, bf16[128,2048]{1,0:T(8,128)(2,1)}, u32[]{:S(2)}, u32[]{:S(2)}) collective-permute-start(bf16[128,2048]{1,0:T(8,128)(2,1)S(1)} %get-tuple-element.29), channel_id=1, source_target_pairs={{0,1},{1,0},{2,3},{3,2},{4,5},{5,4},{6,7},{7,6},{8,9},{9,8},{10,11... | collective-permute-start | bytes 1572872 | tf_op jit(solution)/shard_map/ppermute | solution.py:37
  75.7 10.0 %collective-permute-start = (bf16[264,256]{1,0:T(8,128)(2,1)S(1)}, bf16[264,256]{1,0:T(8,128)(2,1)S(1)}, u32[]{:S(2)}, u32[]{:S(2)}) collective-permute-start(bf16[264,256]{1,0:T(8,128)(2,1)S(1)} %copy-done.6), channel_id=1, source_target_pairs={{0,8},{8,16},{16,24},{24,0},{1,9},{9,17},{17,25},{25,1},{2,10},{10... | collective-permute-start | bytes 405512 | tf_op jit(solution)/shard_map/ppermute | solution.py:37
  76.3 9.4 %collective-permute-start.1 = (bf16[264,256]{1,0:T(8,128)(2,1)S(1)}, bf16[264,256]{1,0:T(8,128)(2,1)S(1)}, u32[]{:S(2)}, u32[]{:S(2)}) collective-permute-start(bf16[264,256]{1,0:T(8,128)(2,1)S(1)} %copy-done.6), channel_id=1, source_target_pairs={{0,16},{8,24},{16,0},{24,8},{1,17},{9,25},{17,1},{25,9},{2,18},{10... | collective-permute-start | bytes 405512 | tf_op jit(solution)/shard_map/ppermute | solution.py:37
  78.0 8.3 %collective-permute-start.2 = (bf16[264,256]{1,0:T(8,128)(2,1)S(1)}, bf16[264,256]{1,0:T(8,128)(2,1)S(1)}, u32[]{:S(2)}, u32[]{:S(2)}) collective-permute-start(bf16[264,256]{1,0:T(8,128)(2,1)S(1)} %copy-done.6), channel_id=1, source_target_pairs={{0,24},{8,0},{16,8},{24,16},{1,25},{9,1},{17,9},{25,17},{2,26},{10... | collective-permute-start | bytes 405512 | tf_op jit(solution)/shard_map/ppermute | solution.py:37
  85.7 1.3 copy-start.10
  85.7 1.3 copy-start.11
  86.3 0.7 copy-start.12
  89.1 12.2 %collective-permute-start.3 = (bf16[264,256]{1,0:T(8,128)(2,1)}, bf16[264,256]{1,0:T(8,128)(2,1)S(1)}, u32[]{:S(2)}, u32[]{:S(2)}) collective-permute-start(bf16[264,256]{1,0:T(8,128)(2,1)} %get-tuple-element.19), channel_id=1, source_target_pairs={{0,32},{32,64},{64,96},{1,33},{33,65},{65,97},{2,34},{34,66},{66,9... | collective-permute-start | bytes 405512 | tf_op jit(solution)/shard_map/ppermute | solution.py:37
  91.0 11.4 %collective-permute-start.4 = (bf16[264,256]{1,0:T(8,128)(2,1)}, bf16[264,256]{1,0:T(8,128)(2,1)S(1)}, u32[]{:S(2)}, u32[]{:S(2)}) collective-permute-start(bf16[264,256]{1,0:T(8,128)(2,1)} %get-tuple-element.19), channel_id=1, source_target_pairs={{0,64},{32,96},{1,65},{33,97},{2,66},{34,98},{3,67},{35,99},{4,68}... | collective-permute-start | bytes 405512 | tf_op jit(solution)/shard_map/ppermute | solution.py:37
  95.5 6.9 %collective-permute-start.5 = (bf16[264,256]{1,0:T(8,128)(2,1)}, bf16[264,256]{1,0:T(8,128)(2,1)S(1)}, u32[]{:S(2)}, u32[]{:S(2)}) collective-permute-start(bf16[264,256]{1,0:T(8,128)(2,1)} %get-tuple-element.19), channel_id=1, source_target_pairs={{0,96},{1,97},{2,98},{3,99},{4,100},{5,101},{6,102},{7,103},{8,104... | collective-permute-start | bytes 405512 | tf_op jit(solution)/shard_map/ppermute | solution.py:37
  96.8 16.0 %collective-permute-start.13 = (bf16[128,2048]{1,0:T(8,128)(2,1)}, bf16[128,2048]{1,0:T(8,128)(2,1)}, u32[]{:S(2)}, u32[]{:S(2)}) collective-permute-start(bf16[128,2048]{1,0:T(8,128)(2,1)} %get-tuple-element.31), channel_id=1, source_target_pairs={{0,2},{2,4},{4,6},{6,0},{1,3},{3,5},{5,7},{7,1},{8,10},{10,12},{12... | collective-permute-start | bytes 1572872 | tf_op jit(solution)/shard_map/ppermute | solution.py:37
  97.8 25.8 %collective-permute-start.12 = (bf16[128,2048]{1,0:T(8,128)(2,1)}, bf16[128,2048]{1,0:T(8,128)(2,1)}, u32[]{:S(2)}, u32[]{:S(2)}) collective-permute-start(bf16[128,2048]{1,0:T(8,128)(2,1)} %get-tuple-element.30), channel_id=1, source_target_pairs={{0,6},{2,0},{4,2},{6,4},{1,7},{3,1},{5,3},{7,5},{8,14},{10,8},{12,... | collective-permute-start | bytes 1572872 | tf_op jit(solution)/shard_map/ppermute | solution.py:37
  101.3 1.1 copy-start.7
  101.3 23.5 %collective-permute-start.17 = (bf16[128,2048]{1,0:T(8,128)(2,1)S(1)}, bf16[128,2048]{1,0:T(8,128)(2,1)S(1)}, u32[]{:S(2)}, u32[]{:S(2)}) collective-permute-start(bf16[128,2048]{1,0:T(8,128)(2,1)S(1)} %add_convert_fusion.1), channel_id=1, source_target_pairs={{0,4},{2,6},{4,0},{6,2},{1,5},{3,7},{5,1},{7,3},{8,12},{10,14},{12... | collective-permute-start | bytes 1572872 | tf_op jit(solution)/shard_map/ppermute | solution.py:37
  102.4 0.7 copy-start.8
  102.4 0.7 copy-start.9
  108.1 25.7 %all-to-all-start = ((bf16[8,256,256]{2,1,0:T(8,128)(2,1)}), bf16[8,256,256]{2,1,0:T(8,128)(2,1)}, u32[]{:S(2)}, u32[]{:S(2)}) async-start(bf16[8,256,256]{2,1,0:T(8,128)(2,1)} %bitcast.28), calls=%async_computation | async-start | bytes 2097152 | tf_op jit(solution)/shard_map/all_to_all | solution.py:427
  133.9 15.0 %all-to-all-start.2 = ((bf16[16,8,2048]{2,1,0:T(8,128)(2,1)}), bf16[16,8,2048]{2,1,0:T(8,128)(2,1)S(1)}, u32[]{:S(2)}, u32[]{:S(2)}) async-start(bf16[16,8,2048]{2,1,0:T(8,128)(2,1)} %fusion), calls=%async_computation.2 | async-start | bytes 1048576 | tf_op jit(solution)/shard_map/all_to_all | solution.py:430
  148.8 0.8 copy-start.4

commit v5 on v4

--- a/solution.py
+++ b/solution.py
@@ -19,7 +19,7 @@
 norm_eps = 1e-06
 
 
-FFN_VMEM = 30 * 2**20
+MIB = 2**20
 
 f32 = jnp.float32
 bf16 = jnp.bfloat16
@@ -39,6 +39,12 @@
 
 def vm(x):
     return pltpu.with_memory_space_constraint(x, pltpu.VMEM)
+
+
+def grid_params(mib):
+    return pltpu.CompilerParams(
+        dimension_semantics=("arbitrary",), vmem_limit_bytes=mib * MIB
+    )
 
 
 def after(x, *earlier):
@@ -123,17 +129,28 @@
         in_specs=[in_vmem] * (n_x + 3),
         out_specs=[in_vmem] * (len(keep) + 1),
         scratch_shapes=[pltpu.VMEM((rows, ff), bf16)],
-        compiler_params=pltpu.CompilerParams(vmem_limit_bytes=FFN_VMEM),
+        compiler_params=pltpu.CompilerParams(vmem_limit_bytes=30 * MIB),
         cost_estimate=pl.CostEstimate(
             flops=6 * rows * width * ff,
             bytes_accessed=2 * (3 * width * ff + 2 * rows * width),
             transcendentals=rows * ff,
         ),
-    )(*[vm(x) for x in (*keep, *give)], *[vm(w) for w in weights])
+    )(*[vm(x) for x in (*keep, *give)], *weights)
 
 
 def local_kernel(
-    base_ref, q_ref, k_ref, v_ref, ld_ref, cos_ref, sin_ref, kept_ref, qd_ref, send_ref, state, before
+    base_ref,
+    q_ref,
+    k_ref,
+    v_ref,
+    ld_ref,
+    cos_ref,
+    sin_ref,
+    kept_ref,
+    qd_ref,
+    send_ref,
+    state,
+    before,
 ):
     b = pl.program_id(0)
 
@@ -224,8 +241,11 @@
             table,
         ],
         out_specs=[seq, seq, pl.BlockSpec((HEAD_DIM + 8, HEAD_DIM), lambda b: (0, 0))],
-        scratch_shapes=[pltpu.VMEM((HEAD_DIM, HEAD_DIM), f32), pltpu.VMEM((8, HALF), f32)],
-        compiler_params=pltpu.CompilerParams(dimension_semantics=("arbitrary",)),
+        scratch_shapes=[
+            pltpu.VMEM((HEAD_DIM, HEAD_DIM), f32),
+            pltpu.VMEM((8, HALF), f32),
+        ],
+        compiler_params=grid_params(16),
         cost_estimate=pl.CostEstimate(
             flops=6 * 10**9, bytes_accessed=6 * 2**20, transcendentals=2**20
         ),
@@ -268,15 +288,26 @@
         in_specs=[pl.BlockSpec(memory_space=pltpu.SMEM)]
         + [pl.BlockSpec(memory_space=pltpu.VMEM)] * 4,
         out_specs=[pl.BlockSpec(memory_space=pltpu.VMEM)] * 2,
+        compiler_params=pltpu.CompilerParams(vmem_limit_bytes=8 * MIB),
         cost_estimate=pl.CostEstimate(
-            flops=5 * 10**8, bytes_accessed=10**6, transcendentals=0
+            flops=2 * 10**10, bytes_accessed=10**6, transcendentals=0
         ),
         name="middle",
     )(x, own, one, two, three)
 
 
 def finish_kernel(
-    before_ref, one_ref, two_ref, three_ref, kept_ref, qd_ref, gate_ref, gain_ref, out_ref, start
+    place_ref,
+    before_ref,
+    one_ref,
+    two_ref,
+    three_ref,
+    kept_ref,
+    qd_ref,
+    gate_ref,
+    gain_ref,
+    out_ref,
+    start,
 ):
     @pl.when(pl.program_id(0) == 0)
     def _():
@@ -290,58 +321,69 @@
     scale = lax.rsqrt(jnp.mean(retained * retained, axis=-1, keepdims=True) + norm_eps)
     gate = gate_ref[...].astype(f32)
     gate = gate / (1.0 + jnp.exp(-gate))
-    out_ref[...] = (gate * retained * scale * gain_ref[...]).astype(bf16)
-
-
-def finish(before, one, two, three, kept, qd, gate, gain):
+    done = (gate * retained * scale * gain_ref[...]).astype(bf16)
+    rows = BLOCK // 2
+    for c in range(2):
+        other = lax.rem(place_ref[1] + c, 2)
+        out_ref[pl.ds(pl.multiple_of(other * rows, rows), rows), :] = done[c * rows : (c + 1) * rows]
+
+
+def finish(place, before, one, two, three, kept, qd, gate, gain):
     rows = qd.shape[0]
-    seq = pl.BlockSpec((BLOCK, HEAD_DIM), lambda b: (b, 0))
-    whole = pl.BlockSpec((HEAD_DIM + 8, HEAD_DIM), lambda b: (0, 0))
+    seq = pl.BlockSpec((BLOCK, HEAD_DIM), lambda b, place: (b, 0))
+    whole = pl.BlockSpec((HEAD_DIM + 8, HEAD_DIM), lambda b, place: (0, 0))
     return pl.pallas_call(
         finish_kernel,
-        grid=(rows // BLOCK,),
+        grid_spec=pltpu.PrefetchScalarGridSpec(
+            num_scalar_prefetch=1,
+            grid=(rows // BLOCK,),
+            in_specs=[whole] * 4
+            + [seq] * 3
+            + [pl.BlockSpec((1, HEAD_DIM), lambda b, place: (0, 0))],
+            out_specs=pl.BlockSpec(
+                (BLOCK, HEAD_DIM), lambda b, place: (lax.rem(b - place[0] + 4, 4), 0)
+            ),
+            scratch_shapes=[pltpu.VMEM((HEAD_DIM, HEAD_DIM), bf16)],
+        ),
         out_shape=jax.ShapeDtypeStruct((rows, HEAD_DIM), bf16),
-        in_specs=[whole] * 4 + [seq] * 3 + [pl.BlockSpec((1, HEAD_DIM), lambda b: (0, 0))],
-        out_specs=seq,
-        scratch_shapes=[pltpu.VMEM((HEAD_DIM, HEAD_DIM), bf16)],
-        compiler_params=pltpu.CompilerParams(dimension_semantics=("arbitrary",)),
+        compiler_params=grid_params(12),
         cost_estimate=pl.CostEstimate(
             flops=2 * 10**9, bytes_accessed=5 * 2**20, transcendentals=2**19
         ),
         name="finish",
-    )(before, one, two, three, kept, qd, gate, gain)
-
-
-def project_kernel(rows_ref, w_ref, out_ref):
-    parts = w_ref.shape[0] // HEAD_DIM
-    rows = rows_ref.shape[0] // parts
+    )(place, before, one, two, three, kept, qd, gate, gain)
+
+
+def project_kernel(head_ref, *refs):
+    pieces, w_ref, out_ref = refs[:-2], refs[-2], refs[-1]
     total = None
-    for s in range(parts):
-        at = s * HEAD_DIM
-        part = mm(rows_ref[s * rows : (s + 1) * rows, :], w_ref[at : at + HEAD_DIM, :])
+    for s, piece in enumerate(pieces):
+        at = pl.multiple_of(head_ref[s] * HEAD_DIM, HEAD_DIM)
+        part = mm(piece[...], w_ref[pl.ds(at, HEAD_DIM), :])
         total = part if total is None else total + part
     out_ref[...] = total.astype(bf16)
 
 
-def project(pieces, w_out):
+def project(heads, pieces, w_out):
     whole, width = w_out.shape
-    rows = pieces.shape[0] * HEAD_DIM // whole
+    rows = pieces[0].shape[0]
     cols = 256
     return pl.pallas_call(
         project_kernel,
-        grid=(width // cols,),
+        grid_spec=pltpu.PrefetchScalarGridSpec(
+            num_scalar_prefetch=1,
+            grid=(width // cols,),
+            in_specs=[pl.BlockSpec((rows, HEAD_DIM), lambda n, heads: (0, 0))] * len(pieces)
+            + [pl.BlockSpec((whole, cols), lambda n, heads: (0, n))],
+            out_specs=pl.BlockSpec((rows, cols), lambda n, heads: (0, n)),
+        ),
         out_shape=jax.ShapeDtypeStruct((rows, width), bf16),
-        in_specs=[
-            pl.BlockSpec(pieces.shape, lambda n: (0, 0)),
-            pl.BlockSpec((whole, cols), lambda n: (0, n)),
-        ],
-        out_specs=pl.BlockSpec((rows, cols), lambda n: (0, n)),
-        compiler_params=pltpu.CompilerParams(dimension_semantics=("arbitrary",)),
+        compiler_params=grid_params(12),
         cost_estimate=pl.CostEstimate(
             flops=4 * 10**9, bytes_accessed=10 * 2**20, transcendentals=0
         ),
         name="project",
-    )(pieces, w_out)
+    )(heads, *pieces, w_out)
 
 
 def angle_tables():
@@ -376,6 +418,7 @@
     outgoing = pl.pallas_call(
         pre_kernel,
         out_shape=jax.ShapeDtypeStruct((SLOTS, width), bf16),
+        compiler_params=pltpu.CompilerParams(vmem_limit_bytes=8 * MIB),
         cost_estimate=pl.CostEstimate(flops=2 * 10**9, bytes_accessed=10**6, transcendentals=0),
         name="pre",
     )(moe_in, ids, moe_gain.reshape(1, -1))
@@ -407,8 +450,8 @@
     by_z = [shift(whole, "z", s, wrap=False) for s in (1, 2, 3)]
     up_c = shift(up, "core", 1, 2)
     down_c = shift(down, "core", 1, 2)
+    n = own.shape[0]
     weights = (w_gate[0], w_up[0], w_down[0])
-    n = own.shape[0]
     *keep, give1 = ffn([own, up, down], [own_c, up_c, down_c], weights)
     got1 = shift(give1, "core", 1, 2)
     far_c = shift(far, "core", 1, 2)
@@ -421,17 +464,34 @@
     keep2, give2 = ffn([after(far, near[2])], [far_c], weights)
     got2 = shift(give2, "core", 1, 2)
     back_far = shift((keep2.astype(f32) + got2.astype(f32)).astype(bf16), "y", 2)
+    y_index, c_index = lax.axis_index("y"), lax.axis_index("core")
+    place = jnp.stack([y_index, c_index]).astype(jnp.int32)
     heads_out = finish(
-        before, *by_z, kept, qd, mix_gate, ret_gain.reshape(1, -1)
+        place, before, *by_z, kept, qd, mix_gate, ret_gain.reshape(1, -1)
     )
-    pieces = lax.all_to_all(heads_out, tp, split_axis=0, concat_axis=0, tiled=True)
+    pieces, sources = [], []
+    m = seq_rows // 8
+    for dy in range(4):
+        for dc in range(2):
+            at = (2 * dy + dc) * m
+            piece = heads_out[at : at + m]
+            if dy or dc:
+                pairs = [
+                    (2 * y + c, 2 * ((y + dy) % 4) + (c + dc) % 2)
+                    for y in range(4)
+                    for c in range(2)
+                ]
+                piece = lax.ppermute(piece, tp, pairs)
+            pieces.append(piece)
+            sources.append(2 * lax.rem(y_index - dy + 4, 4) + lax.rem(c_index + dc, 2))
     parts = (near[0], back_up, back_down, back_far)
     expert_rows = sum(v.astype(f32) for v in parts).astype(bf16)
     returned = lax.all_to_all(expert_rows, ep, split_axis=0, concat_axis=0, tiled=True)
-    mix_out = project(pieces, w_out)
+    mix_out = project(jnp.stack(sources).astype(jnp.int32), pieces, w_out)
     moe_out = pl.pallas_call(
         combine_kernel,
         out_shape=jax.ShapeDtypeStruct(moe_in.shape, bf16),
+        compiler_params=pltpu.CompilerParams(vmem_limit_bytes=8 * MIB),
         cost_estimate=pl.CostEstimate(flops=10**9, bytes_accessed=10**6, transcendentals=0),
         name="combine",
     )(returned, ids, route_weights.T)

time: 153 us -> 149 us (0.974)
  local copies, waits for them, and re-layouts: 8.32 us -> 21.7 us
  Pallas kernels: 39.8 us -> 29 us
  waiting for transfers between devices: 58.4 us -> 50.4 us
    ppermute x0 -> x7, waiting for transfers between devices: none -> 23.3 us  [on_device(): piece = lax.ppermute(piece, tp, pairs)]
    ppermute x18, waiting for transfers between devices: 46.2 us -> 22.9 us  [shift(): return lax.ppermute(x, axis, pairs)]
    unnamed x26 -> x50, local copies, waits for them, and re-layouts: 8.25 us -> 21.5 us
    all_to_all x1 -> x0, waiting for transfers between devices: 6.63 us -> none  [on_device(): lax.all_to_all(heads_out, tp, split_axis=0, concat_axis=0, tiled=True)]
    ppermute x0 -> x7, starting transfers between devices: none -> 6.53 us  [on_device(): piece = lax.ppermute(piece, tp, pairs)]
    pallas_call x2, Pallas kernels: 13.7 us -> 8.47 us  [the longest x1 6.17 us: project(): pl.pallas_call(project_kernel, grid_spec=pltpu.PrefetchScalarGridSpec(num...]
    all_to_all x1 -> x0, starting transfers between devices: 4.23 us -> none  [on_device(): lax.all_to_all(heads_out, tp, split_axis=0, concat_axis=0, tiled=True)]
    pallas_call x1, Pallas kernels: 6.55 us -> 3.6 us  [local_part(): pl.pallas_call(local_kernel, grid=(blocks,), out_shape=[jax.ShapeDtypeStr...]
  transfers between devices with their start and end apart: 21 -> 27, of which waited for: 13 -> 10; matrix products, arithmetic and copies ran while one was open for 4% -> 3% of each run, Pallas kernels for 15% -> 11%
where the time goes in v5:
time: 149 us; the launch traced here: 146 us
  waiting for transfers between devices  50.4 us (34%)
  starting transfers between devices  40.2 us (27%)
  Pallas kernels  29 us (19%)
  local copies, waits for them, and re-layouts  21.7 us (15%)
  other arithmetic  4.15 us (3%)
    ppermute x7, waiting for transfers between devices, on_device(): piece = lax.ppermute(piece, tp, pairs)  23.3 us
    ppermute x18, waiting for transfers between devices, shift(): return lax.ppermute(x, axis, pairs)  22.9 us
    ppermute x18, starting transfers between devices, shift(): return lax.ppermute(x, axis, pairs)  22.2 us
    unnamed x50, local copies, waits for them, and re-layouts  21.5 us
    pallas_call x2, Pallas kernels, ffn(): pl.pallas_call(functools.partial(ffn_kernel, n_x), out_shape=[pltpu.VMEM(...  14.1 us
    all_to_all x1, starting transfers between devices, on_device(): own = lax.all_to_all(outgoing, ep, split_axis=0, concat_axis=0, tiled=True)  7.99 us
    ppermute x7, starting transfers between devices, on_device(): piece = lax.ppermute(piece, tp, pairs)  6.53 us
    pallas_call x1, Pallas kernels, project(): pl.pallas_call(project_kernel, grid_spec=pltpu.PrefetchScalarGridSpec(num...  6.17 us
  transfers between devices with their start and end apart: 27, of which 10 were waited for; matrix products, arithmetic and copies ran while one was open for 3% of the time, Pallas kernels for 11%

profile of v5, /device:TPU:0, one launch (start us, length us, event | category | flops | bytes accessed | tf_op | source)
XLA Modules:
  0.0 146.4 jit_solution(1703037907501987104)
XLA Ops:
  0.6 0.9 copy-done.11
  1.5 0.7 copy-done.12
  2.2 0.7 copy-done.15
  2.9 1.3 pre.1
  4.3 8.0 %all-to-all-start = ((bf16[16,8,2048]{2,1,0:T(8,128)(2,1)}), bf16[16,8,2048]{2,1,0:T(8,128)(2,1)S(1)}, u32[]{:S(2)}, u32[]{:S(2)}) async-start(bf16[16,8,2048]{2,1,0:T(8,128)(2,1)} %bitcast.16), calls=%async_computation | async-start | bytes 1048576 | tf_op jit(solution)/shard_map/all_to_all | solution.py:425
  12.5 1.2 copy-done.9
  13.7 3.6 %local.1 = (f32[2048,256]{1,0:T(8,128)S(1)}, bf16[2048,256]{1,0:T(8,128)(2,1)S(1)}, bf16[264,256]{1,0:T(8,128)(2,1)S(1)}) custom-call(f32[4,2,128]{2,1,0:T(2,128)S(1)} %pad_maximum_fusion.base_ref, bf16[2048,256]{1,0:T(8,128)(2,1)S(1)} %copy-done.7, bf16[2048,256]{1,0:T(8,128)(2,1)S(1)} %copy-done.8, bf16[2048,256]{1,0:T(8,128)(2,1)S(1)} %copy-done.9, ...), custom_call_target="tpu_custom_call" | custom-call | flops 6000000000 | bytes 6291456 | tf_op jit(solution)/shard_map/local/pallas_call | solution.py:226
  17.4 1.3 copy-done.20
  18.7 1.0 copy-done.22
  19.7 4.1 %all-to-all-done = bf16[16,8,2048]{2,1,0:T(8,128)(2,1)S(1)} async-done(((bf16[16,8,2048]{2,1,0:T(8,128)(2,1)}), bf16[16,8,2048]{2,1,0:T(8,128)(2,1)S(1)}, u32[]{:S(2)}, u32[]{:S(2)}) %all-to-all-start) | async-done | bytes 524320 | tf_op jit(solution)/shard_map/all_to_all | solution.py:425
  23.8 1.6 %collective-permute-start.13 = (bf16[128,2048]{1,0:T(8,128)(2,1)S(1)}, bf16[128,2048]{1,0:T(8,128)(2,1)S(1)}, u32[]{:S(2)}, u32[]{:S(2)}) collective-permute-start(bf16[128,2048]{1,0:T(8,128)(2,1)S(1)} %bitcast.32), channel_id=1, source_target_pairs={{0,2},{2,4},{4,6},{6,0},{1,3},{3,5},{5,7},{7,1},{8,10},{10,12},{12... | collective-permute-start | bytes 1572872 | tf_op jit(solution)/shard_map/ppermute | solution.py:37
  25.4 1.7 %collective-permute-start.14 = (bf16[128,2048]{1,0:T(8,128)(2,1)S(1)}, bf16[128,2048]{1,0:T(8,128)(2,1)S(1)}, u32[]{:S(2)}, u32[]{:S(2)}) collective-permute-start(bf16[128,2048]{1,0:T(8,128)(2,1)S(1)} %bitcast.33), channel_id=1, source_target_pairs={{0,6},{2,0},{4,2},{6,4},{1,7},{3,1},{5,3},{7,5},{8,14},{10,8},{12,... | collective-permute-start | bytes 1572872 | tf_op jit(solution)/shard_map/ppermute | solution.py:37
  27.1 10.3 %collective-permute-done.13.refs_1_ = bf16[128,2048]{1,0:T(8,128)(2,1)S(1)} collective-permute-done((bf16[128,2048]{1,0:T(8,128)(2,1)S(1)}, bf16[128,2048]{1,0:T(8,128)(2,1)S(1)}, u32[]{:S(2)}, u32[]{:S(2)}) %collective-permute-start.13) | collective-permute-done | bytes 524320 | tf_op jit(solution)/shard_map/ppermute | solution.py:37
  37.9 1.4 collective-permute-done.16.refs_4_
  39.3 0.7 collective-permute-done.17.refs_5_
  40.0 2.0 %copy-done = bf16[1,2048,896]{2,1,0:T(8,128)(2,1)S(1)} copy-done((bf16[1,2048,896]{2,1,0:T(8,128)(2,1)S(1)}, bf16[1,2048,896]{2,1,0:T(8,128)(2,1)}, u32[]{:S(2)}) %copy-start) | copy-done | bytes 3670040
  42.1 2.0 %copy-done.2 = bf16[1,2048,896]{2,1,0:T(8,128)(2,1)S(1)} copy-done((bf16[1,2048,896]{2,1,0:T(8,128)(2,1)S(1)}, bf16[1,2048,896]{2,1,0:T(8,128)(2,1)}, u32[]{:S(2)}) %copy-start.2) | copy-done | bytes 3670040
  44.1 2.0 %copy-done.4 = bf16[1,896,2048]{2,1,0:T(8,128)(2,1)S(1)} copy-done((bf16[1,896,2048]{2,1,0:T(8,128)(2,1)S(1)}, bf16[1,896,2048]{2,1,0:T(8,128)(2,1)}, u32[]{:S(2)}) %copy-start.4) | copy-done | bytes 3670040
  46.1 10.8 %shard_map.176 = (bf16[128,2048]{1,0:T(8,128)(2,1)S(1)}, bf16[128,2048]{1,0:T(8,128)(2,1)S(1)}, bf16[128,2048]{1,0:T(8,128)(2,1)S(1)}, bf16[384,2048]{1,0:T(8,128)(2,1)}) custom-call(bf16[128,2048]{1,0:T(8,128)(2,1)S(1)} %bitcast.35, bf16[128,2048]{1,0:T(8,128)(2,1)S(1)} %collective-permute-done.13.refs_1_, ...), custom_call_target="tpu_custom_call" | custom-call | flops 8455716864 | bytes 17301504 | tf_op jit(solution)/shard_map/pallas_call | solution.py:125
  57.1 2.2 %collective-permute-start.21 = (bf16[128,2048]{1,0:T(8,128)(2,1)S(1)}, bf16[128,2048]{1,0:T(8,128)(2,1)S(1)}, u32[]{:S(2)}, u32[]{:S(2)}) collective-permute-start(bf16[128,2048]{1,0:T(8,128)(2,1)S(1)} %bitcast.36), channel_id=1, source_target_pairs={{0,4},{2,6},{4,0},{6,2},{1,5},{3,7},{5,1},{7,3},{8,12},{10,14},{12... | collective-permute-start | bytes 1572872 | tf_op jit(solution)/shard_map/ppermute | solution.py:37
  59.8 1.7 %collective-permute-start.1 = (bf16[264,256]{1,0:T(8,128)(2,1)S(1)}, bf16[264,256]{1,0:T(8,128)(2,1)S(1)}, u32[]{:S(2)}, u32[]{:S(2)}) collective-permute-start(bf16[264,256]{1,0:T(8,128)(2,1)S(1)} %get-tuple-element.17.own_ref), channel_id=1, source_target_pairs={{0,16},{8,24},{16,0},{24,8},{1,17},{9,25},{17,1},{25,9},{2,18},{10... | collective-permute-start | bytes 405512 | tf_op jit(solution)/shard_map/ppermute | solution.py:37
  61.5 1.2 collective-permute-start.2
  62.6 10.1 %collective-permute-done.21.refs_0_ = bf16[128,2048]{1,0:T(8,128)(2,1)S(1)} collective-permute-done((bf16[128,2048]{1,0:T(8,128)(2,1)S(1)}, bf16[128,2048]{1,0:T(8,128)(2,1)S(1)}, u32[]{:S(2)}, u32[]{:S(2)}) %collective-permute-start.21) | collective-permute-done | bytes 524320 | tf_op jit(solution)/shard_map/ppermute | solution.py:37
  72.8 1.6 %add_convert_fusion.3 = (bf16[128,2048]{1,0:T(8,128)(2,1)S(1)}, bf16[128,2048]{1,0:T(8,128)(2,1)S(1)}) fusion(bf16[128,2048]{1,0:T(8,128)(2,1)S(1)} %get-tuple-element.25, bf16[384,2048]{1,0:T(8,128)(2,1)} %collective-permute-done.18, bf16[128,2048]{1,0:T(8,128)(2,1)S(1)} %get-tuple-element.26), kind=kLoop, calls=%fused_computation.3 | loop fusion | flops 2097152 | bytes 3145728 | tf_op jit(solution)/shard_map/convert_element_type | solution.py:459
  74.7 2.0 %copy-done.1 = bf16[1,2048,896]{2,1,0:T(8,128)(2,1)S(1)} copy-done((bf16[1,2048,896]{2,1,0:T(8,128)(2,1)S(1)}, bf16[1,2048,896]{2,1,0:T(8,128)(2,1)}, u32[]{:S(2)}) %copy-start.1) | copy-done | bytes 3670040
  76.7 2.0 %copy-done.3 = bf16[1,2048,896]{2,1,0:T(8,128)(2,1)S(1)} copy-done((bf16[1,2048,896]{2,1,0:T(8,128)(2,1)S(1)}, bf16[1,2048,896]{2,1,0:T(8,128)(2,1)}, u32[]{:S(2)}) %copy-start.3) | copy-done | bytes 3670040
  78.8 2.0 %copy-done.5 = bf16[1,896,2048]{2,1,0:T(8,128)(2,1)S(1)} copy-done((bf16[1,896,2048]{2,1,0:T(8,128)(2,1)S(1)}, bf16[1,896,2048]{2,1,0:T(8,128)(2,1)}, u32[]{:S(2)}) %copy-start.5) | copy-done | bytes 3670040
  80.8 3.3 %shard_map.177 = (bf16[128,2048]{1,0:T(8,128)(2,1)S(1)}, bf16[128,2048]{1,0:T(8,128)(2,1)S(1)}) custom-call(bf16[128,2048]{1,0:T(8,128)(2,1)S(1)} %collective-permute-done.21.refs_0_, bf16[128,2048]{1,0:T(8,128)(2,1)S(1)} %collective-permute-done.22.refs_1_, bf16[2048,896]{1,0:T(8,128)(2,1)S(1)} %bitcast.26, bf16[2048,896]{1,0:T(8,128)(2,1)S(1)} %bitcast.28, ...), custom_call_target="tpu_custom_call" | custom-call | flops 2818572288 | bytes 13107200 | tf_op jit(solution)/shard_map/pallas_call | solution.py:125
  84.8 2.2 %collective-permute-start.3 = (bf16[264,256]{1,0:T(8,128)(2,1)S(1)}, bf16[264,256]{1,0:T(8,128)(2,1)S(1)}, u32[]{:S(2)}, u32[]{:S(2)}) collective-permute-start(bf16[264,256]{1,0:T(8,128)(2,1)S(1)} %get-tuple-element.19), channel_id=1, source_target_pairs={{0,32},{32,64},{64,96},{1,33},{33,65},{65,97},{2,34},{34,66},{66,9... | collective-permute-start | bytes 405512 | tf_op jit(solution)/shard_map/ppermute | solution.py:37
  87.0 4.5 %collective-permute-start.4 = (bf16[264,256]{1,0:T(8,128)(2,1)S(1)}, bf16[264,256]{1,0:T(8,128)(2,1)S(1)}, u32[]{:S(2)}, u32[]{:S(2)}) collective-permute-start(bf16[264,256]{1,0:T(8,128)(2,1)S(1)} %get-tuple-element.19), channel_id=1, source_target_pairs={{0,64},{32,96},{1,65},{33,97},{2,66},{34,98},{3,67},{35,99},{4,68}... | collective-permute-start | bytes 405512 | tf_op jit(solution)/shard_map/ppermute | solution.py:37
  91.5 1.3 collective-permute-start.5
  92.8 0.9 collective-permute-start.20
  93.7 2.4 %collective-permute-start.19 = (bf16[128,2048]{1,0:T(8,128)(2,1)S(1)}, bf16[128,2048]{1,0:T(8,128)(2,1)S(1)}, u32[]{:S(2)}, u32[]{:S(2)}) collective-permute-start(bf16[128,2048]{1,0:T(8,128)(2,1)S(1)} %get-tuple-element.30), channel_id=1, source_target_pairs={{0,6},{2,0},{4,2},{6,4},{1,7},{3,1},{5,3},{7,5},{8,14},{10,8},{12,... | collective-permute-start | bytes 1572872 | tf_op jit(solution)/shard_map/ppermute | solution.py:37
  96.3 1.0 collective-permute-start.24
  97.4 2.3 %finish.1 = bf16[2048,256]{1,0:T(8,128)(2,1)S(1)} custom-call(s32[2]{0:T(128)S(1)} %pad_add_fusion.place_ref, f32[264,256]{1,0:T(8,128)S(1)} %get-tuple-element.18.before_ref, bf16[264,256]{1,0:T(8,128)(2,1)S(1)} %collective-permute-done.3.one_ref, bf16[264,256]{1,0:T(8,128)(2,1)S(1)} %collective-permute-done.4.two_ref, ...), custom_call_target="tpu_custom_call" | custom-call | flops 2000000000 | bytes 5242880 | tf_op jit(solution)/shard_map/finish/pallas_call | solution.py:335
  99.8 0.9 collective-permute-start.7
  101.2 1.0 collective-permute-start.8
  102.2 20.8 %collective-permute-done.7.refs_2_ = bf16[256,256]{1,0:T(8,128)(2,1)S(1)} collective-permute-done((bf16[256,256]{1,0:T(8,128)(2,1)S(1)}, bf16[256,256]{1,0:T(8,128)(2,1)S(1)}, u32[]{:S(2)}, u32[]{:S(2)}) %collective-permute-start.7) | collective-permute-done | bytes 131104 | tf_op jit(solution)/shard_map/ppermute | solution.py:484
  122.9 1.0 collective-permute-start.9
  123.9 1.5 collective-permute-start.11
  125.4 2.1 %collective-permute-start.12 = (bf16[256,256]{1,0:T(8,128)(2,1)S(1)}, bf16[256,256]{1,0:T(8,128)(2,1)S(1)}, u32[]{:S(2)}, u32[]{:S(2)}) collective-permute-start(bf16[256,256]{1,0:T(8,128)(2,1)S(1)} %get-tuple-element.32), channel_id=1, source_target_pairs={{0,7},{1,6},{2,1},{3,0},{4,3},{5,2},{6,5},{7,4},{8,15},{9,14},{10,... | collective-permute-start | bytes 393224 | tf_op jit(solution)/shard_map/ppermute | solution.py:484
  127.5 2.3 %fusion = bf16[16,8,2048]{2,1,0:T(8,128)(2,1)} fusion(bf16[128,2048]{1,0:T(8,128)(2,1)S(1)} %collective-permute-done.24, bf16[128,2048]{1,0:T(8,128)(2,1)S(1)} %collective-permute-done.20, bf16[128,2048]{1,0:T(8,128)(2,1)S(1)} %collective-permute-done.19, bf16[128,2048]{1,0:T(8,128)(2,1)S(1)} %get-tuple-element.23, bf16[384,2048]{1,0:T(8,128)(2,1)} %collective-permute-done.18), kind=kLoop, calls=%fused_computation.5 | loop fusion | flops 3145728 | bytes 3145728 | tf_op jit(solution)/shard_map/all_to_all | solution.py:489
  129.7 3.6 %all-to-all-start.1 = ((bf16[16,8,2048]{2,1,0:T(8,128)(2,1)}), bf16[16,8,2048]{2,1,0:T(8,128)(2,1)S(1)}, u32[]{:S(2)}, u32[]{:S(2)}) async-start(bf16[16,8,2048]{2,1,0:T(8,128)(2,1)} %fusion), calls=%async_computation.1 | async-start | bytes 1048576 | tf_op jit(solution)/shard_map/all_to_all | solution.py:489
  133.4 0.7 collective-permute-done.11.refs_6_
  134.1 1.5 %collective-permute-done.12.refs_7_ = bf16[256,256]{1,0:T(8,128)(2,1)S(1)} collective-permute-done((bf16[256,256]{1,0:T(8,128)(2,1)S(1)}, bf16[256,256]{1,0:T(8,128)(2,1)S(1)}, u32[]{:S(2)}, u32[]{:S(2)}) %collective-permute-start.12) | collective-permute-done | bytes 131104 | tf_op jit(solution)/shard_map/ppermute | solution.py:484
  135.6 3.4 %copy-done.6 = bf16[2048,2048]{1,0:T(8,128)(2,1)S(1)} copy-done((bf16[2048,2048]{1,0:T(8,128)(2,1)S(1)}, bf16[2048,2048]{1,0:T(8,128)(2,1)}, u32[]{:S(2)}) %copy-start.6) | copy-done | bytes 8388632
  139.0 6.2 %project.1 = bf16[256,2048]{1,0:T(8,128)(2,1)} custom-call(s32[8]{0:T(128)S(1)} %stack.49.head_ref, bf16[256,256]{1,0:T(8,128)(2,1)S(1)} %get-tuple-element.39.refs_0_, bf16[256,256]{1,0:T(8,128)(2,1)S(1)} %collective-permute-done.6.refs_1_, bf16[256,256]{1,0:T(8,128)(2,1)S(1)} %collective-permute-done.7.refs_2_, ...), custom_call_target="tpu_custom_call" | custom-call | flops 4000000000 | bytes 10485760 | tf_op jit(solution)/shard_map/project/pallas_call | solution.py:371
  145.2 1.2 combine.1
  (74 shorter events, 3.3 us)
Async XLA Ops:
  2.9 9.5 %copy-start.24 = (f32[128]{0:T(128)S(1)}, f32[128]{0:T(128)}, u32[]{:S(2)}) copy-start(f32[128]{0:T(128)} %constant.52.clone) | copy-start | bytes 1540
  2.9 9.6 %copy-start.7 = (bf16[2048,256]{1,0:T(8,128)(2,1)S(1)}, bf16[2048,256]{1,0:T(8,128)(2,1)}, u32[]{:S(2)}) copy-start(bf16[2048,256]{1,0:T(8,128)(2,1)} %q_ref) | copy-start | bytes 3145732
  2.9 9.6 %copy-start.8 = (bf16[2048,256]{1,0:T(8,128)(2,1)S(1)}, bf16[2048,256]{1,0:T(8,128)(2,1)}, u32[]{:S(2)}) copy-start(bf16[2048,256]{1,0:T(8,128)(2,1)} %k_ref.1) | copy-start | bytes 3145732
  2.9 9.6 %copy-start.13 = (f32[2048,1]{0,1:T(1,128)S(1)}, f32[2048,1]{0,1:T(1,128)}, u32[]{:S(2)}) copy-start(f32[2048,1]{0,1:T(1,128)} %param.21) | copy-start | bytes 24580
  2.9 9.6 %copy-start.18 = (f32[512,128]{1,0:T(8,128)S(1)}, f32[512,128]{1,0:T(8,128)}, u32[]{:S(2)}) copy-start(f32[512,128]{1,0:T(8,128)} %constant.53.clone.cos_ref) | copy-start | bytes 786436
  2.9 9.6 %copy-start.19 = (f32[512,128]{1,0:T(8,128)S(1)}, f32[512,128]{1,0:T(8,128)}, u32[]{:S(2)}) copy-start(f32[512,128]{1,0:T(8,128)} %constant.54.clone.sin_ref) | copy-start | bytes 786436
  4.3 19.5 %all-to-all-start = ((bf16[16,8,2048]{2,1,0:T(8,128)(2,1)}), bf16[16,8,2048]{2,1,0:T(8,128)(2,1)S(1)}, u32[]{:S(2)}, u32[]{:S(2)}) async-start(bf16[16,8,2048]{2,1,0:T(8,128)(2,1)} %bitcast.16), calls=%async_computation | async-start | bytes 1048576 | tf_op jit(solution)/shard_map/all_to_all | solution.py:425
  12.5 1.2 copy-start.9
  17.3 1.4 copy-start.20
  23.8 13.6 %collective-permute-start.13 = (bf16[128,2048]{1,0:T(8,128)(2,1)S(1)}, bf16[128,2048]{1,0:T(8,128)(2,1)S(1)}, u32[]{:S(2)}, u32[]{:S(2)}) collective-permute-start(bf16[128,2048]{1,0:T(8,128)(2,1)S(1)} %bitcast.32), channel_id=1, source_target_pairs={{0,2},{2,4},{4,6},{6,0},{1,3},{3,5},{5,7},{7,1},{8,10},{10,12},{12... | collective-permute-start | bytes 1572872 | tf_op jit(solution)/shard_map/ppermute | solution.py:37
  25.4 12.0 %collective-permute-start.14 = (bf16[128,2048]{1,0:T(8,128)(2,1)S(1)}, bf16[128,2048]{1,0:T(8,128)(2,1)S(1)}, u32[]{:S(2)}, u32[]{:S(2)}) collective-permute-start(bf16[128,2048]{1,0:T(8,128)(2,1)S(1)} %bitcast.33), channel_id=1, source_target_pairs={{0,6},{2,0},{4,2},{6,4},{1,7},{3,1},{5,3},{7,5},{8,14},{10,8},{12,... | collective-permute-start | bytes 1572872 | tf_op jit(solution)/shard_map/ppermute | solution.py:37
  27.1 10.8 %collective-permute-start.15 = (bf16[128,2048]{1,0:T(8,128)(2,1)S(1)}, bf16[128,2048]{1,0:T(8,128)(2,1)S(1)}, u32[]{:S(2)}, u32[]{:S(2)}) collective-permute-start(bf16[128,2048]{1,0:T(8,128)(2,1)S(1)} %bitcast.34), channel_id=1, source_target_pairs={{0,1},{1,0},{2,3},{3,2},{4,5},{5,4},{6,7},{7,6},{8,9},{9,8},{10,11... | collective-permute-start | bytes 1572872 | tf_op jit(solution)/shard_map/ppermute | solution.py:37
  37.4 1.9 %collective-permute-start.16 = (bf16[128,2048]{1,0:T(8,128)(2,1)S(1)}, bf16[128,2048]{1,0:T(8,128)(2,1)S(1)}, u32[]{:S(2)}, u32[]{:S(2)}) collective-permute-start(bf16[128,2048]{1,0:T(8,128)(2,1)S(1)} %collective-permute-done.13.refs_1_), channel_id=1, source_target_pairs={{0,1},{1,0},{2,3},{3,2},{4,5},{5,4},{6,7},{7,6},{8,9},{9,8},{10,11... | collective-permute-start | bytes 1572872 | tf_op jit(solution)/shard_map/ppermute | solution.py:37
  37.4 2.6 %collective-permute-start.17 = (bf16[128,2048]{1,0:T(8,128)(2,1)S(1)}, bf16[128,2048]{1,0:T(8,128)(2,1)S(1)}, u32[]{:S(2)}, u32[]{:S(2)}) collective-permute-start(bf16[128,2048]{1,0:T(8,128)(2,1)S(1)} %collective-permute-done.14.refs_2_), channel_id=1, source_target_pairs={{0,1},{1,0},{2,3},{3,2},{4,5},{5,4},{6,7},{7,6},{8,9},{9,8},{10,11... | collective-permute-start | bytes 1572872 | tf_op jit(solution)/shard_map/ppermute | solution.py:37
  40.0 2.0 %copy-start = (bf16[1,2048,896]{2,1,0:T(8,128)(2,1)S(1)}, bf16[1,2048,896]{2,1,0:T(8,128)(2,1)}, u32[]{:S(2)}) copy-start(bf16[1,2048,896]{2,1,0:T(8,128)(2,1)} %param.28) | copy-start | bytes 11010052
  42.1 2.0 %copy-start.2 = (bf16[1,2048,896]{2,1,0:T(8,128)(2,1)S(1)}, bf16[1,2048,896]{2,1,0:T(8,128)(2,1)}, u32[]{:S(2)}) copy-start(bf16[1,2048,896]{2,1,0:T(8,128)(2,1)} %param.29) | copy-start | bytes 11010052
  44.1 2.0 %copy-start.4 = (bf16[1,896,2048]{2,1,0:T(8,128)(2,1)S(1)}, bf16[1,896,2048]{2,1,0:T(8,128)(2,1)}, u32[]{:S(2)}) copy-start(bf16[1,896,2048]{2,1,0:T(8,128)(2,1)} %param.30) | copy-start | bytes 11010052
  56.9 15.9 %collective-permute-start.18 = (bf16[384,2048]{1,0:T(8,128)(2,1)}, bf16[384,2048]{1,0:T(8,128)(2,1)}, u32[]{:S(2)}, u32[]{:S(2)}) collective-permute-start(bf16[384,2048]{1,0:T(8,128)(2,1)} %get-tuple-element.24), channel_id=1, source_target_pairs={{0,1},{1,0},{2,3},{3,2},{4,5},{5,4},{6,7},{7,6},{8,9},{9,8},{10,11... | collective-permute-start | bytes 4718600 | tf_op jit(solution)/shard_map/ppermute | solution.py:37
  57.1 15.7 %collective-permute-start.21 = (bf16[128,2048]{1,0:T(8,128)(2,1)S(1)}, bf16[128,2048]{1,0:T(8,128)(2,1)S(1)}, u32[]{:S(2)}, u32[]{:S(2)}) collective-permute-start(bf16[128,2048]{1,0:T(8,128)(2,1)S(1)} %bitcast.36), channel_id=1, source_target_pairs={{0,4},{2,6},{4,0},{6,2},{1,5},{3,7},{5,1},{7,3},{8,12},{10,14},{12... | collective-permute-start | bytes 1572872 | tf_op jit(solution)/shard_map/ppermute | solution.py:37
  59.2 25.2 %collective-permute-start = (bf16[264,256]{1,0:T(8,128)(2,1)S(1)}, bf16[264,256]{1,0:T(8,128)(2,1)S(1)}, u32[]{:S(2)}, u32[]{:S(2)}) collective-permute-start(bf16[264,256]{1,0:T(8,128)(2,1)S(1)} %get-tuple-element.17.own_ref), channel_id=1, source_target_pairs={{0,8},{8,16},{16,24},{24,0},{1,9},{9,17},{17,25},{25,1},{2,10},{10... | collective-permute-start | bytes 405512 | tf_op jit(solution)/shard_map/ppermute | solution.py:37
  59.8 24.7 %collective-permute-start.1 = (bf16[264,256]{1,0:T(8,128)(2,1)S(1)}, bf16[264,256]{1,0:T(8,128)(2,1)S(1)}, u32[]{:S(2)}, u32[]{:S(2)}) collective-permute-start(bf16[264,256]{1,0:T(8,128)(2,1)S(1)} %get-tuple-element.17.own_ref), channel_id=1, source_target_pairs={{0,16},{8,24},{16,0},{24,8},{1,17},{9,25},{17,1},{25,9},{2,18},{10... | collective-permute-start | bytes 405512 | tf_op jit(solution)/shard_map/ppermute | solution.py:37
  61.5 23.0 %collective-permute-start.2 = (bf16[264,256]{1,0:T(8,128)(2,1)S(1)}, bf16[264,256]{1,0:T(8,128)(2,1)S(1)}, u32[]{:S(2)}, u32[]{:S(2)}) collective-permute-start(bf16[264,256]{1,0:T(8,128)(2,1)S(1)} %get-tuple-element.17.own_ref), channel_id=1, source_target_pairs={{0,24},{8,0},{16,8},{24,16},{1,25},{9,1},{17,9},{25,17},{2,26},{10... | collective-permute-start | bytes 405512 | tf_op jit(solution)/shard_map/ppermute | solution.py:37
  72.8 1.9 %collective-permute-start.22 = (bf16[128,2048]{1,0:T(8,128)(2,1)S(1)}, bf16[128,2048]{1,0:T(8,128)(2,1)S(1)}, u32[]{:S(2)}, u32[]{:S(2)}) collective-permute-start(bf16[128,2048]{1,0:T(8,128)(2,1)S(1)} %collective-permute-done.21.refs_0_), channel_id=1, source_target_pairs={{0,1},{1,0},{2,3},{3,2},{4,5},{5,4},{6,7},{7,6},{8,9},{9,8},{10,11... | collective-permute-start | bytes 1572872 | tf_op jit(solution)/shard_map/ppermute | solution.py:37
  74.7 2.0 %copy-start.1 = (bf16[1,2048,896]{2,1,0:T(8,128)(2,1)S(1)}, bf16[1,2048,896]{2,1,0:T(8,128)(2,1)}, u32[]{:S(2)}) copy-start(bf16[1,2048,896]{2,1,0:T(8,128)(2,1)} %param.28) | copy-start | bytes 11010052
  76.7 2.0 %copy-start.3 = (bf16[1,2048,896]{2,1,0:T(8,128)(2,1)S(1)}, bf16[1,2048,896]{2,1,0:T(8,128)(2,1)}, u32[]{:S(2)}) copy-start(bf16[1,2048,896]{2,1,0:T(8,128)(2,1)} %param.29) | copy-start | bytes 11010052
  78.7 2.0 %copy-start.5 = (bf16[1,896,2048]{2,1,0:T(8,128)(2,1)S(1)}, bf16[1,896,2048]{2,1,0:T(8,128)(2,1)}, u32[]{:S(2)}) copy-start(bf16[1,896,2048]{2,1,0:T(8,128)(2,1)} %param.30) | copy-start | bytes 11010052
  84.1 9.7 %collective-permute-start.23 = (bf16[128,2048]{1,0:T(8,128)(2,1)S(1)}, bf16[128,2048]{1,0:T(8,128)(2,1)S(1)}, u32[]{:S(2)}, u32[]{:S(2)}) collective-permute-start(bf16[128,2048]{1,0:T(8,128)(2,1)S(1)} %get-tuple-element.29), channel_id=1, source_target_pairs={{0,1},{1,0},{2,3},{3,2},{4,5},{5,4},{6,7},{7,6},{8,9},{9,8},{10,11... | collective-permute-start | bytes 1572872 | tf_op jit(solution)/shard_map/ppermute | solution.py:37
  84.5 12.9 %copy-start.10 = (bf16[2048,256]{1,0:T(8,128)(2,1)S(1)}, bf16[2048,256]{1,0:T(8,128)(2,1)}, u32[]{:S(2)}) copy-start(bf16[2048,256]{1,0:T(8,128)(2,1)} %gate_ref.1) | copy-start | bytes 3145732
  84.5 12.9 %copy-start.14 = (f32[256]{0:T(256)S(1)}, f32[256]{0:T(256)}, u32[]{:S(2)}) copy-start(f32[256]{0:T(256)} %param.22) | copy-start | bytes 3076
  84.5 12.9 %copy-start.21 = (f32[2048,256]{1,0:T(8,128)S(1)}, f32[2048,256]{1,0:T(8,128)}, u32[]{:S(2)}) copy-start(f32[2048,256]{1,0:T(8,128)} %copy-done.20) | copy-start | bytes 6291460
  84.5 12.9 %copy-start.23 = (bf16[2048,256]{1,0:T(8,128)(2,1)S(1)}, bf16[2048,256]{1,0:T(8,128)(2,1)}, u32[]{:S(2)}) copy-start(bf16[2048,256]{1,0:T(8,128)(2,1)} %copy-done.22) | copy-start | bytes 3145732
  84.8 11.5 %collective-permute-start.3 = (bf16[264,256]{1,0:T(8,128)(2,1)S(1)}, bf16[264,256]{1,0:T(8,128)(2,1)S(1)}, u32[]{:S(2)}, u32[]{:S(2)}) collective-permute-start(bf16[264,256]{1,0:T(8,128)(2,1)S(1)} %get-tuple-element.19), channel_id=1, source_target_pairs={{0,32},{32,64},{64,96},{1,33},{33,65},{65,97},{2,34},{34,66},{66,9... | collective-permute-start | bytes 405512 | tf_op jit(solution)/shard_map/ppermute | solution.py:37
  87.0 10.4 %collective-permute-start.4 = (bf16[264,256]{1,0:T(8,128)(2,1)S(1)}, bf16[264,256]{1,0:T(8,128)(2,1)S(1)}, u32[]{:S(2)}, u32[]{:S(2)}) collective-permute-start(bf16[264,256]{1,0:T(8,128)(2,1)S(1)} %get-tuple-element.19), channel_id=1, source_target_pairs={{0,64},{32,96},{1,65},{33,97},{2,66},{34,98},{3,67},{35,99},{4,68}... | collective-permute-start | bytes 405512 | tf_op jit(solution)/shard_map/ppermute | solution.py:37
  91.5 5.8 %collective-permute-start.5 = (bf16[264,256]{1,0:T(8,128)(2,1)S(1)}, bf16[264,256]{1,0:T(8,128)(2,1)S(1)}, u32[]{:S(2)}, u32[]{:S(2)}) collective-permute-start(bf16[264,256]{1,0:T(8,128)(2,1)S(1)} %get-tuple-element.19), channel_id=1, source_target_pairs={{0,96},{1,97},{2,98},{3,99},{4,100},{5,101},{6,102},{7,103},{8,104... | collective-permute-start | bytes 405512 | tf_op jit(solution)/shard_map/ppermute | solution.py:37
  92.8 31.1 %collective-permute-start.20 = (bf16[128,2048]{1,0:T(8,128)(2,1)S(1)}, bf16[128,2048]{1,0:T(8,128)(2,1)S(1)}, u32[]{:S(2)}, u32[]{:S(2)}) collective-permute-start(bf16[128,2048]{1,0:T(8,128)(2,1)S(1)} %get-tuple-element.31), channel_id=1, source_target_pairs={{0,2},{2,4},{4,6},{6,0},{1,3},{3,5},{5,7},{7,1},{8,10},{10,12},{12... | collective-permute-start | bytes 1572872 | tf_op jit(solution)/shard_map/ppermute | solution.py:37
  93.7 30.2 %collective-permute-start.19 = (bf16[128,2048]{1,0:T(8,128)(2,1)S(1)}, bf16[128,2048]{1,0:T(8,128)(2,1)S(1)}, u32[]{:S(2)}, u32[]{:S(2)}) collective-permute-start(bf16[128,2048]{1,0:T(8,128)(2,1)S(1)} %get-tuple-element.30), channel_id=1, source_target_pairs={{0,6},{2,0},{4,2},{6,4},{1,7},{3,1},{5,3},{7,5},{8,14},{10,8},{12,... | collective-permute-start | bytes 1572872 | tf_op jit(solution)/shard_map/ppermute | solution.py:37
  96.3 29.1 %collective-permute-start.24 = (bf16[128,2048]{1,0:T(8,128)(2,1)S(1)}, bf16[128,2048]{1,0:T(8,128)(2,1)S(1)}, u32[]{:S(2)}, u32[]{:S(2)}) collective-permute-start(bf16[128,2048]{1,0:T(8,128)(2,1)S(1)} %add_convert_fusion.1), channel_id=1, source_target_pairs={{0,4},{2,6},{4,0},{6,2},{1,5},{3,7},{5,1},{7,3},{8,12},{10,14},{12... | collective-permute-start | bytes 1572872 | tf_op jit(solution)/shard_map/ppermute | solution.py:37
  99.8 1.4 collective-permute-start.6
  99.8 23.1 %collective-permute-start.7 = (bf16[256,256]{1,0:T(8,128)(2,1)S(1)}, bf16[256,256]{1,0:T(8,128)(2,1)S(1)}, u32[]{:S(2)}, u32[]{:S(2)}) collective-permute-start(bf16[256,256]{1,0:T(8,128)(2,1)S(1)} %get-tuple-element.37), channel_id=1, source_target_pairs={{0,2},{1,3},{2,4},{3,5},{4,6},{5,7},{6,0},{7,1},{8,10},{9,11},{10,... | collective-permute-start | bytes 393224 | tf_op jit(solution)/shard_map/ppermute | solution.py:484
  101.2 32.2 %collective-permute-start.8 = (bf16[256,256]{1,0:T(8,128)(2,1)S(1)}, bf16[256,256]{1,0:T(8,128)(2,1)S(1)}, u32[]{:S(2)}, u32[]{:S(2)}) collective-permute-start(bf16[256,256]{1,0:T(8,128)(2,1)S(1)} %get-tuple-element.36), channel_id=1, source_target_pairs={{0,3},{1,2},{2,5},{3,4},{4,7},{5,6},{6,1},{7,0},{8,11},{9,10},{10,... | collective-permute-start | bytes 393224 | tf_op jit(solution)/shard_map/ppermute | solution.py:484
  122.9 10.5 %collective-permute-start.9 = (bf16[256,256]{1,0:T(8,128)(2,1)S(1)}, bf16[256,256]{1,0:T(8,128)(2,1)S(1)}, u32[]{:S(2)}, u32[]{:S(2)}) collective-permute-start(bf16[256,256]{1,0:T(8,128)(2,1)S(1)} %get-tuple-element.35), channel_id=1, source_target_pairs={{0,4},{1,5},{2,6},{3,7},{4,0},{5,1},{6,2},{7,3},{8,12},{9,13},{10,... | collective-permute-start | bytes 393224 | tf_op jit(solution)/shard_map/ppermute | solution.py:484
  123.9 9.5 %collective-permute-start.10 = (bf16[256,256]{1,0:T(8,128)(2,1)S(1)}, bf16[256,256]{1,0:T(8,128)(2,1)S(1)}, u32[]{:S(2)}, u32[]{:S(2)}) collective-permute-start(bf16[256,256]{1,0:T(8,128)(2,1)S(1)} %get-tuple-element.34), channel_id=1, source_target_pairs={{0,5},{1,4},{2,7},{3,6},{4,1},{5,0},{6,3},{7,2},{8,13},{9,12},{10,... | collective-permute-start | bytes 393224 | tf_op jit(solution)/shard_map/ppermute | solution.py:484
  123.9 10.2 %collective-permute-start.11 = (bf16[256,256]{1,0:T(8,128)(2,1)S(1)}, bf16[256,256]{1,0:T(8,128)(2,1)S(1)}, u32[]{:S(2)}, u32[]{:S(2)}) collective-permute-start(bf16[256,256]{1,0:T(8,128)(2,1)S(1)} %get-tuple-element.33), channel_id=1, source_target_pairs={{0,6},{1,7},{2,0},{3,1},{4,2},{5,3},{6,4},{7,5},{8,14},{9,15},{10,... | collective-permute-start | bytes 393224 | tf_op jit(solution)/shard_map/ppermute | solution.py:484
  125.4 10.2 %collective-permute-start.12 = (bf16[256,256]{1,0:T(8,128)(2,1)S(1)}, bf16[256,256]{1,0:T(8,128)(2,1)S(1)}, u32[]{:S(2)}, u32[]{:S(2)}) collective-permute-start(bf16[256,256]{1,0:T(8,128)(2,1)S(1)} %get-tuple-element.32), channel_id=1, source_target_pairs={{0,7},{1,6},{2,1},{3,0},{4,3},{5,2},{6,5},{7,4},{8,15},{9,14},{10,... | collective-permute-start | bytes 393224 | tf_op jit(solution)/shard_map/ppermute | solution.py:484
  129.7 15.4 %all-to-all-start.1 = ((bf16[16,8,2048]{2,1,0:T(8,128)(2,1)}), bf16[16,8,2048]{2,1,0:T(8,128)(2,1)S(1)}, u32[]{:S(2)}, u32[]{:S(2)}) async-start(bf16[16,8,2048]{2,1,0:T(8,128)(2,1)} %fusion), calls=%async_computation.1 | async-start | bytes 1048576 | tf_op jit(solution)/shard_map/all_to_all | solution.py:489
  135.6 3.4 %copy-start.6 = (bf16[2048,2048]{1,0:T(8,128)(2,1)S(1)}, bf16[2048,2048]{1,0:T(8,128)(2,1)}, u32[]{:S(2)}) copy-start(bf16[2048,2048]{1,0:T(8,128)(2,1)} %refs_8_.1) | copy-start | bytes 25165828
  139.0 6.2 %copy-start.16 = (s32[32,2]{0,1:T(2,128)S(1)}, s32[32,2]{0,1:T(2,128)}, u32[]{:S(2)}) copy-start(s32[32,2]{0,1:T(2,128)} %param.25) | copy-start | bytes 772
  139.0 6.2 %copy-start.17 = (f32[32,2]{0,1:T(2,128)S(1)}, f32[32,2]{0,1:T(2,128)}, u32[]{:S(2)}) copy-start(f32[32,2]{0,1:T(2,128)} %param.26) | copy-start | bytes 772
  (4 other events, 3.3 us)

commit v6 on v5

--- a/solution.py
+++ b/solution.py
@@ -32,13 +32,17 @@
     return jnp.dot(a, b, preferred_element_type=f32)
 
 
-def shift(x, axis, by, size=4, wrap=True):
-    pairs = [(j, (j + by) % size) for j in range(size) if wrap or 0 <= j + by < size]
+def shift(x, axis, by, size=4):
+    pairs = [(j, (j + by) % size) for j in range(size)]
     return lax.ppermute(x, axis, pairs)
 
 
 def vm(x):
     return pltpu.with_memory_space_constraint(x, pltpu.VMEM)
+
+
+def hb(x):
+    return pltpu.with_memory_space_constraint(x, pltpu.HBM)
 
 
 def grid_params(mib):
@@ -193,7 +197,7 @@
             >= lax.broadcasted_iota(jnp.int32, (half, hi), 1)
         )
         weights = jnp.where(seen, scores * jnp.exp(jnp.where(seen, gap, 0.0)), 0.0).astype(bf16)
-        kept_ref[lo:hi, :] = mm(weights, v[:hi]) + carried[lo:hi]
+        kept_ref[lo:hi, :] = (mm(weights, v[:hi]) + carried[lo:hi]).astype(bf16)
     qd_ref[...] = (q32 * jnp.exp(cum + before[0:1, 0:1])).astype(bf16)
     kd = (k.astype(f32) * jnp.exp(last - cum)).astype(bf16)
     update = lax.dot_general(kd, v, TN, preferred_element_type=f32)
@@ -227,8 +231,8 @@
         local_kernel,
         grid=(blocks,),
         out_shape=[
-            jax.ShapeDtypeStruct((rows, HEAD_DIM), f32),
-            jax.ShapeDtypeStruct((rows, HEAD_DIM), bf16),
+            pltpu.HBM((rows, HEAD_DIM), bf16),
+            pltpu.HBM((rows, HEAD_DIM), bf16),
             jax.ShapeDtypeStruct((HEAD_DIM + 8, HEAD_DIM), bf16),
         ],
         in_specs=[
@@ -250,7 +254,7 @@
             flops=6 * 10**9, bytes_accessed=6 * 2**20, transcendentals=2**20
         ),
         name="local",
-    )(base, q, k, v, ld, cos_t, sin_t)
+    )(base, q, k, hb(v), ld, cos_t, sin_t)
 
 
 def middle_kernel(x_ref, own_ref, one_ref, two_ref, three_ref, before_ref, send_ref):
@@ -311,20 +315,21 @@
 ):
     @pl.when(pl.program_id(0) == 0)
     def _():
-        into = three_ref[0:HEAD_DIM, :].astype(f32)
-        for ref in (two_ref, one_ref):
-            into = ref[0:HEAD_DIM, :].astype(f32) + get_decay(ref) * into
+        into = jnp.zeros((HEAD_DIM, HEAD_DIM), f32)
+        for far, ref in ((3, three_ref), (2, two_ref), (1, one_ref)):
+            longer = ref[0:HEAD_DIM, :].astype(f32) + get_decay(ref) * into
+            into = jnp.where(far <= place_ref[0], longer, into)
         through = before_ref[HEAD_DIM : HEAD_DIM + 1, 0:1]
         start[...] = (before_ref[0:HEAD_DIM, :] + through * into).astype(bf16)
 
-    retained = kept_ref[...] + mm(qd_ref[...], start[...])
+    retained = kept_ref[...].astype(f32) + mm(qd_ref[...], start[...])
     scale = lax.rsqrt(jnp.mean(retained * retained, axis=-1, keepdims=True) + norm_eps)
     gate = gate_ref[...].astype(f32)
     gate = gate / (1.0 + jnp.exp(-gate))
     done = (gate * retained * scale * gain_ref[...]).astype(bf16)
     rows = BLOCK // 2
     for c in range(2):
-        other = lax.rem(place_ref[1] + c, 2)
+        other = lax.rem(place_ref[2] + c, 2)
         out_ref[pl.ds(pl.multiple_of(other * rows, rows), rows), :] = done[c * rows : (c + 1) * rows]
 
 
@@ -341,7 +346,7 @@
             + [seq] * 3
             + [pl.BlockSpec((1, HEAD_DIM), lambda b, place: (0, 0))],
             out_specs=pl.BlockSpec(
-                (BLOCK, HEAD_DIM), lambda b, place: (lax.rem(b - place[0] + 4, 4), 0)
+                (BLOCK, HEAD_DIM), lambda b, place: (lax.rem(b - place[1] + 4, 4), 0)
             ),
             scratch_shapes=[pltpu.VMEM((HEAD_DIM, HEAD_DIM), bf16)],
         ),
@@ -351,7 +356,7 @@
             flops=2 * 10**9, bytes_accessed=5 * 2**20, transcendentals=2**19
         ),
         name="finish",
-    )(place, before, one, two, three, kept, qd, gate, gain)
+    )(place, before, one, two, three, hb(kept), hb(qd), hb(gate), hb(gain))
 
 
 def project_kernel(head_ref, *refs):
@@ -367,7 +372,7 @@
 def project(heads, pieces, w_out):
     whole, width = w_out.shape
     rows = pieces[0].shape[0]
-    cols = 256
+    cols = 512
     return pl.pallas_call(
         project_kernel,
         grid_spec=pltpu.PrefetchScalarGridSpec(
@@ -421,7 +426,7 @@
         compiler_params=pltpu.CompilerParams(vmem_limit_bytes=8 * MIB),
         cost_estimate=pl.CostEstimate(flops=2 * 10**9, bytes_accessed=10**6, transcendentals=0),
         name="pre",
-    )(moe_in, ids, moe_gain.reshape(1, -1))
+    )(hb(moe_in), hb(ids), hb(moe_gain.reshape(1, -1)))
     own = lax.all_to_all(outgoing, ep, split_axis=0, concat_axis=0, tiled=True)
 
     cos_t, sin_t = angle_tables()
@@ -447,7 +452,7 @@
     own_c = shift(own, "core", 1, 2)
     x_index = lax.axis_index("x").astype(jnp.int32).reshape(1)
     before, whole = middle(x_index, end, *by_x)
-    by_z = [shift(whole, "z", s, wrap=False) for s in (1, 2, 3)]
+    by_z = [shift(whole, "z", s) for s in (1, 2, 3)]
     up_c = shift(up, "core", 1, 2)
     down_c = shift(down, "core", 1, 2)
     n = own.shape[0]
@@ -459,13 +464,14 @@
         (k.astype(f32) + got1[i * n : (i + 1) * n].astype(f32)).astype(bf16)
         for i, k in enumerate(keep)
     ]
+    near = lax.optimization_barrier(near)
     back_up = shift(near[1], "y", -1)
     back_down = shift(near[2], "y", 1)
     keep2, give2 = ffn([after(far, near[2])], [far_c], weights)
     got2 = shift(give2, "core", 1, 2)
     back_far = shift((keep2.astype(f32) + got2.astype(f32)).astype(bf16), "y", 2)
-    y_index, c_index = lax.axis_index("y"), lax.axis_index("core")
-    place = jnp.stack([y_index, c_index]).astype(jnp.int32)
+    y_at, c_at = lax.axis_index("y"), lax.axis_index("core")
+    place = jnp.stack([lax.axis_index("z"), y_at, c_at]).astype(jnp.int32)
     heads_out = finish(
         place, before, *by_z, kept, qd, mix_gate, ret_gain.reshape(1, -1)
     )
@@ -483,7 +489,7 @@
                 ]
                 piece = lax.ppermute(piece, tp, pairs)
             pieces.append(piece)
-            sources.append(2 * lax.rem(y_index - dy + 4, 4) + lax.rem(c_index + dc, 2))
+            sources.append(2 * lax.rem(y_at - dy + 4, 4) + lax.rem(c_at + dc, 2))
     parts = (near[0], back_up, back_down, back_far)
     expert_rows = sum(v.astype(f32) for v in parts).astype(bf16)
     returned = lax.all_to_all(expert_rows, ep, split_axis=0, concat_axis=0, tiled=True)

time: 149 us -> 140 us (0.940)
  local copies, waits for them, and re-layouts: 21.7 us -> 13.8 us
  Pallas kernels: 29 us -> 32.7 us
  starting transfers between devices: 40.2 us -> 38.2 us
    unnamed x50 -> x30, local copies, waits for them, and re-layouts: 21.5 us -> 13.6 us
    ppermute x7, waiting for transfers between devices: 23.3 us -> 18.3 us  [on_device(): piece = lax.ppermute(piece, tp, pairs)]
    ppermute x18, starting transfers between devices: 22.2 us -> 19.6 us  [shift(): return lax.ppermute(x, axis, pairs)]
    pallas_call x1, Pallas kernels: 3.6 us -> 5.62 us  [local_part(): pl.pallas_call(local_kernel, grid=(blocks,), out_shape=[pltpu.HBM((rows,...]
    pallas_call x1, Pallas kernels: 2.3 us -> 4.26 us  [finish(): pl.pallas_call(finish_kernel, grid_spec=pltpu.PrefetchScalarGridSpec(num_...]
    ppermute x18, waiting for transfers between devices: 22.9 us -> 24.7 us  [shift(): return lax.ppermute(x, axis, pairs)]
    all_to_all x1, waiting for transfers between devices: 4.15 us -> 5.67 us  [on_device(): own = lax.all_to_all(outgoing, ep, split_axis=0, concat_axis=0, tiled=True)]
  transfers between devices with their start and end apart: 27 -> 27, of which waited for: 10 -> 11; matrix products, arithmetic and copies ran while one was open for 3% -> 3% of each run, Pallas kernels for 11% -> 13%
where the time goes in v6:
time: 140 us; the launch traced here: 138 us
  waiting for transfers between devices  49 us (35%)
  starting transfers between devices  38.2 us (27%)
  Pallas kernels  32.7 us (23%)
  local copies, waits for them, and re-layouts  13.8 us (10%)
  other arithmetic  3.36 us (2%)
    ppermute x18, waiting for transfers between devices, shift(): return lax.ppermute(x, axis, pairs)  24.7 us
    ppermute x18, starting transfers between devices, shift(): return lax.ppermute(x, axis, pairs)  19.6 us
    ppermute x7, waiting for transfers between devices, on_device(): piece = lax.ppermute(piece, tp, pairs)  18.3 us
    pallas_call x2, Pallas kernels, ffn(): pl.pallas_call(functools.partial(ffn_kernel, n_x), out_shape=[pltpu.VMEM(...  14.1 us
    unnamed x30, local copies, waits for them, and re-layouts  13.6 us
    all_to_all x1, starting transfers between devices, on_device(): own = lax.all_to_all(outgoing, ep, split_axis=0, concat_axis=0, tiled=True)  7.99 us
    ppermute x7, starting transfers between devices, on_device(): piece = lax.ppermute(piece, tp, pairs)  6.97 us
    all_to_all x1, waiting for transfers between devices, on_device(): own = lax.all_to_all(outgoing, ep, split_axis=0, concat_axis=0, tiled=True)  5.67 us
  transfers between devices with their start and end apart: 27, of which 11 were waited for; matrix products, arithmetic and copies ran while one was open for 3% of the time, Pallas kernels for 13%

profile of v6, /device:TPU:0, one launch (start us, length us, event | category | flops | bytes accessed | tf_op | source)
XLA Modules:
  0.0 138.0 jit_solution(9866574940777399038)
XLA Ops:
  0.7 2.4 %pre.1 = bf16[128,2048]{1,0:T(8,128)(2,1)} custom-call(bf16[32,2048]{1,0:T(8,128)(2,1)} %x_ref.1, s32[2,32]{1,0:T(2,128)} %bitcast.39, f32[1,2048]{1,0:T(1,128)} %bitcast.43), custom_call_target="tpu_custom_call" | custom-call | flops 2000000000 | bytes 1000000 | tf_op jit(solution)/shard_map/pre/pallas_call | solution.py:423
  3.1 8.0 %all-to-all-start = ((bf16[16,8,2048]{2,1,0:T(8,128)(2,1)}), bf16[16,8,2048]{2,1,0:T(8,128)(2,1)S(1)}, u32[]{:S(2)}, u32[]{:S(2)}) async-start(bf16[16,8,2048]{2,1,0:T(8,128)(2,1)} %bitcast.17), calls=%async_computation | async-start | bytes 1048576 | tf_op jit(solution)/shard_map/all_to_all | solution.py:430
  11.3 5.6 %local.1 = (bf16[2048,256]{1,0:T(8,128)(2,1)}, bf16[2048,256]{1,0:T(8,128)(2,1)}, bf16[264,256]{1,0:T(8,128)(2,1)S(1)}) custom-call(f32[4,2,128]{2,1,0:T(2,128)S(1)} %pad_maximum_fusion.base_ref, bf16[2048,256]{1,0:T(8,128)(2,1)S(1)} %copy-done.7, bf16[2048,256]{1,0:T(8,128)(2,1)S(1)} %copy-done.8, bf16[2048,256]{1,0:T(8,128)(2,1)} %v_ref.1, ...), custom_call_target="tpu_custom_call" | custom-call | flops 6000000000 | bytes 6291456 | tf_op jit(solution)/shard_map/local/pallas_call | solution.py:230
  17.0 5.7 %all-to-all-done = bf16[16,8,2048]{2,1,0:T(8,128)(2,1)S(1)} async-done(((bf16[16,8,2048]{2,1,0:T(8,128)(2,1)}), bf16[16,8,2048]{2,1,0:T(8,128)(2,1)S(1)}, u32[]{:S(2)}, u32[]{:S(2)}) %all-to-all-start) | async-done | bytes 524320 | tf_op jit(solution)/shard_map/all_to_all | solution.py:430
  22.6 1.6 %collective-permute-start.13 = (bf16[128,2048]{1,0:T(8,128)(2,1)S(1)}, bf16[128,2048]{1,0:T(8,128)(2,1)S(1)}, u32[]{:S(2)}, u32[]{:S(2)}) collective-permute-start(bf16[128,2048]{1,0:T(8,128)(2,1)S(1)} %bitcast.33), channel_id=1, source_target_pairs={{0,2},{2,4},{4,6},{6,0},{1,3},{3,5},{5,7},{7,1},{8,10},{10,12},{12... | collective-permute-start | bytes 1572872 | tf_op jit(solution)/shard_map/ppermute | solution.py:37
  24.2 1.7 %collective-permute-start.14 = (bf16[128,2048]{1,0:T(8,128)(2,1)S(1)}, bf16[128,2048]{1,0:T(8,128)(2,1)S(1)}, u32[]{:S(2)}, u32[]{:S(2)}) collective-permute-start(bf16[128,2048]{1,0:T(8,128)(2,1)S(1)} %bitcast.34), channel_id=1, source_target_pairs={{0,6},{2,0},{4,2},{6,4},{1,7},{3,1},{5,3},{7,5},{8,14},{10,8},{12,... | collective-permute-start | bytes 1572872 | tf_op jit(solution)/shard_map/ppermute | solution.py:37
  25.9 10.3 %collective-permute-done.13.refs_1_ = bf16[128,2048]{1,0:T(8,128)(2,1)S(1)} collective-permute-done((bf16[128,2048]{1,0:T(8,128)(2,1)S(1)}, bf16[128,2048]{1,0:T(8,128)(2,1)S(1)}, u32[]{:S(2)}, u32[]{:S(2)}) %collective-permute-start.13) | collective-permute-done | bytes 524320 | tf_op jit(solution)/shard_map/ppermute | solution.py:37
  36.2 0.5 collective-permute-start.17
  36.7 1.4 %collective-permute-done.16.refs_4_ = bf16[128,2048]{1,0:T(8,128)(2,1)S(1)} collective-permute-done((bf16[128,2048]{1,0:T(8,128)(2,1)S(1)}, bf16[128,2048]{1,0:T(8,128)(2,1)S(1)}, u32[]{:S(2)}, u32[]{:S(2)}) %collective-permute-start.16) | collective-permute-done | bytes 524320 | tf_op jit(solution)/shard_map/ppermute | solution.py:37
  38.1 0.7 collective-permute-done.17.refs_5_
  38.8 2.0 %copy-done = bf16[1,2048,896]{2,1,0:T(8,128)(2,1)S(1)} copy-done((bf16[1,2048,896]{2,1,0:T(8,128)(2,1)S(1)}, bf16[1,2048,896]{2,1,0:T(8,128)(2,1)}, u32[]{:S(2)}) %copy-start) | copy-done | bytes 3670040
  40.9 2.0 %copy-done.2 = bf16[1,2048,896]{2,1,0:T(8,128)(2,1)S(1)} copy-done((bf16[1,2048,896]{2,1,0:T(8,128)(2,1)S(1)}, bf16[1,2048,896]{2,1,0:T(8,128)(2,1)}, u32[]{:S(2)}) %copy-start.2) | copy-done | bytes 3670040
  42.9 2.0 %copy-done.4 = bf16[1,896,2048]{2,1,0:T(8,128)(2,1)S(1)} copy-done((bf16[1,896,2048]{2,1,0:T(8,128)(2,1)S(1)}, bf16[1,896,2048]{2,1,0:T(8,128)(2,1)}, u32[]{:S(2)}) %copy-start.4) | copy-done | bytes 3670040
  45.0 10.8 %shard_map.176 = (bf16[128,2048]{1,0:T(8,128)(2,1)S(1)}, bf16[128,2048]{1,0:T(8,128)(2,1)S(1)}, bf16[128,2048]{1,0:T(8,128)(2,1)S(1)}, bf16[384,2048]{1,0:T(8,128)(2,1)}) custom-call(bf16[128,2048]{1,0:T(8,128)(2,1)S(1)} %bitcast.36, bf16[128,2048]{1,0:T(8,128)(2,1)S(1)} %collective-permute-done.13.refs_1_, ...), custom_call_target="tpu_custom_call" | custom-call | flops 8455716864 | bytes 17301504 | tf_op jit(solution)/shard_map/pallas_call | solution.py:129
  55.9 2.2 %collective-permute-start.21 = (bf16[128,2048]{1,0:T(8,128)(2,1)S(1)}, bf16[128,2048]{1,0:T(8,128)(2,1)S(1)}, u32[]{:S(2)}, u32[]{:S(2)}) collective-permute-start(bf16[128,2048]{1,0:T(8,128)(2,1)S(1)} %bitcast.37), channel_id=1, source_target_pairs={{0,4},{2,6},{4,0},{6,2},{1,5},{3,7},{5,1},{7,3},{8,12},{10,14},{12... | collective-permute-start | bytes 1572872 | tf_op jit(solution)/shard_map/ppermute | solution.py:37
  58.0 0.6 collective-permute-start
  58.6 1.7 %collective-permute-start.1 = (bf16[264,256]{1,0:T(8,128)(2,1)S(1)}, bf16[264,256]{1,0:T(8,128)(2,1)S(1)}, u32[]{:S(2)}, u32[]{:S(2)}) collective-permute-start(bf16[264,256]{1,0:T(8,128)(2,1)S(1)} %get-tuple-element.20.own_ref), channel_id=1, source_target_pairs={{0,16},{8,24},{16,0},{24,8},{1,17},{9,25},{17,1},{25,9},{2,18},{10... | collective-permute-start | bytes 405512 | tf_op jit(solution)/shard_map/ppermute | solution.py:37
  60.3 1.2 collective-permute-start.2
  61.5 10.1 %collective-permute-done.21.refs_0_ = bf16[128,2048]{1,0:T(8,128)(2,1)S(1)} collective-permute-done((bf16[128,2048]{1,0:T(8,128)(2,1)S(1)}, bf16[128,2048]{1,0:T(8,128)(2,1)S(1)}, u32[]{:S(2)}, u32[]{:S(2)}) %collective-permute-start.21) | collective-permute-done | bytes 524320 | tf_op jit(solution)/shard_map/ppermute | solution.py:37
  71.6 1.9 %add_convert_fusion.2 = (bf16[128,2048]{1,0:T(8,128)(2,1)S(1)}, bf16[128,2048]{1,0:T(8,128)(2,1)S(1)}, bf16[128,2048]{1,0:T(8,128)(2,1)S(1)}) fusion(bf16[128,2048]{1,0:T(8,128)(2,1)S(1)} %get-tuple-element.29, bf16[384,2048]{1,0:T(8,128)(2,1)} %collective-permute-done.18, bf16[128,2048]{1,0:T(8,128)(2,1)S(1)} %get-tuple-element.28, ...), kind=kLoop, calls=%fused_computation.2 | loop fusion | flops 3145728 | bytes 4718592 | tf_op jit(solution)/shard_map/convert_element_type | solution.py:464
  73.5 2.0 %copy-done.3 = bf16[1,2048,896]{2,1,0:T(8,128)(2,1)S(1)} copy-done((bf16[1,2048,896]{2,1,0:T(8,128)(2,1)S(1)}, bf16[1,2048,896]{2,1,0:T(8,128)(2,1)}, u32[]{:S(2)}) %copy-start.3) | copy-done | bytes 3670040
  75.6 2.0 %copy-done.5 = bf16[1,896,2048]{2,1,0:T(8,128)(2,1)S(1)} copy-done((bf16[1,896,2048]{2,1,0:T(8,128)(2,1)S(1)}, bf16[1,896,2048]{2,1,0:T(8,128)(2,1)}, u32[]{:S(2)}) %copy-start.5) | copy-done | bytes 3670040
  77.6 3.3 %shard_map.177 = (bf16[128,2048]{1,0:T(8,128)(2,1)S(1)}, bf16[128,2048]{1,0:T(8,128)(2,1)S(1)}) custom-call(bf16[128,2048]{1,0:T(8,128)(2,1)S(1)} %collective-permute-done.21.refs_0_, bf16[128,2048]{1,0:T(8,128)(2,1)S(1)} %collective-permute-done.22.refs_1_, bf16[2048,896]{1,0:T(8,128)(2,1)S(1)} %bitcast.27, bf16[2048,896]{1,0:T(8,128)(2,1)S(1)} %bitcast.29, ...), custom_call_target="tpu_custom_call" | custom-call | flops 2818572288 | bytes 13107200 | tf_op jit(solution)/shard_map/pallas_call | solution.py:129
  80.9 0.6 collective-permute-start.23
  81.5 0.3 middle.1
  81.9 2.6 %collective-permute-start.4 = (bf16[264,256]{1,0:T(8,128)(2,1)S(1)}, bf16[264,256]{1,0:T(8,128)(2,1)S(1)}, u32[]{:S(2)}, u32[]{:S(2)}) collective-permute-start(bf16[264,256]{1,0:T(8,128)(2,1)S(1)} %get-tuple-element.22), channel_id=1, source_target_pairs={{0,64},{32,96},{64,0},{96,32},{1,65},{33,97},{65,1},{97,33},{2,66}... | collective-permute-start | bytes 405512 | tf_op jit(solution)/shard_map/ppermute | solution.py:37
  84.5 1.5 %collective-permute-start.5 = (bf16[264,256]{1,0:T(8,128)(2,1)S(1)}, bf16[264,256]{1,0:T(8,128)(2,1)S(1)}, u32[]{:S(2)}, u32[]{:S(2)}) collective-permute-start(bf16[264,256]{1,0:T(8,128)(2,1)S(1)} %get-tuple-element.22), channel_id=1, source_target_pairs={{0,96},{32,0},{64,32},{96,64},{1,97},{33,1},{65,33},{97,65},{2,98}... | collective-permute-start | bytes 405512 | tf_op jit(solution)/shard_map/ppermute | solution.py:37
  86.0 0.9 collective-permute-start.20
  86.8 2.4 %collective-permute-start.19 = (bf16[128,2048]{1,0:T(8,128)(2,1)S(1)}, bf16[128,2048]{1,0:T(8,128)(2,1)S(1)}, u32[]{:S(2)}, u32[]{:S(2)}) collective-permute-start(bf16[128,2048]{1,0:T(8,128)(2,1)S(1)} %get-tuple-element.31), channel_id=1, source_target_pairs={{0,6},{2,0},{4,2},{6,4},{1,7},{3,1},{5,3},{7,5},{8,14},{10,8},{12,... | collective-permute-start | bytes 1572872 | tf_op jit(solution)/shard_map/ppermute | solution.py:37
  89.3 2.2 %collective-permute-done.3.one_ref = bf16[264,256]{1,0:T(8,128)(2,1)S(1)} collective-permute-done((bf16[264,256]{1,0:T(8,128)(2,1)S(1)}, bf16[264,256]{1,0:T(8,128)(2,1)S(1)}, u32[]{:S(2)}, u32[]{:S(2)}) %collective-permute-start.3) | collective-permute-done | bytes 135200 | tf_op jit(solution)/shard_map/ppermute | solution.py:37
  91.5 2.2 %collective-permute-start.24 = (bf16[128,2048]{1,0:T(8,128)(2,1)S(1)}, bf16[128,2048]{1,0:T(8,128)(2,1)S(1)}, u32[]{:S(2)}, u32[]{:S(2)}) collective-permute-start(bf16[128,2048]{1,0:T(8,128)(2,1)S(1)} %add_convert_fusion.1), channel_id=1, source_target_pairs={{0,4},{2,6},{4,0},{6,2},{1,5},{3,7},{5,1},{7,3},{8,12},{10,14},{12... | collective-permute-start | bytes 1572872 | tf_op jit(solution)/shard_map/ppermute | solution.py:37
  93.7 4.3 %finish.1 = bf16[2048,256]{1,0:T(8,128)(2,1)S(1)} custom-call(s32[3]{0:T(128)S(1)} %pad_add_fusion.place_ref, f32[264,256]{1,0:T(8,128)S(1)} %get-tuple-element.21.before_ref, bf16[264,256]{1,0:T(8,128)(2,1)S(1)} %collective-permute-done.3.one_ref, bf16[264,256]{1,0:T(8,128)(2,1)S(1)} %collective-permute-done.4.two_ref, ...), custom_call_target="tpu_custom_call" | custom-call | flops 2000000000 | bytes 5242880 | tf_op jit(solution)/shard_map/finish/pallas_call | solution.py:340
  98.1 1.0 collective-permute-start.7
  99.1 0.4 collective-permute-done.6.refs_1_
  99.5 0.6 collective-permute-start.8
  100.1 14.6 %collective-permute-done.7.refs_2_ = bf16[256,256]{1,0:T(8,128)(2,1)S(1)} collective-permute-done((bf16[256,256]{1,0:T(8,128)(2,1)S(1)}, bf16[256,256]{1,0:T(8,128)(2,1)S(1)}, u32[]{:S(2)}, u32[]{:S(2)}) %collective-permute-start.7) | collective-permute-done | bytes 131104 | tf_op jit(solution)/shard_map/ppermute | solution.py:490
  114.7 0.9 collective-permute-start.9
  115.7 1.9 %collective-permute-start.10 = (bf16[256,256]{1,0:T(8,128)(2,1)S(1)}, bf16[256,256]{1,0:T(8,128)(2,1)S(1)}, u32[]{:S(2)}, u32[]{:S(2)}) collective-permute-start(bf16[256,256]{1,0:T(8,128)(2,1)S(1)} %get-tuple-element.41), channel_id=1, source_target_pairs={{0,5},{1,4},{2,7},{3,6},{4,1},{5,0},{6,3},{7,2},{8,13},{9,12},{10,... | collective-permute-start | bytes 393224 | tf_op jit(solution)/shard_map/ppermute | solution.py:490
  117.6 0.5 collective-permute-start.11
  118.1 1.9 %collective-permute-start.12 = (bf16[256,256]{1,0:T(8,128)(2,1)S(1)}, bf16[256,256]{1,0:T(8,128)(2,1)S(1)}, u32[]{:S(2)}, u32[]{:S(2)}) collective-permute-start(bf16[256,256]{1,0:T(8,128)(2,1)S(1)} %get-tuple-element.39), channel_id=1, source_target_pairs={{0,7},{1,6},{2,1},{3,0},{4,3},{5,2},{6,5},{7,4},{8,15},{9,14},{10,... | collective-permute-start | bytes 393224 | tf_op jit(solution)/shard_map/ppermute | solution.py:490
  120.0 1.1 fusion
  121.2 3.7 %all-to-all-start.1 = ((bf16[16,8,2048]{2,1,0:T(8,128)(2,1)}), bf16[16,8,2048]{2,1,0:T(8,128)(2,1)S(1)}, u32[]{:S(2)}, u32[]{:S(2)}) async-start(bf16[16,8,2048]{2,1,0:T(8,128)(2,1)} %fusion), calls=%async_computation.1 | async-start | bytes 1048576 | tf_op jit(solution)/shard_map/all_to_all | solution.py:495
  125.0 1.8 %collective-permute-done.11.refs_6_ = bf16[256,256]{1,0:T(8,128)(2,1)S(1)} collective-permute-done((bf16[256,256]{1,0:T(8,128)(2,1)S(1)}, bf16[256,256]{1,0:T(8,128)(2,1)S(1)}, u32[]{:S(2)}, u32[]{:S(2)}) %collective-permute-start.11) | collective-permute-done | bytes 131104 | tf_op jit(solution)/shard_map/ppermute | solution.py:490
  126.8 1.5 %collective-permute-done.12.refs_7_ = bf16[256,256]{1,0:T(8,128)(2,1)S(1)} collective-permute-done((bf16[256,256]{1,0:T(8,128)(2,1)S(1)}, bf16[256,256]{1,0:T(8,128)(2,1)S(1)}, u32[]{:S(2)}, u32[]{:S(2)}) %collective-permute-start.12) | collective-permute-done | bytes 131104 | tf_op jit(solution)/shard_map/ppermute | solution.py:490
  128.3 3.4 %copy-done.6 = bf16[2048,2048]{1,0:T(8,128)(2,1)S(1)} copy-done((bf16[2048,2048]{1,0:T(8,128)(2,1)S(1)}, bf16[2048,2048]{1,0:T(8,128)(2,1)}, u32[]{:S(2)}) %copy-start.6) | copy-done | bytes 8388632
  131.7 4.8 %project.1 = bf16[256,2048]{1,0:T(8,128)(2,1)} custom-call(s32[8]{0:T(128)S(1)} %stack.52.head_ref, bf16[256,256]{1,0:T(8,128)(2,1)S(1)} %get-tuple-element.46.refs_0_, bf16[256,256]{1,0:T(8,128)(2,1)S(1)} %collective-permute-done.6.refs_1_, bf16[256,256]{1,0:T(8,128)(2,1)S(1)} %collective-permute-done.7.refs_2_, ...), custom_call_target="tpu_custom_call" | custom-call | flops 4000000000 | bytes 10485760 | tf_op jit(solution)/shard_map/project/pallas_call | solution.py:376
  136.5 0.3 all-to-all-done.1
  136.7 1.2 combine.1
  (54 shorter events, 0.9 us)
Async XLA Ops:
  0.6 10.6 %copy-start.14 = (f32[128]{0:T(128)S(1)}, f32[128]{0:T(128)}, u32[]{:S(2)}) copy-start(f32[128]{0:T(128)} %constant.52.clone) | copy-start | bytes 1540
  0.6 10.6 %copy-start.7 = (bf16[2048,256]{1,0:T(8,128)(2,1)S(1)}, bf16[2048,256]{1,0:T(8,128)(2,1)}, u32[]{:S(2)}) copy-start(bf16[2048,256]{1,0:T(8,128)(2,1)} %q_ref) | copy-start | bytes 3145732
  0.7 10.6 %copy-start.8 = (bf16[2048,256]{1,0:T(8,128)(2,1)S(1)}, bf16[2048,256]{1,0:T(8,128)(2,1)}, u32[]{:S(2)}) copy-start(bf16[2048,256]{1,0:T(8,128)(2,1)} %k_ref.1) | copy-start | bytes 3145732
  0.7 10.6 %copy-start.9 = (f32[2048,1]{0,1:T(1,128)S(1)}, f32[2048,1]{0,1:T(1,128)}, u32[]{:S(2)}) copy-start(f32[2048,1]{0,1:T(1,128)} %param.21) | copy-start | bytes 24580
  0.7 10.6 %copy-start.12 = (f32[512,128]{1,0:T(8,128)S(1)}, f32[512,128]{1,0:T(8,128)}, u32[]{:S(2)}) copy-start(f32[512,128]{1,0:T(8,128)} %constant.53.clone.cos_ref) | copy-start | bytes 786436
  0.7 10.6 %copy-start.13 = (f32[512,128]{1,0:T(8,128)S(1)}, f32[512,128]{1,0:T(8,128)}, u32[]{:S(2)}) copy-start(f32[512,128]{1,0:T(8,128)} %constant.54.clone.sin_ref) | copy-start | bytes 786436
  3.1 19.5 %all-to-all-start = ((bf16[16,8,2048]{2,1,0:T(8,128)(2,1)}), bf16[16,8,2048]{2,1,0:T(8,128)(2,1)S(1)}, u32[]{:S(2)}, u32[]{:S(2)}) async-start(bf16[16,8,2048]{2,1,0:T(8,128)(2,1)} %bitcast.17), calls=%async_computation | async-start | bytes 1048576 | tf_op jit(solution)/shard_map/all_to_all | solution.py:430
  22.6 13.5 %collective-permute-start.13 = (bf16[128,2048]{1,0:T(8,128)(2,1)S(1)}, bf16[128,2048]{1,0:T(8,128)(2,1)S(1)}, u32[]{:S(2)}, u32[]{:S(2)}) collective-permute-start(bf16[128,2048]{1,0:T(8,128)(2,1)S(1)} %bitcast.33), channel_id=1, source_target_pairs={{0,2},{2,4},{4,6},{6,0},{1,3},{3,5},{5,7},{7,1},{8,10},{10,12},{12... | collective-permute-start | bytes 1572872 | tf_op jit(solution)/shard_map/ppermute | solution.py:37
  24.2 12.0 %collective-permute-start.14 = (bf16[128,2048]{1,0:T(8,128)(2,1)S(1)}, bf16[128,2048]{1,0:T(8,128)(2,1)S(1)}, u32[]{:S(2)}, u32[]{:S(2)}) collective-permute-start(bf16[128,2048]{1,0:T(8,128)(2,1)S(1)} %bitcast.34), channel_id=1, source_target_pairs={{0,6},{2,0},{4,2},{6,4},{1,7},{3,1},{5,3},{7,5},{8,14},{10,8},{12,... | collective-permute-start | bytes 1572872 | tf_op jit(solution)/shard_map/ppermute | solution.py:37
  25.9 10.8 %collective-permute-start.15 = (bf16[128,2048]{1,0:T(8,128)(2,1)S(1)}, bf16[128,2048]{1,0:T(8,128)(2,1)S(1)}, u32[]{:S(2)}, u32[]{:S(2)}) collective-permute-start(bf16[128,2048]{1,0:T(8,128)(2,1)S(1)} %bitcast.35), channel_id=1, source_target_pairs={{0,1},{1,0},{2,3},{3,2},{4,5},{5,4},{6,7},{7,6},{8,9},{9,8},{10,11... | collective-permute-start | bytes 1572872 | tf_op jit(solution)/shard_map/ppermute | solution.py:37
  36.2 1.9 %collective-permute-start.16 = (bf16[128,2048]{1,0:T(8,128)(2,1)S(1)}, bf16[128,2048]{1,0:T(8,128)(2,1)S(1)}, u32[]{:S(2)}, u32[]{:S(2)}) collective-permute-start(bf16[128,2048]{1,0:T(8,128)(2,1)S(1)} %collective-permute-done.13.refs_1_), channel_id=1, source_target_pairs={{0,1},{1,0},{2,3},{3,2},{4,5},{5,4},{6,7},{7,6},{8,9},{9,8},{10,11... | collective-permute-start | bytes 1572872 | tf_op jit(solution)/shard_map/ppermute | solution.py:37
  36.2 2.6 %collective-permute-start.17 = (bf16[128,2048]{1,0:T(8,128)(2,1)S(1)}, bf16[128,2048]{1,0:T(8,128)(2,1)S(1)}, u32[]{:S(2)}, u32[]{:S(2)}) collective-permute-start(bf16[128,2048]{1,0:T(8,128)(2,1)S(1)} %collective-permute-done.14.refs_2_), channel_id=1, source_target_pairs={{0,1},{1,0},{2,3},{3,2},{4,5},{5,4},{6,7},{7,6},{8,9},{9,8},{10,11... | collective-permute-start | bytes 1572872 | tf_op jit(solution)/shard_map/ppermute | solution.py:37
  38.8 2.0 %copy-start = (bf16[1,2048,896]{2,1,0:T(8,128)(2,1)S(1)}, bf16[1,2048,896]{2,1,0:T(8,128)(2,1)}, u32[]{:S(2)}) copy-start(bf16[1,2048,896]{2,1,0:T(8,128)(2,1)} %param.28) | copy-start | bytes 11010052
  40.9 2.0 %copy-start.2 = (bf16[1,2048,896]{2,1,0:T(8,128)(2,1)S(1)}, bf16[1,2048,896]{2,1,0:T(8,128)(2,1)}, u32[]{:S(2)}) copy-start(bf16[1,2048,896]{2,1,0:T(8,128)(2,1)} %param.29) | copy-start | bytes 11010052
  42.9 2.0 %copy-start.4 = (bf16[1,896,2048]{2,1,0:T(8,128)(2,1)S(1)}, bf16[1,896,2048]{2,1,0:T(8,128)(2,1)}, u32[]{:S(2)}) copy-start(bf16[1,896,2048]{2,1,0:T(8,128)(2,1)} %param.30) | copy-start | bytes 11010052
  55.7 15.9 %collective-permute-start.18 = (bf16[384,2048]{1,0:T(8,128)(2,1)}, bf16[384,2048]{1,0:T(8,128)(2,1)}, u32[]{:S(2)}, u32[]{:S(2)}) collective-permute-start(bf16[384,2048]{1,0:T(8,128)(2,1)} %get-tuple-element.27), channel_id=1, source_target_pairs={{0,1},{1,0},{2,3},{3,2},{4,5},{5,4},{6,7},{7,6},{8,9},{9,8},{10,11... | collective-permute-start | bytes 4718600 | tf_op jit(solution)/shard_map/ppermute | solution.py:37
  55.9 15.7 %collective-permute-start.21 = (bf16[128,2048]{1,0:T(8,128)(2,1)S(1)}, bf16[128,2048]{1,0:T(8,128)(2,1)S(1)}, u32[]{:S(2)}, u32[]{:S(2)}) collective-permute-start(bf16[128,2048]{1,0:T(8,128)(2,1)S(1)} %bitcast.37), channel_id=1, source_target_pairs={{0,4},{2,6},{4,0},{6,2},{1,5},{3,7},{5,1},{7,3},{8,12},{10,14},{12... | collective-permute-start | bytes 1572872 | tf_op jit(solution)/shard_map/ppermute | solution.py:37
  58.0 23.5 %collective-permute-start = (bf16[264,256]{1,0:T(8,128)(2,1)S(1)}, bf16[264,256]{1,0:T(8,128)(2,1)S(1)}, u32[]{:S(2)}, u32[]{:S(2)}) collective-permute-start(bf16[264,256]{1,0:T(8,128)(2,1)S(1)} %get-tuple-element.20.own_ref), channel_id=1, source_target_pairs={{0,8},{8,16},{16,24},{24,0},{1,9},{9,17},{17,25},{25,1},{2,10},{10... | collective-permute-start | bytes 405512 | tf_op jit(solution)/shard_map/ppermute | solution.py:37
  58.6 22.9 %collective-permute-start.1 = (bf16[264,256]{1,0:T(8,128)(2,1)S(1)}, bf16[264,256]{1,0:T(8,128)(2,1)S(1)}, u32[]{:S(2)}, u32[]{:S(2)}) collective-permute-start(bf16[264,256]{1,0:T(8,128)(2,1)S(1)} %get-tuple-element.20.own_ref), channel_id=1, source_target_pairs={{0,16},{8,24},{16,0},{24,8},{1,17},{9,25},{17,1},{25,9},{2,18},{10... | collective-permute-start | bytes 405512 | tf_op jit(solution)/shard_map/ppermute | solution.py:37
  60.3 21.2 %collective-permute-start.2 = (bf16[264,256]{1,0:T(8,128)(2,1)S(1)}, bf16[264,256]{1,0:T(8,128)(2,1)S(1)}, u32[]{:S(2)}, u32[]{:S(2)}) collective-permute-start(bf16[264,256]{1,0:T(8,128)(2,1)S(1)} %get-tuple-element.20.own_ref), channel_id=1, source_target_pairs={{0,24},{8,0},{16,8},{24,16},{1,25},{9,1},{17,9},{25,17},{2,26},{10... | collective-permute-start | bytes 405512 | tf_op jit(solution)/shard_map/ppermute | solution.py:37
  61.4 12.1 %copy-start.1 = (bf16[1,2048,896]{2,1,0:T(8,128)(2,1)S(1)}, bf16[1,2048,896]{2,1,0:T(8,128)(2,1)}, u32[]{:S(2)}) copy-start(bf16[1,2048,896]{2,1,0:T(8,128)(2,1)} %param.28) | copy-start | bytes 11010052
  71.6 1.9 %collective-permute-start.22 = (bf16[128,2048]{1,0:T(8,128)(2,1)S(1)}, bf16[128,2048]{1,0:T(8,128)(2,1)S(1)}, u32[]{:S(2)}, u32[]{:S(2)}) collective-permute-start(bf16[128,2048]{1,0:T(8,128)(2,1)S(1)} %collective-permute-done.21.refs_0_), channel_id=1, source_target_pairs={{0,1},{1,0},{2,3},{3,2},{4,5},{5,4},{6,7},{7,6},{8,9},{9,8},{10,11... | collective-permute-start | bytes 1572872 | tf_op jit(solution)/shard_map/ppermute | solution.py:37
  73.5 2.0 %copy-start.3 = (bf16[1,2048,896]{2,1,0:T(8,128)(2,1)S(1)}, bf16[1,2048,896]{2,1,0:T(8,128)(2,1)}, u32[]{:S(2)}) copy-start(bf16[1,2048,896]{2,1,0:T(8,128)(2,1)} %param.29) | copy-start | bytes 11010052
  75.6 2.0 %copy-start.5 = (bf16[1,896,2048]{2,1,0:T(8,128)(2,1)S(1)}, bf16[1,896,2048]{2,1,0:T(8,128)(2,1)}, u32[]{:S(2)}) copy-start(bf16[1,896,2048]{2,1,0:T(8,128)(2,1)} %param.30) | copy-start | bytes 11010052
  80.9 5.9 %collective-permute-start.23 = (bf16[128,2048]{1,0:T(8,128)(2,1)S(1)}, bf16[128,2048]{1,0:T(8,128)(2,1)S(1)}, u32[]{:S(2)}, u32[]{:S(2)}) collective-permute-start(bf16[128,2048]{1,0:T(8,128)(2,1)S(1)} %get-tuple-element.35), channel_id=1, source_target_pairs={{0,1},{1,0},{2,3},{3,2},{4,5},{5,4},{6,7},{7,6},{8,9},{9,8},{10,11... | collective-permute-start | bytes 1572872 | tf_op jit(solution)/shard_map/ppermute | solution.py:37
  81.8 9.7 %collective-permute-start.3 = (bf16[264,256]{1,0:T(8,128)(2,1)S(1)}, bf16[264,256]{1,0:T(8,128)(2,1)S(1)}, u32[]{:S(2)}, u32[]{:S(2)}) collective-permute-start(bf16[264,256]{1,0:T(8,128)(2,1)S(1)} %get-tuple-element.22), channel_id=1, source_target_pairs={{0,32},{32,64},{64,96},{96,0},{1,33},{33,65},{65,97},{97,1},{2,34}... | collective-permute-start | bytes 405512 | tf_op jit(solution)/shard_map/ppermute | solution.py:37
  81.9 11.8 %collective-permute-start.4 = (bf16[264,256]{1,0:T(8,128)(2,1)S(1)}, bf16[264,256]{1,0:T(8,128)(2,1)S(1)}, u32[]{:S(2)}, u32[]{:S(2)}) collective-permute-start(bf16[264,256]{1,0:T(8,128)(2,1)S(1)} %get-tuple-element.22), channel_id=1, source_target_pairs={{0,64},{32,96},{64,0},{96,32},{1,65},{33,97},{65,1},{97,33},{2,66}... | collective-permute-start | bytes 405512 | tf_op jit(solution)/shard_map/ppermute | solution.py:37
  84.5 9.2 %collective-permute-start.5 = (bf16[264,256]{1,0:T(8,128)(2,1)S(1)}, bf16[264,256]{1,0:T(8,128)(2,1)S(1)}, u32[]{:S(2)}, u32[]{:S(2)}) collective-permute-start(bf16[264,256]{1,0:T(8,128)(2,1)S(1)} %get-tuple-element.22), channel_id=1, source_target_pairs={{0,96},{32,0},{64,32},{96,64},{1,97},{33,1},{65,33},{97,65},{2,98}... | collective-permute-start | bytes 405512 | tf_op jit(solution)/shard_map/ppermute | solution.py:37
  86.0 29.7 %collective-permute-start.20 = (bf16[128,2048]{1,0:T(8,128)(2,1)S(1)}, bf16[128,2048]{1,0:T(8,128)(2,1)S(1)}, u32[]{:S(2)}, u32[]{:S(2)}) collective-permute-start(bf16[128,2048]{1,0:T(8,128)(2,1)S(1)} %get-tuple-element.32), channel_id=1, source_target_pairs={{0,2},{2,4},{4,6},{6,0},{1,3},{3,5},{5,7},{7,1},{8,10},{10,12},{12... | collective-permute-start | bytes 1572872 | tf_op jit(solution)/shard_map/ppermute | solution.py:37
  86.8 30.8 %collective-permute-start.19 = (bf16[128,2048]{1,0:T(8,128)(2,1)S(1)}, bf16[128,2048]{1,0:T(8,128)(2,1)S(1)}, u32[]{:S(2)}, u32[]{:S(2)}) collective-permute-start(bf16[128,2048]{1,0:T(8,128)(2,1)S(1)} %get-tuple-element.31), channel_id=1, source_target_pairs={{0,6},{2,0},{4,2},{6,4},{1,7},{3,1},{5,3},{7,5},{8,14},{10,8},{12,... | collective-permute-start | bytes 1572872 | tf_op jit(solution)/shard_map/ppermute | solution.py:37
  91.5 26.6 %collective-permute-start.24 = (bf16[128,2048]{1,0:T(8,128)(2,1)S(1)}, bf16[128,2048]{1,0:T(8,128)(2,1)S(1)}, u32[]{:S(2)}, u32[]{:S(2)}) collective-permute-start(bf16[128,2048]{1,0:T(8,128)(2,1)S(1)} %add_convert_fusion.1), channel_id=1, source_target_pairs={{0,4},{2,6},{4,0},{6,2},{1,5},{3,7},{5,1},{7,3},{8,12},{10,14},{12... | collective-permute-start | bytes 1572872 | tf_op jit(solution)/shard_map/ppermute | solution.py:37
  98.0 1.4 %collective-permute-start.6 = (bf16[256,256]{1,0:T(8,128)(2,1)S(1)}, bf16[256,256]{1,0:T(8,128)(2,1)S(1)}, u32[]{:S(2)}, u32[]{:S(2)}) collective-permute-start(bf16[256,256]{1,0:T(8,128)(2,1)S(1)} %get-tuple-element.45), channel_id=1, source_target_pairs={{0,1},{1,0},{2,3},{3,2},{4,5},{5,4},{6,7},{7,6},{8,9},{9,8},{10,11... | collective-permute-start | bytes 393224 | tf_op jit(solution)/shard_map/ppermute | solution.py:490
  98.1 16.6 %collective-permute-start.7 = (bf16[256,256]{1,0:T(8,128)(2,1)S(1)}, bf16[256,256]{1,0:T(8,128)(2,1)S(1)}, u32[]{:S(2)}, u32[]{:S(2)}) collective-permute-start(bf16[256,256]{1,0:T(8,128)(2,1)S(1)} %get-tuple-element.44), channel_id=1, source_target_pairs={{0,2},{1,3},{2,4},{3,5},{4,6},{5,7},{6,0},{7,1},{8,10},{9,11},{10,... | collective-permute-start | bytes 393224 | tf_op jit(solution)/shard_map/ppermute | solution.py:490
  99.5 25.5 %collective-permute-start.8 = (bf16[256,256]{1,0:T(8,128)(2,1)S(1)}, bf16[256,256]{1,0:T(8,128)(2,1)S(1)}, u32[]{:S(2)}, u32[]{:S(2)}) collective-permute-start(bf16[256,256]{1,0:T(8,128)(2,1)S(1)} %get-tuple-element.43), channel_id=1, source_target_pairs={{0,3},{1,2},{2,5},{3,4},{4,7},{5,6},{6,1},{7,0},{8,11},{9,10},{10,... | collective-permute-start | bytes 393224 | tf_op jit(solution)/shard_map/ppermute | solution.py:490
  114.7 10.2 %collective-permute-start.9 = (bf16[256,256]{1,0:T(8,128)(2,1)S(1)}, bf16[256,256]{1,0:T(8,128)(2,1)S(1)}, u32[]{:S(2)}, u32[]{:S(2)}) collective-permute-start(bf16[256,256]{1,0:T(8,128)(2,1)S(1)} %get-tuple-element.42), channel_id=1, source_target_pairs={{0,4},{1,5},{2,6},{3,7},{4,0},{5,1},{6,2},{7,3},{8,12},{9,13},{10,... | collective-permute-start | bytes 393224 | tf_op jit(solution)/shard_map/ppermute | solution.py:490
  115.7 9.3 %collective-permute-start.10 = (bf16[256,256]{1,0:T(8,128)(2,1)S(1)}, bf16[256,256]{1,0:T(8,128)(2,1)S(1)}, u32[]{:S(2)}, u32[]{:S(2)}) collective-permute-start(bf16[256,256]{1,0:T(8,128)(2,1)S(1)} %get-tuple-element.41), channel_id=1, source_target_pairs={{0,5},{1,4},{2,7},{3,6},{4,1},{5,0},{6,3},{7,2},{8,13},{9,12},{10,... | collective-permute-start | bytes 393224 | tf_op jit(solution)/shard_map/ppermute | solution.py:490
  117.6 9.2 %collective-permute-start.11 = (bf16[256,256]{1,0:T(8,128)(2,1)S(1)}, bf16[256,256]{1,0:T(8,128)(2,1)S(1)}, u32[]{:S(2)}, u32[]{:S(2)}) collective-permute-start(bf16[256,256]{1,0:T(8,128)(2,1)S(1)} %get-tuple-element.40), channel_id=1, source_target_pairs={{0,6},{1,7},{2,0},{3,1},{4,2},{5,3},{6,4},{7,5},{8,14},{9,15},{10,... | collective-permute-start | bytes 393224 | tf_op jit(solution)/shard_map/ppermute | solution.py:490
  118.1 10.2 %collective-permute-start.12 = (bf16[256,256]{1,0:T(8,128)(2,1)S(1)}, bf16[256,256]{1,0:T(8,128)(2,1)S(1)}, u32[]{:S(2)}, u32[]{:S(2)}) collective-permute-start(bf16[256,256]{1,0:T(8,128)(2,1)S(1)} %get-tuple-element.39), channel_id=1, source_target_pairs={{0,7},{1,6},{2,1},{3,0},{4,3},{5,2},{6,5},{7,4},{8,15},{9,14},{10,... | collective-permute-start | bytes 393224 | tf_op jit(solution)/shard_map/ppermute | solution.py:490
  121.2 15.6 %all-to-all-start.1 = ((bf16[16,8,2048]{2,1,0:T(8,128)(2,1)}), bf16[16,8,2048]{2,1,0:T(8,128)(2,1)S(1)}, u32[]{:S(2)}, u32[]{:S(2)}) async-start(bf16[16,8,2048]{2,1,0:T(8,128)(2,1)} %fusion), calls=%async_computation.1 | async-start | bytes 1048576 | tf_op jit(solution)/shard_map/all_to_all | solution.py:495
  128.3 3.4 %copy-start.6 = (bf16[2048,2048]{1,0:T(8,128)(2,1)S(1)}, bf16[2048,2048]{1,0:T(8,128)(2,1)}, u32[]{:S(2)}) copy-start(bf16[2048,2048]{1,0:T(8,128)(2,1)} %refs_8_.1) | copy-start | bytes 25165828
  131.7 5.1 %copy-start.10 = (s32[32,2]{0,1:T(2,128)S(1)}, s32[32,2]{0,1:T(2,128)}, u32[]{:S(2)}) copy-start(s32[32,2]{0,1:T(2,128)} %param.25) | copy-start | bytes 772
  131.7 5.1 %copy-start.11 = (f32[32,2]{0,1:T(2,128)S(1)}, f32[32,2]{0,1:T(2,128)}, u32[]{:S(2)}) copy-start(f32[32,2]{0,1:T(2,128)} %param.26) | copy-start | bytes 772

commit v7 on v6

--- a/solution.py
+++ b/solution.py
@@ -140,6 +140,32 @@
             transcendentals=rows * ff,
         ),
     )(*[vm(x) for x in (*keep, *give)], *weights)
+
+
+def sum_kernel(plan, n_in, *refs):
+    outs = refs[n_in:]
+    for out, terms in zip(outs, plan, strict=True):
+        rows = out.shape[0]
+        total = None
+        for i, at in terms:
+            term = refs[i][at : at + rows, :].astype(f32)
+            total = term if total is None else total + term
+        out[...] = total.astype(bf16)
+
+
+def sums(arrays, plan):
+    rows, width = arrays[0].shape
+    in_vmem = pl.BlockSpec(memory_space=pltpu.VMEM)
+    return pl.pallas_call(
+        functools.partial(sum_kernel, plan, len(arrays)),
+        out_shape=[pltpu.VMEM((rows, width), bf16)] * len(plan),
+        in_specs=[in_vmem] * len(arrays),
+        out_specs=[in_vmem] * len(plan),
+        compiler_params=pltpu.CompilerParams(vmem_limit_bytes=8 * MIB),
+        cost_estimate=pl.CostEstimate(
+            flops=10**9, bytes_accessed=2 * 2**20, transcendentals=0
+        ),
+    )(*[vm(v) for v in arrays])
 
 
 def local_kernel(
@@ -286,7 +312,7 @@
     return pl.pallas_call(
         middle_kernel,
         out_shape=[
-            jax.ShapeDtypeStruct((HEAD_DIM + 8, HEAD_DIM), f32),
+            pltpu.HBM((HEAD_DIM + 8, HEAD_DIM), f32),
             jax.ShapeDtypeStruct((HEAD_DIM + 8, HEAD_DIM), bf16),
         ],
         in_specs=[pl.BlockSpec(memory_space=pltpu.SMEM)]
@@ -356,39 +382,46 @@
             flops=2 * 10**9, bytes_accessed=5 * 2**20, transcendentals=2**19
         ),
         name="finish",
-    )(place, before, one, two, three, hb(kept), hb(qd), hb(gate), hb(gain))
+    )(place, hb(before), one, two, three, hb(kept), hb(qd), hb(gate), hb(gain))
 
 
 def project_kernel(head_ref, *refs):
-    pieces, w_ref, out_ref = refs[:-2], refs[-2], refs[-1]
-    total = None
-    for s, piece in enumerate(pieces):
-        at = pl.multiple_of(head_ref[s] * HEAD_DIM, HEAD_DIM)
-        part = mm(piece[...], w_ref[pl.ds(at, HEAD_DIM), :])
-        total = part if total is None else total + part
-    out_ref[...] = total.astype(bf16)
+    pieces, w_ref, out_ref, buf, sems = refs[:-4], *refs[-4:]
+    cols = out_ref.shape[1] // sems.shape[0]
+    copies = []
+    for n in range(sems.shape[0]):
+        at = pl.ds(n * cols, cols)
+        c = pltpu.make_async_copy(w_ref.at[:, at], buf.at[:, at], sems.at[n])
+        c.start()
+        copies.append(c)
+    for n, c in enumerate(copies):
+        c.wait()
+        total = None
+        for s, piece in enumerate(pieces):
+            at = pl.multiple_of(head_ref[s] * HEAD_DIM, HEAD_DIM)
+            part = mm(piece[...], buf[pl.ds(at, HEAD_DIM), n * cols : (n + 1) * cols])
+            total = part if total is None else total + part
+        out_ref[:, n * cols : (n + 1) * cols] = total.astype(bf16)
 
 
 def project(heads, pieces, w_out):
     whole, width = w_out.shape
     rows = pieces[0].shape[0]
-    cols = 512
+    in_vmem = pl.BlockSpec(memory_space=pltpu.VMEM)
     return pl.pallas_call(
         project_kernel,
-        grid_spec=pltpu.PrefetchScalarGridSpec(
-            num_scalar_prefetch=1,
-            grid=(width // cols,),
-            in_specs=[pl.BlockSpec((rows, HEAD_DIM), lambda n, heads: (0, 0))] * len(pieces)
-            + [pl.BlockSpec((whole, cols), lambda n, heads: (0, n))],
-            out_specs=pl.BlockSpec((rows, cols), lambda n, heads: (0, n)),
-        ),
         out_shape=jax.ShapeDtypeStruct((rows, width), bf16),
-        compiler_params=grid_params(12),
+        in_specs=[pl.BlockSpec(memory_space=pltpu.SMEM)]
+        + [in_vmem] * len(pieces)
+        + [pl.BlockSpec(memory_space=pl.ANY)],
+        out_specs=in_vmem,
+        scratch_shapes=[pltpu.VMEM((whole, width), bf16), pltpu.SemaphoreType.DMA((4,))],
+        compiler_params=pltpu.CompilerParams(vmem_limit_bytes=16 * MIB),
         cost_estimate=pl.CostEstimate(
             flops=4 * 10**9, bytes_accessed=10 * 2**20, transcendentals=0
         ),
         name="project",
-    )(heads, *pieces, w_out)
+    )(heads, *[vm(v) for v in pieces], hb(w_out))
 
 
 def angle_tables():
@@ -460,16 +493,13 @@
     *keep, give1 = ffn([own, up, down], [own_c, up_c, down_c], weights)
     got1 = shift(give1, "core", 1, 2)
     far_c = shift(far, "core", 1, 2)
-    near = [
-        (k.astype(f32) + got1[i * n : (i + 1) * n].astype(f32)).astype(bf16)
-        for i, k in enumerate(keep)
-    ]
-    near = lax.optimization_barrier(near)
+    near = sums([*keep, got1], tuple(((i, 0), (3, i * n)) for i in range(3)))
     back_up = shift(near[1], "y", -1)
     back_down = shift(near[2], "y", 1)
     keep2, give2 = ffn([after(far, near[2])], [far_c], weights)
     got2 = shift(give2, "core", 1, 2)
-    back_far = shift((keep2.astype(f32) + got2.astype(f32)).astype(bf16), "y", 2)
+    (away,) = sums([keep2, got2], (((0, 0), (1, 0)),))
+    back_far = shift(away, "y", 2)
     y_at, c_at = lax.axis_index("y"), lax.axis_index("core")
     place = jnp.stack([lax.axis_index("z"), y_at, c_at]).astype(jnp.int32)
     heads_out = finish(
@@ -490,8 +520,9 @@
                 piece = lax.ppermute(piece, tp, pairs)
             pieces.append(piece)
             sources.append(2 * lax.rem(y_at - dy + 4, 4) + lax.rem(c_at + dc, 2))
-    parts = (near[0], back_up, back_down, back_far)
-    expert_rows = sum(v.astype(f32) for v in parts).astype(bf16)
+    (expert_rows,) = sums(
+        [near[0], back_up, back_down, back_far], (tuple((i, 0) for i in range(4)),)
+    )
     returned = lax.all_to_all(expert_rows, ep, split_axis=0, concat_axis=0, tiled=True)
     mix_out = project(jnp.stack(sources).astype(jnp.int32), pieces, w_out)
     moe_out = pl.pallas_call(

time: 140 us -> 149 us (1.064)
  waiting for transfers between devices: 49 us -> 54.7 us
  Pallas kernels: 32.7 us -> 36.6 us
  other arithmetic: 3.36 us -> 0.16 us
  local copies, waits for them, and re-layouts: 13.8 us -> 16.2 us
    pallas_call x2 -> x5, Pallas kernels: 5.07 us -> 9.96 us  [the longest x1 6.03 us: project(): pl.pallas_call(project_kernel, out_shape=jax.ShapeDtypeStruct((rows, widt...]
    all_to_all x1, waiting for transfers between devices: 0.26 us -> 3.44 us  [on_device(): lax.all_to_all(expert_rows, ep, split_axis=0, concat_axis=0, tiled=True)]
    ppermute x18, waiting for transfers between devices: 24.7 us -> 27.8 us  [shift(): return lax.ppermute(x, axis, pairs)]
    unnamed x30 -> x40, local copies, waits for them, and re-layouts: 13.6 us -> 15.9 us
    convert_element_type x2 -> x0, other arithmetic: 2.05 us -> none  [the longest x1 1.92 us: on_device(): (k.astype(f32) + got1[i * n:(i + 1) * n].astype(f32)).astype(bf16)]
  transfers between devices with their start and end apart: 27 -> 27, of which waited for: 11 -> 11; matrix products, arithmetic and copies ran while one was open for 3% -> 0% of each run, Pallas kernels for 13% -> 16%
where the time goes in v7:
time: 149 us; the launch traced here: 148 us
  waiting for transfers between devices  54.7 us (37%)
  starting transfers between devices  39.5 us (27%)
  Pallas kernels  36.6 us (25%)
  local copies, waits for them, and re-layouts  16.2 us (11%)
    ppermute x18, waiting for transfers between devices, shift(): return lax.ppermute(x, axis, pairs)  27.8 us
    ppermute x18, starting transfers between devices, shift(): return lax.ppermute(x, axis, pairs)  19.7 us
    ppermute x7, waiting for transfers between devices, on_device(): piece = lax.ppermute(piece, tp, pairs)  17.8 us
    unnamed x40, local copies, waits for them, and re-layouts  15.9 us
    pallas_call x2, Pallas kernels, ffn(): pl.pallas_call(functools.partial(ffn_kernel, n_x), out_shape=[pltpu.VMEM(...  12.9 us
    all_to_all x1, starting transfers between devices, on_device(): own = lax.all_to_all(outgoing, ep, split_axis=0, concat_axis=0, tiled=True)  7.99 us
    ppermute x7, starting transfers between devices, on_device(): piece = lax.ppermute(piece, tp, pairs)  6.86 us
    pallas_call x1, Pallas kernels, project(): pl.pallas_call(project_kernel, out_shape=jax.ShapeDtypeStruct((rows, widt...  6.03 us
  transfers between devices with their start and end apart: 27, of which 11 were waited for; matrix products, arithmetic and copies ran while one was open for 0% of the time, Pallas kernels for 16%

profile of v7, /device:TPU:0, one launch (start us, length us, event | category | flops | bytes accessed | tf_op | source)
XLA Modules:
  0.0 148.1 jit_solution(2997839668662038492)
XLA Ops:
  0.7 2.4 %pre.1 = bf16[128,2048]{1,0:T(8,128)(2,1)} custom-call(bf16[32,2048]{1,0:T(8,128)(2,1)} %x_ref.1, s32[2,32]{1,0:T(2,128)} %bitcast.38, f32[1,2048]{1,0:T(1,128)} %bitcast.42), custom_call_target="tpu_custom_call" | custom-call | flops 2000000000 | bytes 1000000 | tf_op jit(solution)/shard_map/pre/pallas_call | solution.py:456
  3.1 8.0 %all-to-all-start = ((bf16[16,8,2048]{2,1,0:T(8,128)(2,1)}), bf16[16,8,2048]{2,1,0:T(8,128)(2,1)S(1)}, u32[]{:S(2)}, u32[]{:S(2)}) async-start(bf16[16,8,2048]{2,1,0:T(8,128)(2,1)} %bitcast.17), calls=%async_computation | async-start | bytes 1048576 | tf_op jit(solution)/shard_map/all_to_all | solution.py:463
  11.3 5.6 %local.1 = (bf16[2048,256]{1,0:T(8,128)(2,1)}, bf16[2048,256]{1,0:T(8,128)(2,1)}, bf16[264,256]{1,0:T(8,128)(2,1)S(1)}) custom-call(f32[4,2,128]{2,1,0:T(2,128)S(1)} %pad_maximum_fusion.base_ref, bf16[2048,256]{1,0:T(8,128)(2,1)S(1)} %copy-done.6, bf16[2048,256]{1,0:T(8,128)(2,1)S(1)} %copy-done.7, bf16[2048,256]{1,0:T(8,128)(2,1)} %v_ref.1, ...), custom_call_target="tpu_custom_call" | custom-call | flops 6000000000 | bytes 6291456 | tf_op jit(solution)/shard_map/local/pallas_call | solution.py:256
  17.0 5.7 %all-to-all-done = bf16[16,8,2048]{2,1,0:T(8,128)(2,1)S(1)} async-done(((bf16[16,8,2048]{2,1,0:T(8,128)(2,1)}), bf16[16,8,2048]{2,1,0:T(8,128)(2,1)S(1)}, u32[]{:S(2)}, u32[]{:S(2)}) %all-to-all-start) | async-done | bytes 524320 | tf_op jit(solution)/shard_map/all_to_all | solution.py:463
  22.6 1.6 %collective-permute-start.13 = (bf16[128,2048]{1,0:T(8,128)(2,1)S(1)}, bf16[128,2048]{1,0:T(8,128)(2,1)S(1)}, u32[]{:S(2)}, u32[]{:S(2)}) collective-permute-start(bf16[128,2048]{1,0:T(8,128)(2,1)S(1)} %bitcast.32), channel_id=1, source_target_pairs={{0,2},{2,4},{4,6},{6,0},{1,3},{3,5},{5,7},{7,1},{8,10},{10,12},{12... | collective-permute-start | bytes 1572872 | tf_op jit(solution)/shard_map/ppermute | solution.py:37
  24.2 1.7 %collective-permute-start.14 = (bf16[128,2048]{1,0:T(8,128)(2,1)S(1)}, bf16[128,2048]{1,0:T(8,128)(2,1)S(1)}, u32[]{:S(2)}, u32[]{:S(2)}) collective-permute-start(bf16[128,2048]{1,0:T(8,128)(2,1)S(1)} %bitcast.33), channel_id=1, source_target_pairs={{0,6},{2,0},{4,2},{6,4},{1,7},{3,1},{5,3},{7,5},{8,14},{10,8},{12,... | collective-permute-start | bytes 1572872 | tf_op jit(solution)/shard_map/ppermute | solution.py:37
  25.9 10.3 %collective-permute-done.13.refs_1_ = bf16[128,2048]{1,0:T(8,128)(2,1)S(1)} collective-permute-done((bf16[128,2048]{1,0:T(8,128)(2,1)S(1)}, bf16[128,2048]{1,0:T(8,128)(2,1)S(1)}, u32[]{:S(2)}, u32[]{:S(2)}) %collective-permute-start.13) | collective-permute-done | bytes 524320 | tf_op jit(solution)/shard_map/ppermute | solution.py:37
  36.7 1.4 collective-permute-done.16.refs_4_
  38.1 0.7 collective-permute-done.17.refs_5_
  38.8 2.0 %copy-done = bf16[1,2048,896]{2,1,0:T(8,128)(2,1)S(1)} copy-done((bf16[1,2048,896]{2,1,0:T(8,128)(2,1)S(1)}, bf16[1,2048,896]{2,1,0:T(8,128)(2,1)}, u32[]{:S(2)}) %copy-start) | copy-done | bytes 3670040
  40.9 2.0 %copy-done.2 = bf16[1,2048,896]{2,1,0:T(8,128)(2,1)S(1)} copy-done((bf16[1,2048,896]{2,1,0:T(8,128)(2,1)S(1)}, bf16[1,2048,896]{2,1,0:T(8,128)(2,1)}, u32[]{:S(2)}) %copy-start.2) | copy-done | bytes 3670040
  42.9 2.0 %copy-done.4 = bf16[1,896,2048]{2,1,0:T(8,128)(2,1)S(1)} copy-done((bf16[1,896,2048]{2,1,0:T(8,128)(2,1)S(1)}, bf16[1,896,2048]{2,1,0:T(8,128)(2,1)}, u32[]{:S(2)}) %copy-start.4) | copy-done | bytes 3670040
  44.9 9.6 %shard_map.176 = (bf16[128,2048]{1,0:T(8,128)(2,1)S(1)}, bf16[128,2048]{1,0:T(8,128)(2,1)S(1)}, bf16[128,2048]{1,0:T(8,128)(2,1)S(1)}, bf16[384,2048]{1,0:T(8,128)(2,1)S(1)}) custom-call(bf16[128,2048]{1,0:T(8,128)(2,1)S(1)} %bitcast.35, bf16[128,2048]{1,0:T(8,128)(2,1)S(1)} %collective-permute-done.13.refs_1_, ...), custom_call_target="tpu_custom_call" | custom-call | flops 8455716864 | bytes 17301504 | tf_op jit(solution)/shard_map/pallas_call | solution.py:129
  54.5 0.8 copy-done.13
  55.3 0.8 copy-done.15
  56.1 0.8 copy-done.17
  57.1 2.2 %collective-permute-start.21 = (bf16[128,2048]{1,0:T(8,128)(2,1)S(1)}, bf16[128,2048]{1,0:T(8,128)(2,1)S(1)}, u32[]{:S(2)}, u32[]{:S(2)}) collective-permute-start(bf16[128,2048]{1,0:T(8,128)(2,1)S(1)} %bitcast.36), channel_id=1, source_target_pairs={{0,4},{2,6},{4,0},{6,2},{1,5},{3,7},{5,1},{7,3},{8,12},{10,14},{12... | collective-permute-start | bytes 1572872 | tf_op jit(solution)/shard_map/ppermute | solution.py:37
  59.2 13.5 %collective-permute-done.21.refs_0_ = bf16[128,2048]{1,0:T(8,128)(2,1)S(1)} collective-permute-done((bf16[128,2048]{1,0:T(8,128)(2,1)S(1)}, bf16[128,2048]{1,0:T(8,128)(2,1)S(1)}, u32[]{:S(2)}, u32[]{:S(2)}) %collective-permute-start.21) | collective-permute-done | bytes 524320 | tf_op jit(solution)/shard_map/ppermute | solution.py:37
  73.3 1.7 %collective-permute-start.1 = (bf16[264,256]{1,0:T(8,128)(2,1)S(1)}, bf16[264,256]{1,0:T(8,128)(2,1)S(1)}, u32[]{:S(2)}, u32[]{:S(2)}) collective-permute-start(bf16[264,256]{1,0:T(8,128)(2,1)S(1)} %get-tuple-element.20.own_ref), channel_id=1, source_target_pairs={{0,16},{8,24},{16,0},{24,8},{1,17},{9,25},{17,1},{25,9},{2,18},{10... | collective-permute-start | bytes 405512 | tf_op jit(solution)/shard_map/ppermute | solution.py:37
  75.0 1.2 collective-permute-start.2
  76.2 1.2 copy-done.14
  77.4 1.1 copy-done.16
  78.5 1.0 copy-done.18
  79.5 1.8 %shard_map.177 = (bf16[128,2048]{1,0:T(8,128)(2,1)S(1)}, bf16[128,2048]{1,0:T(8,128)(2,1)S(1)}, bf16[128,2048]{1,0:T(8,128)(2,1)S(1)}) custom-call(bf16[128,2048]{1,0:T(8,128)(2,1)S(1)} %copy-done.14, bf16[128,2048]{1,0:T(8,128)(2,1)S(1)} %copy-done.16, bf16[128,2048]{1,0:T(8,128)(2,1)S(1)} %copy-done.18, bf16[384,2048]{1,0:T(8,128)(2,1)} %collective-permute-done.18.refs_3_), custom_call_target="tpu_custom_call" | custom-call | flops 1000000000 | bytes 2097152 | tf_op jit(solution)/shard_map/pallas_call | solution.py:159
  81.3 2.0 %copy-done.3 = bf16[1,2048,896]{2,1,0:T(8,128)(2,1)S(1)} copy-done((bf16[1,2048,896]{2,1,0:T(8,128)(2,1)S(1)}, bf16[1,2048,896]{2,1,0:T(8,128)(2,1)}, u32[]{:S(2)}) %copy-start.3) | copy-done | bytes 3670040
  83.3 2.0 %copy-done.5 = bf16[1,896,2048]{2,1,0:T(8,128)(2,1)S(1)} copy-done((bf16[1,896,2048]{2,1,0:T(8,128)(2,1)S(1)}, bf16[1,896,2048]{2,1,0:T(8,128)(2,1)}, u32[]{:S(2)}) %copy-start.5) | copy-done | bytes 3670040
  85.4 3.3 %shard_map.178 = (bf16[128,2048]{1,0:T(8,128)(2,1)S(1)}, bf16[128,2048]{1,0:T(8,128)(2,1)S(1)}) custom-call(bf16[128,2048]{1,0:T(8,128)(2,1)S(1)} %collective-permute-done.21.refs_0_, bf16[128,2048]{1,0:T(8,128)(2,1)S(1)} %collective-permute-done.22.refs_1_, bf16[2048,896]{1,0:T(8,128)(2,1)S(1)} %bitcast.26, bf16[2048,896]{1,0:T(8,128)(2,1)S(1)} %bitcast.28, ...), custom_call_target="tpu_custom_call" | custom-call | flops 2818572288 | bytes 13107200 | tf_op jit(solution)/shard_map/pallas_call | solution.py:129
  88.8 1.0 middle.1
  89.8 1.0 collective-permute-start.3
  90.8 1.7 %collective-permute-start.4 = (bf16[264,256]{1,0:T(8,128)(2,1)S(1)}, bf16[264,256]{1,0:T(8,128)(2,1)S(1)}, u32[]{:S(2)}, u32[]{:S(2)}) collective-permute-start(bf16[264,256]{1,0:T(8,128)(2,1)S(1)} %get-tuple-element.22), channel_id=1, source_target_pairs={{0,64},{32,96},{64,0},{96,32},{1,65},{33,97},{65,1},{97,33},{2,66}... | collective-permute-start | bytes 405512 | tf_op jit(solution)/shard_map/ppermute | solution.py:37
  92.5 2.1 %collective-permute-start.5 = (bf16[264,256]{1,0:T(8,128)(2,1)S(1)}, bf16[264,256]{1,0:T(8,128)(2,1)S(1)}, u32[]{:S(2)}, u32[]{:S(2)}) collective-permute-start(bf16[264,256]{1,0:T(8,128)(2,1)S(1)} %get-tuple-element.22), channel_id=1, source_target_pairs={{0,96},{32,0},{64,32},{96,64},{1,97},{33,1},{65,33},{97,65},{2,98}... | collective-permute-start | bytes 405512 | tf_op jit(solution)/shard_map/ppermute | solution.py:37
  94.7 0.9 collective-permute-start.20
  95.5 2.4 %collective-permute-start.19 = (bf16[128,2048]{1,0:T(8,128)(2,1)S(1)}, bf16[128,2048]{1,0:T(8,128)(2,1)S(1)}, u32[]{:S(2)}, u32[]{:S(2)}) collective-permute-start(bf16[128,2048]{1,0:T(8,128)(2,1)S(1)} %get-tuple-element.31), channel_id=1, source_target_pairs={{0,6},{2,0},{4,2},{6,4},{1,7},{3,1},{5,3},{7,5},{8,14},{10,8},{12,... | collective-permute-start | bytes 1572872 | tf_op jit(solution)/shard_map/ppermute | solution.py:37
  98.1 1.8 %collective-permute-done.3.one_ref = bf16[264,256]{1,0:T(8,128)(2,1)S(1)} collective-permute-done((bf16[264,256]{1,0:T(8,128)(2,1)S(1)}, bf16[264,256]{1,0:T(8,128)(2,1)S(1)}, u32[]{:S(2)}, u32[]{:S(2)}) %collective-permute-start.3) | collective-permute-done | bytes 135200 | tf_op jit(solution)/shard_map/ppermute | solution.py:37
  99.9 2.2 %collective-permute-start.24 = (bf16[128,2048]{1,0:T(8,128)(2,1)S(1)}, bf16[128,2048]{1,0:T(8,128)(2,1)S(1)}, u32[]{:S(2)}, u32[]{:S(2)}) collective-permute-start(bf16[128,2048]{1,0:T(8,128)(2,1)S(1)} %shard_map.179), channel_id=1, source_target_pairs={{0,4},{2,6},{4,0},{6,2},{1,5},{3,7},{5,1},{7,3},{8,12},{10,14},{12... | collective-permute-start | bytes 1572872 | tf_op jit(solution)/shard_map/ppermute | solution.py:37
  102.1 4.5 %finish.1 = bf16[2048,256]{1,0:T(8,128)(2,1)S(1)} custom-call(s32[3]{0:T(128)S(1)} %pad_add_fusion.place_ref, f32[264,256]{1,0:T(8,128)} %get-tuple-element.21.before_ref, bf16[264,256]{1,0:T(8,128)(2,1)S(1)} %collective-permute-done.3.one_ref, bf16[264,256]{1,0:T(8,128)(2,1)S(1)} %collective-permute-done.4.two_ref, ...), custom_call_target="tpu_custom_call" | custom-call | flops 2000000000 | bytes 5242880 | tf_op jit(solution)/shard_map/finish/pallas_call | solution.py:366
  106.7 1.0 collective-permute-start.7
  108.0 0.6 collective-permute-start.8
  108.7 15.3 %collective-permute-done.7.refs_2_ = bf16[256,256]{1,0:T(8,128)(2,1)S(1)} collective-permute-done((bf16[256,256]{1,0:T(8,128)(2,1)S(1)}, bf16[256,256]{1,0:T(8,128)(2,1)S(1)}, u32[]{:S(2)}, u32[]{:S(2)}) %collective-permute-start.7) | collective-permute-done | bytes 131104 | tf_op jit(solution)/shard_map/ppermute | solution.py:520
  123.9 0.8 collective-permute-start.9
  124.8 1.8 %collective-permute-start.10 = (bf16[256,256]{1,0:T(8,128)(2,1)S(1)}, bf16[256,256]{1,0:T(8,128)(2,1)S(1)}, u32[]{:S(2)}, u32[]{:S(2)}) collective-permute-start(bf16[256,256]{1,0:T(8,128)(2,1)S(1)} %get-tuple-element.38), channel_id=1, source_target_pairs={{0,5},{1,4},{2,7},{3,6},{4,1},{5,0},{6,3},{7,2},{8,13},{9,12},{10,... | collective-permute-start | bytes 393224 | tf_op jit(solution)/shard_map/ppermute | solution.py:520
  127.2 1.9 %collective-permute-start.12 = (bf16[256,256]{1,0:T(8,128)(2,1)S(1)}, bf16[256,256]{1,0:T(8,128)(2,1)S(1)}, u32[]{:S(2)}, u32[]{:S(2)}) collective-permute-start(bf16[256,256]{1,0:T(8,128)(2,1)S(1)} %get-tuple-element.36), channel_id=1, source_target_pairs={{0,7},{1,6},{2,1},{3,0},{4,3},{5,2},{6,5},{7,4},{8,15},{9,14},{10,... | collective-permute-start | bytes 393224 | tf_op jit(solution)/shard_map/ppermute | solution.py:520
  129.1 1.0 shard_map.180
  130.2 4.9 %all-to-all-start.1 = ((bf16[16,8,2048]{2,1,0:T(8,128)(2,1)}), bf16[16,8,2048]{2,1,0:T(8,128)(2,1)S(1)}, u32[]{:S(2)}, u32[]{:S(2)}) async-start(bf16[16,8,2048]{2,1,0:T(8,128)(2,1)} %bitcast.22), calls=%async_computation.1 | async-start | bytes 1048576 | tf_op jit(solution)/shard_map/all_to_all | solution.py:526
  135.9 1.5 %collective-permute-done.12.refs_7_ = bf16[256,256]{1,0:T(8,128)(2,1)S(1)} collective-permute-done((bf16[256,256]{1,0:T(8,128)(2,1)S(1)}, bf16[256,256]{1,0:T(8,128)(2,1)S(1)}, u32[]{:S(2)}, u32[]{:S(2)}) %collective-permute-start.12) | collective-permute-done | bytes 131104 | tf_op jit(solution)/shard_map/ppermute | solution.py:520
  137.4 6.0 %project.1 = bf16[256,2048]{1,0:T(8,128)(2,1)} custom-call(s32[8]{0:T(128)S(1)} %stack.52.head_ref, bf16[256,256]{1,0:T(8,128)(2,1)S(1)} %get-tuple-element.43.refs_0_, bf16[256,256]{1,0:T(8,128)(2,1)S(1)} %collective-permute-done.6.refs_1_, bf16[256,256]{1,0:T(8,128)(2,1)S(1)} %collective-permute-done.7.refs_2_, ...), custom_call_target="tpu_custom_call" | custom-call | flops 4000000000 | bytes 10485760 | tf_op jit(solution)/shard_map/project/pallas_call | solution.py:411
  143.4 3.4 %all-to-all-done.1 = bf16[16,8,2048]{2,1,0:T(8,128)(2,1)S(1)} async-done(((bf16[16,8,2048]{2,1,0:T(8,128)(2,1)}), bf16[16,8,2048]{2,1,0:T(8,128)(2,1)S(1)}, u32[]{:S(2)}, u32[]{:S(2)}) %all-to-all-start.1) | async-done | bytes 524320 | tf_op jit(solution)/shard_map/all_to_all | solution.py:526
  146.9 1.2 combine.1
  (64 shorter events, 3.6 us)
Async XLA Ops:
  0.6 10.6 %copy-start.19 = (f32[128]{0:T(128)S(1)}, f32[128]{0:T(128)}, u32[]{:S(2)}) copy-start(f32[128]{0:T(128)} %constant.52.clone) | copy-start | bytes 1540
  0.6 10.6 %copy-start.6 = (bf16[2048,256]{1,0:T(8,128)(2,1)S(1)}, bf16[2048,256]{1,0:T(8,128)(2,1)}, u32[]{:S(2)}) copy-start(bf16[2048,256]{1,0:T(8,128)(2,1)} %q_ref) | copy-start | bytes 3145732
  0.7 10.6 %copy-start.7 = (bf16[2048,256]{1,0:T(8,128)(2,1)S(1)}, bf16[2048,256]{1,0:T(8,128)(2,1)}, u32[]{:S(2)}) copy-start(bf16[2048,256]{1,0:T(8,128)(2,1)} %k_ref.1) | copy-start | bytes 3145732
  0.7 10.6 %copy-start.8 = (f32[2048,1]{0,1:T(1,128)S(1)}, f32[2048,1]{0,1:T(1,128)}, u32[]{:S(2)}) copy-start(f32[2048,1]{0,1:T(1,128)} %param.21) | copy-start | bytes 24580
  0.7 10.6 %copy-start.11 = (f32[512,128]{1,0:T(8,128)S(1)}, f32[512,128]{1,0:T(8,128)}, u32[]{:S(2)}) copy-start(f32[512,128]{1,0:T(8,128)} %constant.53.clone.cos_ref) | copy-start | bytes 786436
  0.7 10.6 %copy-start.12 = (f32[512,128]{1,0:T(8,128)S(1)}, f32[512,128]{1,0:T(8,128)}, u32[]{:S(2)}) copy-start(f32[512,128]{1,0:T(8,128)} %constant.54.clone.sin_ref) | copy-start | bytes 786436
  3.1 19.5 %all-to-all-start = ((bf16[16,8,2048]{2,1,0:T(8,128)(2,1)}), bf16[16,8,2048]{2,1,0:T(8,128)(2,1)S(1)}, u32[]{:S(2)}, u32[]{:S(2)}) async-start(bf16[16,8,2048]{2,1,0:T(8,128)(2,1)} %bitcast.17), calls=%async_computation | async-start | bytes 1048576 | tf_op jit(solution)/shard_map/all_to_all | solution.py:463
  22.6 13.5 %collective-permute-start.13 = (bf16[128,2048]{1,0:T(8,128)(2,1)S(1)}, bf16[128,2048]{1,0:T(8,128)(2,1)S(1)}, u32[]{:S(2)}, u32[]{:S(2)}) collective-permute-start(bf16[128,2048]{1,0:T(8,128)(2,1)S(1)} %bitcast.32), channel_id=1, source_target_pairs={{0,2},{2,4},{4,6},{6,0},{1,3},{3,5},{5,7},{7,1},{8,10},{10,12},{12... | collective-permute-start | bytes 1572872 | tf_op jit(solution)/shard_map/ppermute | solution.py:37
  24.2 12.0 %collective-permute-start.14 = (bf16[128,2048]{1,0:T(8,128)(2,1)S(1)}, bf16[128,2048]{1,0:T(8,128)(2,1)S(1)}, u32[]{:S(2)}, u32[]{:S(2)}) collective-permute-start(bf16[128,2048]{1,0:T(8,128)(2,1)S(1)} %bitcast.33), channel_id=1, source_target_pairs={{0,6},{2,0},{4,2},{6,4},{1,7},{3,1},{5,3},{7,5},{8,14},{10,8},{12,... | collective-permute-start | bytes 1572872 | tf_op jit(solution)/shard_map/ppermute | solution.py:37
  25.9 10.8 %collective-permute-start.15 = (bf16[128,2048]{1,0:T(8,128)(2,1)S(1)}, bf16[128,2048]{1,0:T(8,128)(2,1)S(1)}, u32[]{:S(2)}, u32[]{:S(2)}) collective-permute-start(bf16[128,2048]{1,0:T(8,128)(2,1)S(1)} %bitcast.34), channel_id=1, source_target_pairs={{0,1},{1,0},{2,3},{3,2},{4,5},{5,4},{6,7},{7,6},{8,9},{9,8},{10,11... | collective-permute-start | bytes 1572872 | tf_op jit(solution)/shard_map/ppermute | solution.py:37
  36.2 1.9 %collective-permute-start.16 = (bf16[128,2048]{1,0:T(8,128)(2,1)S(1)}, bf16[128,2048]{1,0:T(8,128)(2,1)S(1)}, u32[]{:S(2)}, u32[]{:S(2)}) collective-permute-start(bf16[128,2048]{1,0:T(8,128)(2,1)S(1)} %collective-permute-done.13.refs_1_), channel_id=1, source_target_pairs={{0,1},{1,0},{2,3},{3,2},{4,5},{5,4},{6,7},{7,6},{8,9},{9,8},{10,11... | collective-permute-start | bytes 1572872 | tf_op jit(solution)/shard_map/ppermute | solution.py:37
  36.2 2.6 %collective-permute-start.17 = (bf16[128,2048]{1,0:T(8,128)(2,1)S(1)}, bf16[128,2048]{1,0:T(8,128)(2,1)S(1)}, u32[]{:S(2)}, u32[]{:S(2)}) collective-permute-start(bf16[128,2048]{1,0:T(8,128)(2,1)S(1)} %collective-permute-done.14.refs_2_), channel_id=1, source_target_pairs={{0,1},{1,0},{2,3},{3,2},{4,5},{5,4},{6,7},{7,6},{8,9},{9,8},{10,11... | collective-permute-start | bytes 1572872 | tf_op jit(solution)/shard_map/ppermute | solution.py:37
  38.8 2.0 %copy-start = (bf16[1,2048,896]{2,1,0:T(8,128)(2,1)S(1)}, bf16[1,2048,896]{2,1,0:T(8,128)(2,1)}, u32[]{:S(2)}) copy-start(bf16[1,2048,896]{2,1,0:T(8,128)(2,1)} %param.28) | copy-start | bytes 11010052
  40.9 2.0 %copy-start.2 = (bf16[1,2048,896]{2,1,0:T(8,128)(2,1)S(1)}, bf16[1,2048,896]{2,1,0:T(8,128)(2,1)}, u32[]{:S(2)}) copy-start(bf16[1,2048,896]{2,1,0:T(8,128)(2,1)} %param.29) | copy-start | bytes 11010052
  42.9 2.0 %copy-start.4 = (bf16[1,896,2048]{2,1,0:T(8,128)(2,1)S(1)}, bf16[1,896,2048]{2,1,0:T(8,128)(2,1)}, u32[]{:S(2)}) copy-start(bf16[1,896,2048]{2,1,0:T(8,128)(2,1)} %param.30) | copy-start | bytes 11010052
  54.5 0.8 copy-start.13
  55.3 0.8 copy-start.15
  56.1 0.8 copy-start.17
  56.9 19.3 %collective-permute-start.18 = (bf16[384,2048]{1,0:T(8,128)(2,1)S(1)}, bf16[384,2048]{1,0:T(8,128)(2,1)}, u32[]{:S(2)}, u32[]{:S(2)}) collective-permute-start(bf16[384,2048]{1,0:T(8,128)(2,1)S(1)} %get-tuple-element.29), channel_id=1, source_target_pairs={{0,1},{1,0},{2,3},{3,2},{4,5},{5,4},{6,7},{7,6},{8,9},{9,8},{10,11... | collective-permute-start | bytes 4718600 | tf_op jit(solution)/shard_map/ppermute | solution.py:37
  57.1 15.7 %collective-permute-start.21 = (bf16[128,2048]{1,0:T(8,128)(2,1)S(1)}, bf16[128,2048]{1,0:T(8,128)(2,1)S(1)}, u32[]{:S(2)}, u32[]{:S(2)}) collective-permute-start(bf16[128,2048]{1,0:T(8,128)(2,1)S(1)} %bitcast.36), channel_id=1, source_target_pairs={{0,4},{2,6},{4,0},{6,2},{1,5},{3,7},{5,1},{7,3},{8,12},{10,14},{12... | collective-permute-start | bytes 1572872 | tf_op jit(solution)/shard_map/ppermute | solution.py:37
  72.8 8.5 %collective-permute-start.22 = (bf16[128,2048]{1,0:T(8,128)(2,1)S(1)}, bf16[128,2048]{1,0:T(8,128)(2,1)S(1)}, u32[]{:S(2)}, u32[]{:S(2)}) collective-permute-start(bf16[128,2048]{1,0:T(8,128)(2,1)S(1)} %collective-permute-done.21.refs_0_), channel_id=1, source_target_pairs={{0,1},{1,0},{2,3},{3,2},{4,5},{5,4},{6,7},{7,6},{8,9},{9,8},{10,11... | collective-permute-start | bytes 1572872 | tf_op jit(solution)/shard_map/ppermute | solution.py:37
  72.8 16.0 %collective-permute-start = (bf16[264,256]{1,0:T(8,128)(2,1)S(1)}, bf16[264,256]{1,0:T(8,128)(2,1)S(1)}, u32[]{:S(2)}, u32[]{:S(2)}) collective-permute-start(bf16[264,256]{1,0:T(8,128)(2,1)S(1)} %get-tuple-element.20.own_ref), channel_id=1, source_target_pairs={{0,8},{8,16},{16,24},{24,0},{1,9},{9,17},{17,25},{25,1},{2,10},{10... | collective-permute-start | bytes 405512 | tf_op jit(solution)/shard_map/ppermute | solution.py:37
  73.3 15.5 %collective-permute-start.1 = (bf16[264,256]{1,0:T(8,128)(2,1)S(1)}, bf16[264,256]{1,0:T(8,128)(2,1)S(1)}, u32[]{:S(2)}, u32[]{:S(2)}) collective-permute-start(bf16[264,256]{1,0:T(8,128)(2,1)S(1)} %get-tuple-element.20.own_ref), channel_id=1, source_target_pairs={{0,16},{8,24},{16,0},{24,8},{1,17},{9,25},{17,1},{25,9},{2,18},{10... | collective-permute-start | bytes 405512 | tf_op jit(solution)/shard_map/ppermute | solution.py:37
  75.0 13.8 %collective-permute-start.2 = (bf16[264,256]{1,0:T(8,128)(2,1)S(1)}, bf16[264,256]{1,0:T(8,128)(2,1)S(1)}, u32[]{:S(2)}, u32[]{:S(2)}) collective-permute-start(bf16[264,256]{1,0:T(8,128)(2,1)S(1)} %get-tuple-element.20.own_ref), channel_id=1, source_target_pairs={{0,24},{8,0},{16,8},{24,16},{1,25},{9,1},{17,9},{25,17},{2,26},{10... | collective-permute-start | bytes 405512 | tf_op jit(solution)/shard_map/ppermute | solution.py:37
  76.2 5.1 %copy-start.1 = (bf16[1,2048,896]{2,1,0:T(8,128)(2,1)S(1)}, bf16[1,2048,896]{2,1,0:T(8,128)(2,1)}, u32[]{:S(2)}) copy-start(bf16[1,2048,896]{2,1,0:T(8,128)(2,1)} %param.28) | copy-start | bytes 11010052
  76.2 1.2 copy-start.14
  77.4 1.1 copy-start.16
  78.5 1.0 copy-start.18
  81.3 2.0 %copy-start.3 = (bf16[1,2048,896]{2,1,0:T(8,128)(2,1)S(1)}, bf16[1,2048,896]{2,1,0:T(8,128)(2,1)}, u32[]{:S(2)}) copy-start(bf16[1,2048,896]{2,1,0:T(8,128)(2,1)} %param.29) | copy-start | bytes 11010052
  83.3 2.0 %copy-start.5 = (bf16[1,896,2048]{2,1,0:T(8,128)(2,1)S(1)}, bf16[1,896,2048]{2,1,0:T(8,128)(2,1)}, u32[]{:S(2)}) copy-start(bf16[1,896,2048]{2,1,0:T(8,128)(2,1)} %param.30) | copy-start | bytes 11010052
  88.7 6.8 %collective-permute-start.23 = (bf16[128,2048]{1,0:T(8,128)(2,1)S(1)}, bf16[128,2048]{1,0:T(8,128)(2,1)S(1)}, u32[]{:S(2)}, u32[]{:S(2)}) collective-permute-start(bf16[128,2048]{1,0:T(8,128)(2,1)S(1)} %get-tuple-element.35), channel_id=1, source_target_pairs={{0,1},{1,0},{2,3},{3,2},{4,5},{5,4},{6,7},{7,6},{8,9},{9,8},{10,11... | collective-permute-start | bytes 1572872 | tf_op jit(solution)/shard_map/ppermute | solution.py:37
  89.8 10.1 %collective-permute-start.3 = (bf16[264,256]{1,0:T(8,128)(2,1)S(1)}, bf16[264,256]{1,0:T(8,128)(2,1)S(1)}, u32[]{:S(2)}, u32[]{:S(2)}) collective-permute-start(bf16[264,256]{1,0:T(8,128)(2,1)S(1)} %get-tuple-element.22), channel_id=1, source_target_pairs={{0,32},{32,64},{64,96},{96,0},{1,33},{33,65},{65,97},{97,1},{2,34}... | collective-permute-start | bytes 405512 | tf_op jit(solution)/shard_map/ppermute | solution.py:37
  90.8 11.3 %collective-permute-start.4 = (bf16[264,256]{1,0:T(8,128)(2,1)S(1)}, bf16[264,256]{1,0:T(8,128)(2,1)S(1)}, u32[]{:S(2)}, u32[]{:S(2)}) collective-permute-start(bf16[264,256]{1,0:T(8,128)(2,1)S(1)} %get-tuple-element.22), channel_id=1, source_target_pairs={{0,64},{32,96},{64,0},{96,32},{1,65},{33,97},{65,1},{97,33},{2,66}... | collective-permute-start | bytes 405512 | tf_op jit(solution)/shard_map/ppermute | solution.py:37
  92.5 9.6 %collective-permute-start.5 = (bf16[264,256]{1,0:T(8,128)(2,1)S(1)}, bf16[264,256]{1,0:T(8,128)(2,1)S(1)}, u32[]{:S(2)}, u32[]{:S(2)}) collective-permute-start(bf16[264,256]{1,0:T(8,128)(2,1)S(1)} %get-tuple-element.22), channel_id=1, source_target_pairs={{0,96},{32,0},{64,32},{96,64},{1,97},{33,1},{65,33},{97,65},{2,98}... | collective-permute-start | bytes 405512 | tf_op jit(solution)/shard_map/ppermute | solution.py:37
  94.7 31.9 %collective-permute-start.20 = (bf16[128,2048]{1,0:T(8,128)(2,1)S(1)}, bf16[128,2048]{1,0:T(8,128)(2,1)S(1)}, u32[]{:S(2)}, u32[]{:S(2)}) collective-permute-start(bf16[128,2048]{1,0:T(8,128)(2,1)S(1)} %get-tuple-element.32), channel_id=1, source_target_pairs={{0,2},{2,4},{4,6},{6,0},{1,3},{3,5},{5,7},{7,1},{8,10},{10,12},{12... | collective-permute-start | bytes 1572872 | tf_op jit(solution)/shard_map/ppermute | solution.py:37
  95.5 29.2 %collective-permute-start.19 = (bf16[128,2048]{1,0:T(8,128)(2,1)S(1)}, bf16[128,2048]{1,0:T(8,128)(2,1)S(1)}, u32[]{:S(2)}, u32[]{:S(2)}) collective-permute-start(bf16[128,2048]{1,0:T(8,128)(2,1)S(1)} %get-tuple-element.31), channel_id=1, source_target_pairs={{0,6},{2,0},{4,2},{6,4},{1,7},{3,1},{5,3},{7,5},{8,14},{10,8},{12,... | collective-permute-start | bytes 1572872 | tf_op jit(solution)/shard_map/ppermute | solution.py:37
  99.9 27.3 %collective-permute-start.24 = (bf16[128,2048]{1,0:T(8,128)(2,1)S(1)}, bf16[128,2048]{1,0:T(8,128)(2,1)S(1)}, u32[]{:S(2)}, u32[]{:S(2)}) collective-permute-start(bf16[128,2048]{1,0:T(8,128)(2,1)S(1)} %shard_map.179), channel_id=1, source_target_pairs={{0,4},{2,6},{4,0},{6,2},{1,5},{3,7},{5,1},{7,3},{8,12},{10,14},{12... | collective-permute-start | bytes 1572872 | tf_op jit(solution)/shard_map/ppermute | solution.py:37
  106.6 1.4 collective-permute-start.6
  106.7 17.2 %collective-permute-start.7 = (bf16[256,256]{1,0:T(8,128)(2,1)S(1)}, bf16[256,256]{1,0:T(8,128)(2,1)S(1)}, u32[]{:S(2)}, u32[]{:S(2)}) collective-permute-start(bf16[256,256]{1,0:T(8,128)(2,1)S(1)} %get-tuple-element.41), channel_id=1, source_target_pairs={{0,2},{1,3},{2,4},{3,5},{4,6},{5,7},{6,0},{7,1},{8,10},{9,11},{10,... | collective-permute-start | bytes 393224 | tf_op jit(solution)/shard_map/ppermute | solution.py:520
  108.0 27.2 %collective-permute-start.8 = (bf16[256,256]{1,0:T(8,128)(2,1)S(1)}, bf16[256,256]{1,0:T(8,128)(2,1)S(1)}, u32[]{:S(2)}, u32[]{:S(2)}) collective-permute-start(bf16[256,256]{1,0:T(8,128)(2,1)S(1)} %get-tuple-element.40), channel_id=1, source_target_pairs={{0,3},{1,2},{2,5},{3,4},{4,7},{5,6},{6,1},{7,0},{8,11},{9,10},{10,... | collective-permute-start | bytes 393224 | tf_op jit(solution)/shard_map/ppermute | solution.py:520
  123.9 11.3 %collective-permute-start.9 = (bf16[256,256]{1,0:T(8,128)(2,1)S(1)}, bf16[256,256]{1,0:T(8,128)(2,1)S(1)}, u32[]{:S(2)}, u32[]{:S(2)}) collective-permute-start(bf16[256,256]{1,0:T(8,128)(2,1)S(1)} %get-tuple-element.39), channel_id=1, source_target_pairs={{0,4},{1,5},{2,6},{3,7},{4,0},{5,1},{6,2},{7,3},{8,12},{9,13},{10,... | collective-permute-start | bytes 393224 | tf_op jit(solution)/shard_map/ppermute | solution.py:520
  124.8 10.5 %collective-permute-start.10 = (bf16[256,256]{1,0:T(8,128)(2,1)S(1)}, bf16[256,256]{1,0:T(8,128)(2,1)S(1)}, u32[]{:S(2)}, u32[]{:S(2)}) collective-permute-start(bf16[256,256]{1,0:T(8,128)(2,1)S(1)} %get-tuple-element.38), channel_id=1, source_target_pairs={{0,5},{1,4},{2,7},{3,6},{4,1},{5,0},{6,3},{7,2},{8,13},{9,12},{10,... | collective-permute-start | bytes 393224 | tf_op jit(solution)/shard_map/ppermute | solution.py:520
  126.6 9.3 %collective-permute-start.11 = (bf16[256,256]{1,0:T(8,128)(2,1)S(1)}, bf16[256,256]{1,0:T(8,128)(2,1)S(1)}, u32[]{:S(2)}, u32[]{:S(2)}) collective-permute-start(bf16[256,256]{1,0:T(8,128)(2,1)S(1)} %get-tuple-element.37), channel_id=1, source_target_pairs={{0,6},{1,7},{2,0},{3,1},{4,2},{5,3},{6,4},{7,5},{8,14},{9,15},{10,... | collective-permute-start | bytes 393224 | tf_op jit(solution)/shard_map/ppermute | solution.py:520
  127.2 10.2 %collective-permute-start.12 = (bf16[256,256]{1,0:T(8,128)(2,1)S(1)}, bf16[256,256]{1,0:T(8,128)(2,1)S(1)}, u32[]{:S(2)}, u32[]{:S(2)}) collective-permute-start(bf16[256,256]{1,0:T(8,128)(2,1)S(1)} %get-tuple-element.36), channel_id=1, source_target_pairs={{0,7},{1,6},{2,1},{3,0},{4,3},{5,2},{6,5},{7,4},{8,15},{9,14},{10,... | collective-permute-start | bytes 393224 | tf_op jit(solution)/shard_map/ppermute | solution.py:520
  130.2 16.7 %all-to-all-start.1 = ((bf16[16,8,2048]{2,1,0:T(8,128)(2,1)}), bf16[16,8,2048]{2,1,0:T(8,128)(2,1)S(1)}, u32[]{:S(2)}, u32[]{:S(2)}) async-start(bf16[16,8,2048]{2,1,0:T(8,128)(2,1)} %bitcast.22), calls=%async_computation.1 | async-start | bytes 1048576 | tf_op jit(solution)/shard_map/all_to_all | solution.py:526
  137.4 9.5 %copy-start.9 = (s32[32,2]{0,1:T(2,128)S(1)}, s32[32,2]{0,1:T(2,128)}, u32[]{:S(2)}) copy-start(s32[32,2]{0,1:T(2,128)} %param.25) | copy-start | bytes 772
  137.4 9.5 %copy-start.10 = (f32[32,2]{0,1:T(2,128)S(1)}, f32[32,2]{0,1:T(2,128)}, u32[]{:S(2)}) copy-start(f32[32,2]{0,1:T(2,128)} %param.26) | copy-start | bytes 772
